TPU v7x, 256 devices: a whole 4x4x8 slice. The times are simulated.
256 devices in a mesh: sp: 32 (over z, y), fs: 4 (over x), tp: 2 (over core).
Axes of the slice: x: 4, y: 4, z: 8, core: 2. Of those that a mesh axis runs over, the one named last changes fastest.
Arguments:
- tokens: bfloat16 [4, 4096, 4096], P('fs', 'sp'), may hold values from -6 to 6
- norm_gain: float32 [4096], replicated, may hold values from 0.1 to 1.9
- pool_proj: bfloat16 [4096, 1024], P(('sp', 'fs'), 'tp'), may hold values from -0.09375 to 0.09375
- query_proj: bfloat16 [4096, 1024], P(('sp', 'fs'), 'tp'), may hold values from -0.09375 to 0.09375
- key_proj: bfloat16 [4096, 1024], P(('sp', 'fs'), 'tp'), may hold values from -0.09375 to 0.09375
- value_proj: bfloat16 [4096, 1024], P(('sp', 'fs'), 'tp'), may hold values from -0.09375 to 0.09375
- pool_map: bfloat16 [4, 256, 256], replicated, may hold values from -0.375 to 0.375
- pool_scale: float32 [1024], replicated, may hold values from 0.1 to 1.9
- decay_rate: float32 [4], P('tp'), may hold values from 2e-05 to 0.034
- start_state: float32 [4, 4, 256, 256], P('fs', 'tp', 'sp'), may hold values from -96 to 96
- pool_back: bfloat16 [1024, 4096], P('tp', ('sp', 'fs')), may hold values from -0.125 to 0.125
- retention_back: bfloat16 [1024, 4096], P('tp', ('sp', 'fs')), may hold values from -0.125 to 0.125
Outputs:
- mixed: bfloat16 [4, 4096, 4096], P('fs', ('sp', 'tp'))
All inputs are finite; a program needn't handle non-finite values.
Results may differ from a plain program's by a relative error of at most 0.014.
Values may be sent and summed in bfloat16 or wider, within the bound.
No kernel may reach another device: no remote copies, remote signals or barrier semaphores. Data moves between devices by JAX's collectives and lax.ppermute only.
A program may use at most 128 MiB of HBM per device.

v0:
```python
import jax
import jax.numpy as jnp
from jax import lax
from jax.experimental import pallas as pl
from jax.experimental.pallas import tpu as pltpu
from jax.sharding import Mesh
from jax.sharding import PartitionSpec as P

NZ, NY, NX = 8, 4, 4
SPAN = 512
HALO = 16
HEAD = 256
HALF = 128
eps = 1e-06
rope_base = 10000.0

bf16 = jnp.bfloat16
f32 = jnp.float32


def ring(n, k):
    return [(i, (i + k) % n) for i in range(n)]


def line(n, k):
    return [(i, i + k) for i in range(n - k)]


def to_heads(k):
    return [(2 * y + c, 2 * (2 * c + (k + y) % 2) + y // 2) for y in range(NY) for c in range(2)]


SWAP = [(0, 1), (1, 0)]


def swap(a):
    return lax.ppermute(a, "c", SWAP)


def direct(a, axis, n):
    return [a] + [lax.ppermute(a, axis, ring(n, k)) for k in range(1, n)]


def z_ring(a, halves):
    chunks = [None] * NZ
    chunks[0] = a
    up = down = a
    for s in range(1, 4):
        up = lax.ppermute(up, "z", ring(NZ, 1))
        down = lax.ppermute(down, "z", ring(NZ, -1))
        chunks[NZ - s], chunks[s] = up, down
    if not halves:
        chunks[4] = lax.ppermute(up, "z", ring(NZ, 1))
        return chunks
    n = a.shape[0] // 2
    return chunks[:4] + chunks[5:] + [lax.ppermute(up[:n], "z", ring(NZ, 1)), lax.ppermute(down[n:], "z", ring(NZ, -1))]


VM = pl.BlockSpec(memory_space=pltpu.VMEM)
SM = pl.BlockSpec(memory_space=pltpu.SMEM)
ANY = pl.BlockSpec(memory_space=pl.ANY)
ROWS = 112


def pack_body(at, pool, query, key, value, state, pback, rback, s0, s1):
    y = at[1]
    eye = (lax.broadcasted_iota(jnp.int32, (32, 32), 0) == lax.broadcasted_iota(jnp.int32, (32, 32), 1)).astype(bf16)

    def turned(ref, rows):
        return lax.dot_general(eye, ref[rows, :], (((1,), (1,)), ((), ())), preferred_element_type=f32).astype(bf16)

    for k, out in enumerate((s0, s1)):
        p = (y + k) % 2
        at_head = pl.ds(pl.multiple_of(p * HEAD, HEAD), HEAD)
        out[0:32, :256] = key[:, at_head]
        out[0:32, 256:] = value[:, at_head]
        out[32:64, :256] = pool[:, at_head]
        out[32:64, 256:] = query[:, at_head]
        out[64:96, :256] = turned(pback, at_head)
        out[64:96, 256:] = turned(rback, at_head)
        s = state[p]
        hi = s.astype(bf16)
        lo = (s - hi.astype(f32)).astype(bf16)
        out[96:112, :256] = jnp.concatenate([hi, hi], axis=0)
        out[96:112, 256:] = jnp.concatenate([lo, lo], axis=0)


def pack(at, *args):
    return pl.pallas_call(
        pack_body, in_specs=[SM] + [VM] * 7, out_specs=[VM] * 2,
        out_shape=[jax.ShapeDtypeStruct((ROWS, 512), bf16)] * 2, name="pack",
    )(at, *args)


def norm_body(at, tok, gain, out, full):
    x, c = at[2], at[3]
    v = tok[...].astype(f32)
    v = v * lax.rsqrt(jnp.mean(v * v, axis=-1, keepdims=True) + eps) * gain[...]
    full[...] = v.astype(bf16)
    lane_in = lax.broadcasted_iota(jnp.int32, (256, 256), 0)
    lane_out = lax.broadcasted_iota(jnp.int32, (256, 256), 1)
    source = (lane_out % 64) // 32 * 128 + (x + NX - lane_out // 64) % NX * 32 + lane_out % 32
    order = (lane_in == source).astype(bf16)
    for zs in range(NZ):
        part = full[:, pl.ds(pl.multiple_of(zs * 512 + c * 256, 256), 256)]
        out[zs] = jnp.dot(part, order, preferred_element_type=f32).astype(bf16)


def norm(at, tok, gain):
    return pl.pallas_call(
        norm_body, in_specs=[SM, VM, VM], out_specs=VM,
        out_shape=jax.ShapeDtypeStruct((NZ, HALF, 256), bf16),
        scratch_shapes=[pltpu.VMEM((HALF, 4096), bf16)], name="norm",
    )(at, tok, gain)


def split_body(at, *refs):
    z, y, c = at[0], at[1], at[3]
    ins, (kv, pq, keep, give) = refs[:NZ], refs[NZ:]
    for kz in range(NZ):
        kv[kz * 64:kz * 64 + 64, :] = ins[kz][0:64, :]
        pq[kz * 64:kz * 64 + 64, :] = ins[kz][64:128, :]
        for out, half in ((keep, c), (give, 1 - c)):
            hi = ins[kz][128:144, pl.ds(pl.multiple_of(half * HALF, HALF), HALF)].astype(f32)
            lo = ins[kz][128:144, pl.ds(pl.multiple_of(HEAD + half * HALF, HALF), HALF)].astype(f32)
            rows = hi + lo
            for k in range(2):
                at_row = ((z + kz) % NZ) * 16 + ((y + k) % 2) * 8
                out[pl.ds(pl.multiple_of(at_row, 8), 8), :] = rows[k * 8:k * 8 + 8]


def split(at, chunks):
    return pl.pallas_call(
        split_body, in_specs=[SM] + [VM] * NZ, out_specs=[VM] * 4,
        out_shape=[jax.ShapeDtypeStruct((512, 512), bf16)] * 2 + [jax.ShapeDtypeStruct((HALF, HALF), f32)] * 2,
        name="split",
    )(at, *chunks)


def lhs_body(at, t0, t1, t2, t3, out):
    z, y = at[0], at[1]
    for k, t in enumerate((t0, t1, t2, t3)):
        rows = pl.ds(pl.multiple_of(((y + NY - k) % NY) * HALF, HALF), HALF)
        for kz in range(NZ):
            out[rows, kz * 256:(kz + 1) * 256] = t[(z + kz) % NZ]


def gather_rows(at, toks):
    return pl.pallas_call(
        lhs_body, in_specs=[SM] + [VM] * 4, out_specs=VM,
        out_shape=jax.ShapeDtypeStruct((SPAN, 2048), bf16), name="rows",
    )(at, *toks)


def place_in(y, ws, rhs):
    for kx, w in enumerate(ws):
        for k in range(2):
            par = (y + k) % 2
            for kz in range(NZ):
                rhs[pl.ds(pl.multiple_of(kz * 256 + kx * 64 + par * 32, 32), 32), :] = w[kz * 64 + k * 32:kz * 64 + k * 32 + 32, :]


def kv_body(at, lhs, w0, w1, w2, w3, kpart, vkeep, send, rhs, res):
    y, c = at[1], at[3]
    place_in(y, (w0, w1, w2, w3), rhs)
    res[...] = jnp.dot(lhs[...], rhs[...], preferred_element_type=f32)
    kpart[...] = res[:, :256]
    vkeep[...] = res[:, pl.ds(pl.multiple_of(HEAD + c * HALF, HALF), HALF)]
    send[:, :256] = res[:, :256].astype(bf16)
    send[:, 256:] = res[:, pl.ds(pl.multiple_of(HEAD + (1 - c) * HALF, HALF), HALF)].astype(bf16)


def project_kv(at, lhs, ws):
    return pl.pallas_call(
        kv_body, in_specs=[SM] + [VM] * 5, out_specs=[VM] * 3,
        out_shape=[jax.ShapeDtypeStruct((SPAN, HEAD), f32), jax.ShapeDtypeStruct((SPAN, HALF), f32),
                   jax.ShapeDtypeStruct((SPAN, 384), bf16)],
        scratch_shapes=[pltpu.VMEM((2048, 512), bf16), pltpu.VMEM((SPAN, 512), f32)], name="project_kv",
    )(at, lhs, *ws)


def pq_body(at, lhs, w0, w1, w2, w3, own, send, rhs):
    place_in(at[1], (w0, w1, w2, w3), rhs)
    r = jnp.dot(lhs[...], rhs[...], preferred_element_type=f32)
    own[...] = r
    send[...] = r.astype(bf16)


def project_pq(at, lhs, ws):
    return pl.pallas_call(
        pq_body, in_specs=[SM] + [VM] * 5, out_specs=[VM] * 2,
        out_shape=[jax.ShapeDtypeStruct((SPAN, 512), f32), jax.ShapeDtypeStruct((SPAN, 512), bf16)],
        scratch_shapes=[pltpu.VMEM((2048, 512), bf16)], name="project_pq",
    )(at, lhs, *ws)


def turn(v, cosine, sine):
    a, b = v[:, :HALF], v[:, HALF:]
    return jnp.concatenate([a * cosine - b * sine, a * sine + b * cosine], axis=1)


def state_body(at, rates, kpart, vkeep, got, cosine, sine, keep, other, rk, val, state, sent, start):
    z, c = at[0], at[3]
    for zs in range(NZ):
        start[pl.ds(pl.multiple_of(zs * 32 + c * 16, 16), 16), :] = keep[zs * 16:zs * 16 + 16, :]
        start[pl.ds(pl.multiple_of(zs * 32 + (1 - c) * 16, 16), 16), :] = other[zs * 16:zs * 16 + 16, :]
    key = (kpart[...] + got[:, :256].astype(f32)).astype(bf16).astype(f32)
    value = (vkeep[...] + got[:, 256:].astype(f32)).astype(bf16)
    val[...] = value
    turned = turn(key, cosine[...], sine[...]) * HEAD ** -0.5
    rk[...] = turned.astype(bf16)
    within = lax.broadcasted_iota(jnp.int32, (SPAN, HEAD), 0).astype(f32)
    faded = (turned * jnp.exp(-(SPAN - 1.0 - within) * rates[0])).astype(bf16)
    s = lax.dot_general(faded, value, (((0,), (0,)), ((), ())), preferred_element_type=f32)
    s = s + jnp.where(z == 0, rates[1], 0.0) * start[...]
    state[...] = s
    sent[...] = s.astype(bf16)


def span_state(at, rates, *args):
    return pl.pallas_call(
        state_body, in_specs=[SM, SM] + [VM] * 7, out_specs=[VM] * 5,
        out_shape=[jax.ShapeDtypeStruct((SPAN, HEAD), bf16), jax.ShapeDtypeStruct((SPAN, HALF), bf16),
                   jax.ShapeDtypeStruct((HEAD, HALF), f32), jax.ShapeDtypeStruct((HEAD, HALF), bf16),
                   jax.ShapeDtypeStruct((HEAD, HALF), f32)],
        name="span_state",
    )(at, rates, *args)


def inside_body(rates, own, got, cosine, sine, rk, val, pool_in, inside, faded):
    pool_in[...] = (own[:, :256] + got[:, :256].astype(f32)).astype(bf16)
    query = (own[:, 256:] + got[:, 256:].astype(f32)).astype(bf16).astype(f32)
    rq = turn(query, cosine[...], sine[...])
    within = lax.broadcasted_iota(jnp.int32, (SPAN, HEAD), 0).astype(f32)
    faded[...] = (rq * jnp.exp(-(within + 1.0) * rates[0])).astype(bf16)
    rq = rq.astype(bf16)
    for b in range(4):
        n = (b + 1) * 128
        scores = lax.dot_general(rq[b * 128:n], rk[:n, :], (((1,), (1,)), ((), ())), preferred_element_type=f32)
        far = lax.broadcasted_iota(jnp.int32, (128, n), 0) + b * 128 - lax.broadcasted_iota(jnp.int32, (128, n), 1)
        fade = jnp.exp(-jnp.maximum(far, 0).astype(f32) * rates[0])
        weights = jnp.where(far >= 0, scores * fade, 0.0).astype(bf16)
        inside[b * 128:n, :] = jnp.dot(weights, val[:n, :], preferred_element_type=f32)


def inside_span(rates, *args):
    return pl.pallas_call(
        inside_body, in_specs=[SM] + [VM] * 6, out_specs=[VM] * 3,
        out_shape=[jax.ShapeDtypeStruct((SPAN, HEAD), bf16), jax.ShapeDtypeStruct((SPAN, HALF), f32),
                   jax.ShapeDtypeStruct((SPAN, HEAD), bf16)],
        name="inside",
    )(rates, *args)


def across_body(at, rates, inside, faded, near, far, start, ret):
    d = rates[1]
    carried = near[...] + d * d * d * far[...].astype(f32) + jnp.where(at[0] == 0, 1.0, 0.0) * start[...]
    ret[...] = inside[...] + jnp.dot(faded[...], carried.astype(bf16), preferred_element_type=f32)


def across_spans(at, rates, *args):
    return pl.pallas_call(
        across_body, in_specs=[SM, SM] + [VM] * 5, out_specs=VM,
        out_shape=jax.ShapeDtypeStruct((SPAN, HALF), f32), name="across",
    )(at, rates, *args)


def pool_body(at, pool_in, before, group_map, scale, out):
    z, y = at[0], at[1]
    ext = jnp.concatenate([before[...], pool_in[...]], axis=0).astype(f32)
    sums = ext
    chosen = None
    for g in range(4):
        sums = sums + pltpu.roll(sums, 2 ** g, 0)
        chosen = sums if chosen is None else jnp.where(y == g, sums, chosen)
    rows = lax.broadcasted_iota(jnp.int32, (SPAN, HEAD), 0) + z * SPAN + 1
    counts = jnp.minimum(lax.shift_left(jnp.int32(2), y), rows).astype(f32)
    differ = (chosen[HALO:] / counts - ext[HALO:]).astype(bf16)
    out[...] = (jnp.dot(differ, group_map[...], preferred_element_type=f32) * scale[...]).astype(bf16)


def pooling(at, *args):
    return pl.pallas_call(
        pool_body, in_specs=[SM] + [VM] * 4, out_specs=VM,
        out_shape=jax.ShapeDtypeStruct((SPAN, HEAD), bf16), name="pooling",
    )(at, *args)


def arrange_body(at, *refs):
    z, y, x = at[0], at[1], at[2]
    ws, out = refs[:9], refs[9]

    def place(ref, first, kz, kx):
        for k in range(2):
            row = ((z + kz) % NZ) * 256 + ((y + k) % 2) * 128 + ((x + NX - kx) % NX) * 32
            out[pl.ds(pl.multiple_of(row, 32), 32), :] = ref[first + k * 32:first + k * 32 + 32, :]

    for i, kz in enumerate((0, 1, 2, 3, 5, 6, 7)):
        for kx in range(NX):
            place(ws[i], kx * 64, kz, kx)
    for kx in range(NX):
        place(ws[7 + kx // 2], (kx % 2) * 64, 4, kx)


def arrange(at, ws):
    return pl.pallas_call(
        arrange_body, in_specs=[SM] + [VM] * 9, out_specs=VM,
        out_shape=jax.ShapeDtypeStruct((2048, SPAN), bf16), name="arrange",
    )(at, *ws)


def back_body(at, pool, ret, other, wt, o0, o1, o2, o3, act, res):
    y, c = at[1], at[3]
    r, o = ret[...], other[...]
    square = jnp.sum(r * r, axis=-1, keepdims=True) + jnp.sum(o * o, axis=-1, keepdims=True)
    factor = lax.rsqrt(square * (1.0 / HEAD) + eps)
    act[:, :256] = pool[...]
    act[:, pl.ds(pl.multiple_of(HEAD + c * HALF, HALF), HALF)] = (r * factor).astype(bf16)
    act[:, pl.ds(pl.multiple_of(HEAD + (1 - c) * HALF, HALF), HALF)] = (o * factor).astype(bf16)
    res[...] = lax.dot_general(act[...], wt[...], (((1,), (1,)), ((), ())), preferred_element_type=f32).astype(bf16)
    for k, out in enumerate((o0, o1, o2, o3)):
        out[...] = res[pl.ds(pl.multiple_of(((y + k) % NY) * HALF, HALF), HALF), :]


def back(at, *args):
    return pl.pallas_call(
        back_body, in_specs=[SM] + [VM] * 4, out_specs=[VM] * 4,
        out_shape=[jax.ShapeDtypeStruct((HALF, 2048), bf16)] * 4,
        scratch_shapes=[pltpu.VMEM((SPAN, 512), bf16), pltpu.VMEM((SPAN, 2048), bf16)], name="back",
    )(at, *args)


def layer(tokens, norm_gain, pool_proj, query_proj, key_proj, value_proj, pool_map, pool_scale,
          decay_rate, start_state, pool_back, retention_back):
    z, y, x, c = (lax.axis_index(a) for a in ("z", "y", "x", "c"))
    at = jnp.stack([z, y, x, c]).astype(jnp.int32)

    s0, s1 = pack(at, pool_proj, query_proj, key_proj, value_proj, start_state[0], pool_back, retention_back)
    r0 = lax.ppermute(s0, ("y", "c"), to_heads(0))
    r1 = lax.ppermute(s1, ("y", "c"), to_heads(1))
    shard_in = jnp.concatenate([r0[:32], r1[:32], r0[32:64], r1[32:64], r0[96:104], r1[96:104]], axis=0)
    shard_out = jnp.concatenate([r0[64:96], r1[64:96]], axis=0)

    toks = direct(norm(at, tokens[0], norm_gain[None]), "y", NY)

    lhs = gather_rows(at, toks)

    in_z = z_ring(shard_in, False)
    plane_kv, plane_pq, keep, give = split(at, in_z)
    kv_list = direct(plane_kv, "x", NX)
    pq_list = direct(plane_pq, "x", NX)
    start_other = swap(give)

    plane_o = jnp.concatenate(direct(shard_out, "x", NX), axis=0)
    wt = arrange(at, z_ring(plane_o, True))

    decays = jnp.where(c == y // 2, decay_rate, swap(decay_rate))
    rate = jnp.where(y % 2 == 0, decays[0], decays[1])
    span_decay = jnp.exp(-SPAN * rate)
    rates = jnp.stack([rate, span_decay])
    scale = lax.dynamic_slice_in_dim(pool_scale, y * HEAD, HEAD, 0)[None]
    group_map = lax.dynamic_index_in_dim(pool_map, y, 0, keepdims=False)
    positions = (jnp.arange(SPAN, dtype=jnp.int32) + z * SPAN)
    inv_freq = 1.0 / rope_base ** jnp.linspace(0.0, 1.0, HALF, dtype=f32)
    angles = positions.astype(f32)[:, None] * inv_freq[None, :]
    cosine, sine = jnp.cos(angles), jnp.sin(angles)

    kpart, vkeep, send = project_kv(at, lhs, kv_list)
    got = swap(send)
    rk, val, state, sent, start = span_state(at, rates, kpart, vkeep, got, cosine, sine, keep, start_other)
    n1, n2, n3 = (lax.ppermute(sent, "z", line(NZ, k)).astype(f32) for k in (1, 2, 3))
    near = n1 + span_decay * (n2 + span_decay * n3)
    far = lax.ppermute((state + span_decay * near).astype(bf16), "z", line(NZ, 4))

    own, send = project_pq(at, lhs, pq_list)
    got = swap(send)
    pool_in, inside, faded = inside_span(rates, own, got, cosine, sine, rk, val)
    before = lax.ppermute(pool_in[SPAN - HALO:], "z", line(NZ, 1))
    pool_out = pooling(at, pool_in, before, group_map, scale)
    ret = across_spans(at, rates, inside, faded, near, far, start)
    other = swap(ret)

    shares = back(at, pool_out, ret, other, wt)
    total = shares[0].astype(f32)
    for k in range(1, NY):
        total = total + lax.ppermute(shares[k], "y", ring(NY, k)).astype(f32)
    total = total.astype(bf16).reshape(2, 64, 2048)
    keep = lax.dynamic_index_in_dim(total, c, 0, keepdims=False).reshape(64, NZ, 256)
    got = swap(lax.dynamic_index_in_dim(total, 1 - c, 0, keepdims=False)).reshape(64, NZ, 256)
    mixed = jnp.where(c == 0, jnp.stack([keep, got], 2), jnp.stack([got, keep], 2))
    return mixed.reshape(1, 64, 4096)


def solution(mesh):
    torus = Mesh(mesh.devices.reshape(NZ, NY, NX, 2), ("z", "y", "x", "c"))
    sp, sp_fs = ("z", "y"), ("z", "y", "x")
    placed = (
        P("x", sp, None), P(), P(sp_fs, "c"), P(sp_fs, "c"), P(sp_fs, "c"), P(sp_fs, "c"), P(), P(),
        P("c"), P("x", "c", sp, None), P("c", sp_fs), P("c", sp_fs),
    )
    return jax.shard_map(layer, mesh=torus, in_specs=placed, out_specs=P("x", ("z", "y", "c"), None), check_vma=False)
```

profile of v0, /device:TPU:1, one launch (start us, length us, event | category | flops | bytes accessed | tf_op | source)
XLA Modules:
  0.0 200.3 jit_solution(12143706854183583380)
XLA Ops:
  5.6 6.2 %collective-permute-start.4 = (bf16[112,512]{1,0:T(8,128)(2,1)}, bf16[112,512]{1,0:T(8,128)(2,1)S(1)}, u32[]{:S(2)}, u32[]{:S(2)}) collective-permute-start(bf16[112,512]{1,0:T(8,128)(2,1)} %get-tuple-element.28), channel_id=1, source_target_pairs={{0,0},{1,16},{8,8},{9,24},{16,1},{17,17},{24,9},{25,25},{2,2},{3,1... | collective-permute-start | bytes 344072 | tf_op jit(solution)/shard_map/ppermute | solution.py:339
  12.4 3.1 %collective-permute-done.4 = bf16[112,512]{1,0:T(8,128)(2,1)S(1)} collective-permute-done((bf16[112,512]{1,0:T(8,128)(2,1)}, bf16[112,512]{1,0:T(8,128)(2,1)S(1)}, u32[]{:S(2)}, u32[]{:S(2)}) %collective-permute-start.4) | collective-permute-done | bytes 114720 | tf_op jit(solution)/shard_map/ppermute | solution.py:339
  19.3 2.8 %norm.1.t0 = bf16[8,128,256]{2,1,0:T(8,128)(2,1)} custom-call(s32[4]{0:T(128)} %pad_add_fusion.at, bf16[128,4096]{1,0:T(8,128)(2,1)} %bitcast.28, f32[1,4096]{1,0:T(1,128)} %bitcast.32), custom_call_target="tpu_custom_call" | custom-call | tf_op jit(solution)/shard_map/norm/pallas_call | solution.py:110
  22.2 4.0 %collective-permute-start.6 = (bf16[144,512]{1,0:T(8,128)(2,1)S(1)}, bf16[144,512]{1,0:T(8,128)(2,1)S(1)}, u32[]{:S(2)}, u32[]{:S(2)}) collective-permute-start(bf16[144,512]{1,0:T(8,128)(2,1)S(1)} %constant_dynamic-update-slice_fusion.refs_0_), channel_id=1, source_target_pairs={{0,224},{32,0},{64,32},{96,64},{128,96},{160,128},{192,160},{224,1... | collective-permute-start | bytes 442376 | tf_op jit(solution)/shard_map/ppermute | solution.py:50
  28.2 3.4 %collective-permute-start.7 = (bf16[144,512]{1,0:T(8,128)(2,1)S(1)}, bf16[144,512]{1,0:T(8,128)(2,1)S(1)}, u32[]{:S(2)}, u32[]{:S(2)}) collective-permute-start(bf16[144,512]{1,0:T(8,128)(2,1)S(1)} %collective-permute-done.6.refs_1_), channel_id=1, source_target_pairs={{0,224},{32,0},{64,32},{96,64},{128,96},{160,128},{192,160},{224,1... | collective-permute-start | bytes 442376 | tf_op jit(solution)/shard_map/ppermute | solution.py:50
  31.6 2.7 %collective-permute-done.7.refs_2_ = bf16[144,512]{1,0:T(8,128)(2,1)S(1)} collective-permute-done((bf16[144,512]{1,0:T(8,128)(2,1)S(1)}, bf16[144,512]{1,0:T(8,128)(2,1)S(1)}, u32[]{:S(2)}, u32[]{:S(2)}) %collective-permute-start.7) | collective-permute-done | bytes 147488 | tf_op jit(solution)/shard_map/ppermute | solution.py:50
  34.3 3.4 %collective-permute-start.8 = (bf16[144,512]{1,0:T(8,128)(2,1)S(1)}, bf16[144,512]{1,0:T(8,128)(2,1)S(1)}, u32[]{:S(2)}, u32[]{:S(2)}) collective-permute-start(bf16[144,512]{1,0:T(8,128)(2,1)S(1)} %collective-permute-done.7.refs_2_), channel_id=1, source_target_pairs={{0,224},{32,0},{64,32},{96,64},{128,96},{160,128},{192,160},{224,1... | collective-permute-start | bytes 442376 | tf_op jit(solution)/shard_map/ppermute | solution.py:50
  39.0 2.5 %collective-permute-start.29 = (bf16[64,512]{1,0:T(8,128)(2,1)S(1)}, bf16[64,512]{1,0:T(8,128)(2,1)S(1)}, u32[]{:S(2)}, u32[]{:S(2)}) collective-permute-start(bf16[64,512]{1,0:T(8,128)(2,1)S(1)} %pad_maximum_fusion), channel_id=1, source_target_pairs={{0,4},{2,6},{4,0},{6,2},{1,5},{3,7},{5,1},{7,3},{8,12},{10,14},{12... | collective-permute-start | bytes 196616 | tf_op jit(solution)/shard_map/ppermute | solution.py:41
  45.2 2.5 %split.1 = (bf16[512,512]{1,0:T(8,128)(2,1)}, bf16[512,512]{1,0:T(8,128)(2,1)}, f32[128,128]{1,0:T(8,128)}, f32[128,128]{1,0:T(8,128)}) custom-call(s32[4]{0:T(128)} %pad_add_fusion.at, bf16[144,512]{1,0:T(8,128)(2,1)} %copy-done.14, bf16[144,512]{1,0:T(8,128)(2,1)} %copy-done.16, bf16[144,512]{1,0:T(8,128)(2,1)} %copy-done.18, bf16[144,512]{1,0:T(8,128)(2,1)} %copy-done.20, ...), custom_call_target="tpu_custom_call" | custom-call | tf_op jit(solution)/shard_map/split/pallas_call | solution.py:133
  47.7 5.2 %collective-permute-start.2 = (bf16[8,128,256]{2,1,0:T(8,128)(2,1)}, bf16[8,128,256]{2,1,0:T(8,128)(2,1)S(1)}, u32[]{:S(2)}, u32[]{:S(2)}) collective-permute-start(bf16[8,128,256]{2,1,0:T(8,128)(2,1)} %norm.1.t0), channel_id=1, source_target_pairs={{0,16},{8,24},{16,0},{24,8},{1,17},{9,25},{17,1},{25,9},{2,18},{10... | collective-permute-start | bytes 1572872 | tf_op jit(solution)/shard_map/ppermute | solution.py:41
  54.4 2.5 %collective-permute-start.18 = (bf16[512,512]{1,0:T(8,128)(2,1)}, bf16[512,512]{1,0:T(8,128)(2,1)S(1)}, u32[]{:S(2)}, u32[]{:S(2)}) collective-permute-start(bf16[512,512]{1,0:T(8,128)(2,1)} %get-tuple-element.33.w0), channel_id=1, source_target_pairs={{0,4},{2,6},{4,0},{6,2},{1,5},{3,7},{5,1},{7,3},{8,12},{10,14},{12... | collective-permute-start | bytes 1572872 | tf_op jit(solution)/shard_map/ppermute | solution.py:41
  58.9 5.9 %collective-permute-done.2.t2 = bf16[8,128,256]{2,1,0:T(8,128)(2,1)S(1)} collective-permute-done((bf16[8,128,256]{2,1,0:T(8,128)(2,1)}, bf16[8,128,256]{2,1,0:T(8,128)(2,1)S(1)}, u32[]{:S(2)}, u32[]{:S(2)}) %collective-permute-start.2) | collective-permute-done | bytes 524320 | tf_op jit(solution)/shard_map/ppermute | solution.py:41
  64.8 2.6 %collective-permute-start.31 = (bf16[256,512]{1,0:T(8,128)(2,1)S(1)}, bf16[256,512]{1,0:T(8,128)(2,1)}, u32[]{:S(2)}, u32[]{:S(2)}) collective-permute-start(bf16[256,512]{1,0:T(8,128)(2,1)S(1)} %constant_dynamic-update-slice_fusion.2.refs_0_), channel_id=1, source_target_pairs={{0,224},{32,0},{64,32},{96,64},{128,96},{160,128},{192,160},{224,1... | collective-permute-start | bytes 786440 | tf_op jit(solution)/shard_map/ppermute | solution.py:50
  67.4 7.9 %collective-permute-done.3.t3 = bf16[8,128,256]{2,1,0:T(8,128)(2,1)S(1)} collective-permute-done((bf16[8,128,256]{2,1,0:T(8,128)(2,1)}, bf16[8,128,256]{2,1,0:T(8,128)(2,1)S(1)}, u32[]{:S(2)}, u32[]{:S(2)}) %collective-permute-start.3) | collective-permute-done | bytes 524320 | tf_op jit(solution)/shard_map/ppermute | solution.py:41
  76.6 2.8 %collective-permute-done.18.w2 = bf16[512,512]{1,0:T(8,128)(2,1)S(1)} collective-permute-done((bf16[512,512]{1,0:T(8,128)(2,1)}, bf16[512,512]{1,0:T(8,128)(2,1)S(1)}, u32[]{:S(2)}, u32[]{:S(2)}) %collective-permute-start.18) | collective-permute-done | bytes 524320 | tf_op jit(solution)/shard_map/ppermute | solution.py:41
  79.9 3.0 %collective-permute-start.15 = (bf16[512,512]{1,0:T(8,128)(2,1)}, bf16[512,512]{1,0:T(8,128)(2,1)}, u32[]{:S(2)}, u32[]{:S(2)}) collective-permute-start(bf16[512,512]{1,0:T(8,128)(2,1)} %get-tuple-element.30.w0), channel_id=1, source_target_pairs={{0,6},{2,0},{4,2},{6,4},{1,7},{3,1},{5,3},{7,5},{8,14},{10,8},{12,... | collective-permute-start | bytes 1572872 | tf_op jit(solution)/shard_map/ppermute | solution.py:41
  84.8 3.1 %rows.1.lhs = bf16[512,2048]{1,0:T(8,128)(2,1)} custom-call(s32[4]{0:T(128)} %pad_add_fusion.at, bf16[8,128,256]{2,1,0:T(8,128)(2,1)} %norm.1.t0, bf16[8,128,256]{2,1,0:T(8,128)(2,1)} %copy-done.3, bf16[8,128,256]{2,1,0:T(8,128)(2,1)} %copy-done.4, bf16[8,128,256]{2,1,0:T(8,128)(2,1)} %copy-done.5), custom_call_target="tpu_custom_call" | custom-call | tf_op jit(solution)/shard_map/rows/pallas_call | solution.py:149
  87.9 4.6 %project_kv.1 = (f32[512,256]{1,0:T(8,128)}, f32[512,128]{1,0:T(8,128)}, bf16[512,384]{1,0:T(8,128)(2,1)}) custom-call(s32[4]{0:T(128)} %pad_add_fusion.at, bf16[512,2048]{1,0:T(8,128)(2,1)} %rows.1.lhs, bf16[512,512]{1,0:T(8,128)(2,1)} %get-tuple-element.33.w0, bf16[512,512]{1,0:T(8,128)(2,1)} %copy-done.6, bf16[512,512]{1,0:T(8,128)(2,1)} %copy-done.7, ...), custom_call_target="tpu_custom_call" | custom-call | tf_op jit(solution)/shard_map/project_kv/pallas_call | solution.py:174
  96.1 5.7 %collective-permute-done.14.w2 = bf16[512,512]{1,0:T(8,128)(2,1)} collective-permute-done((bf16[512,512]{1,0:T(8,128)(2,1)}, bf16[512,512]{1,0:T(8,128)(2,1)}, u32[]{:S(2)}, u32[]{:S(2)}) %collective-permute-start.14) | collective-permute-done | bytes 524320 | tf_op jit(solution)/shard_map/ppermute | solution.py:41
  101.9 4.6 %project_pq.1 = (f32[512,512]{1,0:T(8,128)}, bf16[512,512]{1,0:T(8,128)(2,1)}) custom-call(s32[4]{0:T(128)} %pad_add_fusion.at, bf16[512,2048]{1,0:T(8,128)(2,1)} %rows.1.lhs, bf16[512,512]{1,0:T(8,128)(2,1)} %get-tuple-element.30.w0, bf16[512,512]{1,0:T(8,128)(2,1)} %collective-permute-done.13.w1, bf16[512,512]{1,0:T(8,128)(2,1)} %collective-permute-done.14.w2, ...), custom_call_target="tpu_custom_call" | custom-call | tf_op jit(solution)/shard_map/project_pq/pallas_call | solution.py:190
  106.4 3.2 %collective-permute-start.16 = (bf16[512,512]{1,0:T(8,128)(2,1)}, bf16[512,512]{1,0:T(8,128)(2,1)S(1)}, u32[]{:S(2)}, u32[]{:S(2)}) collective-permute-start(bf16[512,512]{1,0:T(8,128)(2,1)} %get-tuple-element.32), channel_id=1, source_target_pairs={{0,1},{1,0},{2,3},{3,2},{4,5},{5,4},{6,7},{7,6},{8,9},{9,8},{10,11... | collective-permute-start | bytes 1572872 | tf_op jit(solution)/shard_map/ppermute | solution.py:37
  113.7 2.6 %span_state.1 = (bf16[512,256]{1,0:T(8,128)(2,1)}, bf16[512,128]{1,0:T(8,128)(2,1)}, f32[256,128]{1,0:T(8,128)}, bf16[256,128]{1,0:T(8,128)(2,1)}, f32[256,128]{1,0:T(8,128)}) custom-call(s32[4]{0:T(128)} %pad_add_fusion.at, f32[2]{0:T(128)} %pad_maximum_fusion.1.rates, f32[512,256]{1,0:T(8,128)} %get-tuple-element.34.kpart, ...), custom_call_target="tpu_custom_call" | custom-call | tf_op jit(solution)/shard_map/span_state/pallas_call | solution.py:221
  116.3 5.1 %collective-permute-start.25 = (bf16[256,128]{1,0:T(8,128)(2,1)}, bf16[256,128]{1,0:T(8,128)(2,1)S(1)}, u32[]{:S(2)}, u32[]{:S(2)}) collective-permute-start(bf16[256,128]{1,0:T(8,128)(2,1)} %get-tuple-element.44), channel_id=1, source_target_pairs={{0,96},{32,128},{64,160},{96,192},{128,224},{1,97},{33,129},{65,16... | collective-permute-start | bytes 196616 | tf_op jit(solution)/shard_map/ppermute | solution.py:371
  121.4 2.7 %collective-permute-start.24 = (bf16[256,128]{1,0:T(8,128)(2,1)}, bf16[256,128]{1,0:T(8,128)(2,1)S(1)}, u32[]{:S(2)}, u32[]{:S(2)}) collective-permute-start(bf16[256,128]{1,0:T(8,128)(2,1)} %get-tuple-element.44), channel_id=1, source_target_pairs={{0,64},{32,96},{64,128},{96,160},{128,192},{160,224},{1,65},{33,97... | collective-permute-start | bytes 196616 | tf_op jit(solution)/shard_map/ppermute | solution.py:371
  129.9 7.6 %collective-permute-start.26 = (bf16[256,128]{1,0:T(8,128)(2,1)S(1)}, bf16[256,128]{1,0:T(8,128)(2,1)S(1)}, u32[]{:S(2)}, u32[]{:S(2)}) collective-permute-start(bf16[256,128]{1,0:T(8,128)(2,1)S(1)} %get-tuple-element.51), channel_id=1, source_target_pairs={{0,128},{32,160},{64,192},{96,224},{1,129},{33,161},{65,193},{97,2... | collective-permute-start | bytes 196616 | tf_op jit(solution)/shard_map/ppermute | solution.py:373
  138.3 3.4 %inside.1 = (bf16[512,256]{1,0:T(8,128)(2,1)}, f32[512,128]{1,0:T(8,128)}, bf16[512,256]{1,0:T(8,128)(2,1)}) custom-call(f32[2]{0:T(128)} %pad_maximum_fusion.1.rates, f32[512,512]{1,0:T(8,128)} %get-tuple-element.31.own, bf16[512,512]{1,0:T(8,128)(2,1)} %copy-done.8, f32[512,128]{1,0:T(8,128)} %get-tuple-element.62.cosine, ...), custom_call_target="tpu_custom_call" | custom-call | tf_op jit(solution)/shard_map/inside/pallas_call | solution.py:247
  146.4 2.7 %collective-permute-start.38 = (bf16[128,512]{1,0:T(8,128)(2,1)S(1)}, bf16[128,512]{1,0:T(8,128)(2,1)S(1)}, u32[]{:S(2)}, u32[]{:S(2)}) collective-permute-start(bf16[128,512]{1,0:T(8,128)(2,1)S(1)} %slice.61), channel_id=1, source_target_pairs={{0,224},{32,0},{64,32},{96,64},{128,96},{160,128},{192,160},{224,1... | collective-permute-start | bytes 393224 | tf_op jit(solution)/shard_map/ppermute | solution.py:56
  154.4 3.0 %arrange.1.wt = bf16[2048,512]{1,0:T(8,128)(2,1)} custom-call(s32[4]{0:T(128)} %pad_add_fusion.at, bf16[256,512]{1,0:T(8,128)(2,1)} %copy-done.10, bf16[256,512]{1,0:T(8,128)(2,1)} %collective-permute-done.31.refs_1_, bf16[256,512]{1,0:T(8,128)(2,1)} %copy-done.11, bf16[256,512]{1,0:T(8,128)(2,1)} %copy-done.1, bf16[256,512]{1,0:T(8,128)(2,1)} %copy-done.2, ...), custom_call_target="tpu_custom_call" | custom-call | tf_op jit(solution)/shard_map/arrange/pallas_call | solution.py:306
  161.0 4.7 %back.1 = (bf16[128,2048]{1,0:T(8,128)(2,1)}, bf16[128,2048]{1,0:T(8,128)(2,1)}, bf16[128,2048]{1,0:T(8,128)(2,1)}, bf16[128,2048]{1,0:T(8,128)(2,1)}) custom-call(s32[4]{0:T(128)} %pad_add_fusion.at, bf16[512,256]{1,0:T(8,128)(2,1)} %pooling.1.pool, f32[512,128]{1,0:T(8,128)} %across.1.ret, f32[512,128]{1,0:T(8,128)} %copy-done.13, bf16[2048,512]{1,0:T(8,128)(2,1)} %arrange.1.wt), custom_call_target="tpu_custom_call" | custom-call | tf_op jit(solution)/shard_map/back/pallas_call | solution.py:326
  165.6 3.1 %collective-permute-start.41 = (bf16[128,2048]{1,0:T(8,128)(2,1)}, bf16[128,2048]{1,0:T(8,128)(2,1)S(1)}, u32[]{:S(2)}, u32[]{:S(2)}) collective-permute-start(bf16[128,2048]{1,0:T(8,128)(2,1)} %get-tuple-element.50), channel_id=1, source_target_pairs={{0,24},{8,0},{16,8},{24,16},{1,25},{9,1},{17,9},{25,17},{2,26},{10... | collective-permute-start | bytes 1572872 | tf_op jit(solution)/shard_map/ppermute | solution.py:386
  169.3 21.5 %collective-permute-done.41 = bf16[128,2048]{1,0:T(8,128)(2,1)S(1)} collective-permute-done((bf16[128,2048]{1,0:T(8,128)(2,1)}, bf16[128,2048]{1,0:T(8,128)(2,1)S(1)}, u32[]{:S(2)}, u32[]{:S(2)}) %collective-permute-start.41) | collective-permute-done | bytes 524320 | tf_op jit(solution)/shard_map/ppermute | solution.py:386
  190.9 4.1 %collective-permute-done.39 = bf16[128,2048]{1,0:T(8,128)(2,1)S(1)} collective-permute-done((bf16[128,2048]{1,0:T(8,128)(2,1)}, bf16[128,2048]{1,0:T(8,128)(2,1)S(1)}, u32[]{:S(2)}, u32[]{:S(2)}) %collective-permute-start.39) | collective-permute-done | bytes 524320 | tf_op jit(solution)/shard_map/ppermute | solution.py:386
  (157 shorter events, 56.3 us)
Async XLA Ops:
  5.6 9.9 %collective-permute-start.4 = (bf16[112,512]{1,0:T(8,128)(2,1)}, bf16[112,512]{1,0:T(8,128)(2,1)S(1)}, u32[]{:S(2)}, u32[]{:S(2)}) collective-permute-start(bf16[112,512]{1,0:T(8,128)(2,1)} %get-tuple-element.28), channel_id=1, source_target_pairs={{0,0},{1,16},{8,8},{9,24},{16,1},{17,17},{24,9},{25,25},{2,2},{3,1... | collective-permute-start | bytes 344072 | tf_op jit(solution)/shard_map/ppermute | solution.py:339
  17.6 8.5 %collective-permute-start.9 = (bf16[144,512]{1,0:T(8,128)(2,1)S(1)}, bf16[144,512]{1,0:T(8,128)(2,1)S(1)}, u32[]{:S(2)}, u32[]{:S(2)}) collective-permute-start(bf16[144,512]{1,0:T(8,128)(2,1)S(1)} %constant_dynamic-update-slice_fusion.refs_0_), channel_id=1, source_target_pairs={{0,32},{32,64},{64,96},{96,128},{128,160},{160,192},{192,224},{224... | collective-permute-start | bytes 442376 | tf_op jit(solution)/shard_map/ppermute | solution.py:49
  22.2 34.7 %collective-permute-start.1 = (bf16[8,128,256]{2,1,0:T(8,128)(2,1)}, bf16[8,128,256]{2,1,0:T(8,128)(2,1)S(1)}, u32[]{:S(2)}, u32[]{:S(2)}) collective-permute-start(bf16[8,128,256]{2,1,0:T(8,128)(2,1)} %norm.1.t0), channel_id=1, source_target_pairs={{0,8},{8,16},{16,24},{24,0},{1,9},{9,17},{17,25},{25,1},{2,10},{10... | collective-permute-start | bytes 1572872 | tf_op jit(solution)/shard_map/ppermute | solution.py:41
  34.3 7.2 %collective-permute-start.8 = (bf16[144,512]{1,0:T(8,128)(2,1)S(1)}, bf16[144,512]{1,0:T(8,128)(2,1)S(1)}, u32[]{:S(2)}, u32[]{:S(2)}) collective-permute-start(bf16[144,512]{1,0:T(8,128)(2,1)S(1)} %collective-permute-done.7.refs_2_), channel_id=1, source_target_pairs={{0,224},{32,0},{64,32},{96,64},{128,96},{160,128},{192,160},{224,1... | collective-permute-start | bytes 442376 | tf_op jit(solution)/shard_map/ppermute | solution.py:50
  37.7 15.2 %collective-permute-start.28 = (bf16[64,512]{1,0:T(8,128)(2,1)S(1)}, bf16[64,512]{1,0:T(8,128)(2,1)S(1)}, u32[]{:S(2)}, u32[]{:S(2)}) collective-permute-start(bf16[64,512]{1,0:T(8,128)(2,1)S(1)} %pad_maximum_fusion), channel_id=1, source_target_pairs={{0,2},{2,4},{4,6},{6,0},{1,3},{3,5},{5,7},{7,1},{8,10},{10,12},{12... | collective-permute-start | bytes 196616 | tf_op jit(solution)/shard_map/ppermute | solution.py:41
  39.0 13.9 %collective-permute-start.29 = (bf16[64,512]{1,0:T(8,128)(2,1)S(1)}, bf16[64,512]{1,0:T(8,128)(2,1)S(1)}, u32[]{:S(2)}, u32[]{:S(2)}) collective-permute-start(bf16[64,512]{1,0:T(8,128)(2,1)S(1)} %pad_maximum_fusion), channel_id=1, source_target_pairs={{0,4},{2,6},{4,0},{6,2},{1,5},{3,7},{5,1},{7,3},{8,12},{10,14},{12... | collective-permute-start | bytes 196616 | tf_op jit(solution)/shard_map/ppermute | solution.py:41
  41.5 12.9 %collective-permute-start.30 = (bf16[64,512]{1,0:T(8,128)(2,1)S(1)}, bf16[64,512]{1,0:T(8,128)(2,1)}, u32[]{:S(2)}, u32[]{:S(2)}) collective-permute-start(bf16[64,512]{1,0:T(8,128)(2,1)S(1)} %pad_maximum_fusion), channel_id=1, source_target_pairs={{0,6},{2,0},{4,2},{6,4},{1,7},{3,1},{5,3},{7,5},{8,14},{10,8},{12,... | collective-permute-start | bytes 196616 | tf_op jit(solution)/shard_map/ppermute | solution.py:41
  47.7 17.1 %collective-permute-start.2 = (bf16[8,128,256]{2,1,0:T(8,128)(2,1)}, bf16[8,128,256]{2,1,0:T(8,128)(2,1)S(1)}, u32[]{:S(2)}, u32[]{:S(2)}) collective-permute-start(bf16[8,128,256]{2,1,0:T(8,128)(2,1)} %norm.1.t0), channel_id=1, source_target_pairs={{0,16},{8,24},{16,0},{24,8},{1,17},{9,25},{17,1},{25,9},{2,18},{10... | collective-permute-start | bytes 1572872 | tf_op jit(solution)/shard_map/ppermute | solution.py:41
  52.9 22.4 %collective-permute-start.3 = (bf16[8,128,256]{2,1,0:T(8,128)(2,1)}, bf16[8,128,256]{2,1,0:T(8,128)(2,1)S(1)}, u32[]{:S(2)}, u32[]{:S(2)}) collective-permute-start(bf16[8,128,256]{2,1,0:T(8,128)(2,1)} %norm.1.t0), channel_id=1, source_target_pairs={{0,24},{8,0},{16,8},{24,16},{1,25},{9,1},{17,9},{25,17},{2,26},{10... | collective-permute-start | bytes 1572872 | tf_op jit(solution)/shard_map/ppermute | solution.py:41
  52.9 22.4 %collective-permute-start.17 = (bf16[512,512]{1,0:T(8,128)(2,1)}, bf16[512,512]{1,0:T(8,128)(2,1)S(1)}, u32[]{:S(2)}, u32[]{:S(2)}) collective-permute-start(bf16[512,512]{1,0:T(8,128)(2,1)} %get-tuple-element.33.w0), channel_id=1, source_target_pairs={{0,2},{2,4},{4,6},{6,0},{1,3},{3,5},{5,7},{7,1},{8,10},{10,12},{12... | collective-permute-start | bytes 1572872 | tf_op jit(solution)/shard_map/ppermute | solution.py:41
  54.4 25.0 %collective-permute-start.18 = (bf16[512,512]{1,0:T(8,128)(2,1)}, bf16[512,512]{1,0:T(8,128)(2,1)S(1)}, u32[]{:S(2)}, u32[]{:S(2)}) collective-permute-start(bf16[512,512]{1,0:T(8,128)(2,1)} %get-tuple-element.33.w0), channel_id=1, source_target_pairs={{0,4},{2,6},{4,0},{6,2},{1,5},{3,7},{5,1},{7,3},{8,12},{10,14},{12... | collective-permute-start | bytes 1572872 | tf_op jit(solution)/shard_map/ppermute | solution.py:41
  56.8 23.1 %collective-permute-start.19 = (bf16[512,512]{1,0:T(8,128)(2,1)}, bf16[512,512]{1,0:T(8,128)(2,1)}, u32[]{:S(2)}, u32[]{:S(2)}) collective-permute-start(bf16[512,512]{1,0:T(8,128)(2,1)} %get-tuple-element.33.w0), channel_id=1, source_target_pairs={{0,6},{2,0},{4,2},{6,4},{1,7},{3,1},{5,3},{7,5},{8,14},{10,8},{12,... | collective-permute-start | bytes 1572872 | tf_op jit(solution)/shard_map/ppermute | solution.py:41
  64.8 27.7 %collective-permute-start.31 = (bf16[256,512]{1,0:T(8,128)(2,1)S(1)}, bf16[256,512]{1,0:T(8,128)(2,1)}, u32[]{:S(2)}, u32[]{:S(2)}) collective-permute-start(bf16[256,512]{1,0:T(8,128)(2,1)S(1)} %constant_dynamic-update-slice_fusion.2.refs_0_), channel_id=1, source_target_pairs={{0,224},{32,0},{64,32},{96,64},{128,96},{160,128},{192,160},{224,1... | collective-permute-start | bytes 786440 | tf_op jit(solution)/shard_map/ppermute | solution.py:50
  75.3 19.2 %collective-permute-start.34 = (bf16[256,512]{1,0:T(8,128)(2,1)S(1)}, bf16[256,512]{1,0:T(8,128)(2,1)}, u32[]{:S(2)}, u32[]{:S(2)}) collective-permute-start(bf16[256,512]{1,0:T(8,128)(2,1)S(1)} %constant_dynamic-update-slice_fusion.2.refs_0_), channel_id=1, source_target_pairs={{0,32},{32,64},{64,96},{96,128},{128,160},{160,192},{192,224},{224... | collective-permute-start | bytes 786440 | tf_op jit(solution)/shard_map/ppermute | solution.py:49
  75.3 20.7 %collective-permute-start.13 = (bf16[512,512]{1,0:T(8,128)(2,1)}, bf16[512,512]{1,0:T(8,128)(2,1)}, u32[]{:S(2)}, u32[]{:S(2)}) collective-permute-start(bf16[512,512]{1,0:T(8,128)(2,1)} %get-tuple-element.30.w0), channel_id=1, source_target_pairs={{0,2},{2,4},{4,6},{6,0},{1,3},{3,5},{5,7},{7,1},{8,10},{10,12},{12... | collective-permute-start | bytes 1572872 | tf_op jit(solution)/shard_map/ppermute | solution.py:41
  79.4 22.3 %collective-permute-start.14 = (bf16[512,512]{1,0:T(8,128)(2,1)}, bf16[512,512]{1,0:T(8,128)(2,1)}, u32[]{:S(2)}, u32[]{:S(2)}) collective-permute-start(bf16[512,512]{1,0:T(8,128)(2,1)} %get-tuple-element.30.w0), channel_id=1, source_target_pairs={{0,4},{2,6},{4,0},{6,2},{1,5},{3,7},{5,1},{7,3},{8,12},{10,14},{12... | collective-permute-start | bytes 1572872 | tf_op jit(solution)/shard_map/ppermute | solution.py:41
  79.9 21.9 %collective-permute-start.15 = (bf16[512,512]{1,0:T(8,128)(2,1)}, bf16[512,512]{1,0:T(8,128)(2,1)}, u32[]{:S(2)}, u32[]{:S(2)}) collective-permute-start(bf16[512,512]{1,0:T(8,128)(2,1)} %get-tuple-element.30.w0), channel_id=1, source_target_pairs={{0,6},{2,0},{4,2},{6,4},{1,7},{3,1},{5,3},{7,5},{8,14},{10,8},{12,... | collective-permute-start | bytes 1572872 | tf_op jit(solution)/shard_map/ppermute | solution.py:41
  92.5 31.6 %collective-permute-start.32 = (bf16[256,512]{1,0:T(8,128)(2,1)}, bf16[256,512]{1,0:T(8,128)(2,1)S(1)}, u32[]{:S(2)}, u32[]{:S(2)}) collective-permute-start(bf16[256,512]{1,0:T(8,128)(2,1)} %collective-permute-done.31.refs_1_), channel_id=1, source_target_pairs={{0,224},{32,0},{64,32},{96,64},{128,96},{160,128},{192,160},{224,1... | collective-permute-start | bytes 786440 | tf_op jit(solution)/shard_map/ppermute | solution.py:50
  94.5 18.4 %collective-permute-start.20 = (bf16[512,384]{1,0:T(8,128)(2,1)}, bf16[512,384]{1,0:T(8,128)(2,1)S(1)}, u32[]{:S(2)}, u32[]{:S(2)}) collective-permute-start(bf16[512,384]{1,0:T(8,128)(2,1)} %get-tuple-element.36), channel_id=1, source_target_pairs={{0,1},{1,0},{2,3},{3,2},{4,5},{5,4},{6,7},{7,6},{8,9},{9,8},{10,11... | collective-permute-start | bytes 1179656 | tf_op jit(solution)/shard_map/ppermute | solution.py:37
  96.0 30.5 %collective-permute-start.35 = (bf16[256,512]{1,0:T(8,128)(2,1)}, bf16[256,512]{1,0:T(8,128)(2,1)S(1)}, u32[]{:S(2)}, u32[]{:S(2)}) collective-permute-start(bf16[256,512]{1,0:T(8,128)(2,1)} %collective-permute-done.34.refs_6_), channel_id=1, source_target_pairs={{0,32},{32,64},{64,96},{96,128},{128,160},{160,192},{192,224},{224... | collective-permute-start | bytes 786440 | tf_op jit(solution)/shard_map/ppermute | solution.py:49
  106.4 31.1 %collective-permute-start.16 = (bf16[512,512]{1,0:T(8,128)(2,1)}, bf16[512,512]{1,0:T(8,128)(2,1)S(1)}, u32[]{:S(2)}, u32[]{:S(2)}) collective-permute-start(bf16[512,512]{1,0:T(8,128)(2,1)} %get-tuple-element.32), channel_id=1, source_target_pairs={{0,1},{1,0},{2,3},{3,2},{4,5},{5,4},{6,7},{7,6},{8,9},{9,8},{10,11... | collective-permute-start | bytes 1572872 | tf_op jit(solution)/shard_map/ppermute | solution.py:37
  116.3 10.5 %collective-permute-start.25 = (bf16[256,128]{1,0:T(8,128)(2,1)}, bf16[256,128]{1,0:T(8,128)(2,1)S(1)}, u32[]{:S(2)}, u32[]{:S(2)}) collective-permute-start(bf16[256,128]{1,0:T(8,128)(2,1)} %get-tuple-element.44), channel_id=1, source_target_pairs={{0,96},{32,128},{64,160},{96,192},{128,224},{1,97},{33,129},{65,16... | collective-permute-start | bytes 196616 | tf_op jit(solution)/shard_map/ppermute | solution.py:371
  121.4 6.8 %collective-permute-start.24 = (bf16[256,128]{1,0:T(8,128)(2,1)}, bf16[256,128]{1,0:T(8,128)(2,1)S(1)}, u32[]{:S(2)}, u32[]{:S(2)}) collective-permute-start(bf16[256,128]{1,0:T(8,128)(2,1)} %get-tuple-element.44), channel_id=1, source_target_pairs={{0,64},{32,96},{64,128},{96,160},{128,192},{160,224},{1,65},{33,97... | collective-permute-start | bytes 196616 | tf_op jit(solution)/shard_map/ppermute | solution.py:371
  126.5 19.8 %collective-permute-start.33 = (bf16[256,512]{1,0:T(8,128)(2,1)S(1)}, bf16[256,512]{1,0:T(8,128)(2,1)S(1)}, u32[]{:S(2)}, u32[]{:S(2)}) collective-permute-start(bf16[256,512]{1,0:T(8,128)(2,1)S(1)} %collective-permute-done.32.refs_2_), channel_id=1, source_target_pairs={{0,224},{32,0},{64,32},{96,64},{128,96},{160,128},{192,160},{224,1... | collective-permute-start | bytes 786440 | tf_op jit(solution)/shard_map/ppermute | solution.py:50
  126.8 19.4 %collective-permute-start.36 = (bf16[256,512]{1,0:T(8,128)(2,1)S(1)}, bf16[256,512]{1,0:T(8,128)(2,1)S(1)}, u32[]{:S(2)}, u32[]{:S(2)}) collective-permute-start(bf16[256,512]{1,0:T(8,128)(2,1)S(1)} %collective-permute-done.35.refs_5_), channel_id=1, source_target_pairs={{0,32},{32,64},{64,96},{96,128},{128,160},{160,192},{192,224},{224... | collective-permute-start | bytes 786440 | tf_op jit(solution)/shard_map/ppermute | solution.py:49
  129.9 11.9 %collective-permute-start.26 = (bf16[256,128]{1,0:T(8,128)(2,1)S(1)}, bf16[256,128]{1,0:T(8,128)(2,1)S(1)}, u32[]{:S(2)}, u32[]{:S(2)}) collective-permute-start(bf16[256,128]{1,0:T(8,128)(2,1)S(1)} %get-tuple-element.51), channel_id=1, source_target_pairs={{0,128},{32,160},{64,192},{96,224},{1,129},{33,161},{65,193},{97,2... | collective-permute-start | bytes 196616 | tf_op jit(solution)/shard_map/ppermute | solution.py:373
  144.5 15.8 %collective-permute-start.27 = (f32[512,128]{1,0:T(8,128)}, f32[512,128]{1,0:T(8,128)S(1)}, u32[]{:S(2)}, u32[]{:S(2)}) collective-permute-start(f32[512,128]{1,0:T(8,128)} %across.1.ret), channel_id=1, source_target_pairs={{0,1},{1,0},{2,3},{3,2},{4,5},{5,4},{6,7},{7,6},{8,9},{9,8},{10,11... | collective-permute-start | bytes 786440 | tf_op jit(solution)/shard_map/ppermute | solution.py:37
  146.2 6.9 %collective-permute-start.37 = (bf16[128,512]{1,0:T(8,128)(2,1)S(1)}, bf16[128,512]{1,0:T(8,128)(2,1)S(1)}, u32[]{:S(2)}, u32[]{:S(2)}) collective-permute-start(bf16[128,512]{1,0:T(8,128)(2,1)S(1)} %slice.60), channel_id=1, source_target_pairs={{0,32},{32,64},{64,96},{96,128},{128,160},{160,192},{192,224},{224... | collective-permute-start | bytes 393224 | tf_op jit(solution)/shard_map/ppermute | solution.py:56
  149.8 7.7 %collective-permute-start.22 = (bf16[16,256]{1,0:T(8,128)(2,1)S(1)}, bf16[16,256]{1,0:T(8,128)(2,1)S(1)}, u32[]{:S(2)}, u32[]{:S(2)}) collective-permute-start(bf16[16,256]{1,0:T(8,128)(2,1)S(1)} %slice.47), channel_id=1, source_target_pairs={{0,32},{32,64},{64,96},{96,128},{128,160},{160,192},{192,224},{1,3... | collective-permute-start | bytes 24584 | tf_op jit(solution)/shard_map/ppermute | solution.py:378
  165.6 25.2 %collective-permute-start.41 = (bf16[128,2048]{1,0:T(8,128)(2,1)}, bf16[128,2048]{1,0:T(8,128)(2,1)S(1)}, u32[]{:S(2)}, u32[]{:S(2)}) collective-permute-start(bf16[128,2048]{1,0:T(8,128)(2,1)} %get-tuple-element.50), channel_id=1, source_target_pairs={{0,24},{8,0},{16,8},{24,16},{1,25},{9,1},{17,9},{25,17},{2,26},{10... | collective-permute-start | bytes 1572872 | tf_op jit(solution)/shard_map/ppermute | solution.py:386
  168.7 22.1 %collective-permute-start.40 = (bf16[128,2048]{1,0:T(8,128)(2,1)}, bf16[128,2048]{1,0:T(8,128)(2,1)S(1)}, u32[]{:S(2)}, u32[]{:S(2)}) collective-permute-start(bf16[128,2048]{1,0:T(8,128)(2,1)} %get-tuple-element.49), channel_id=1, source_target_pairs={{0,16},{8,24},{16,0},{24,8},{1,17},{9,25},{17,1},{25,9},{2,18},{10... | collective-permute-start | bytes 1572872 | tf_op jit(solution)/shard_map/ppermute | solution.py:386
  168.7 26.2 %collective-permute-start.39 = (bf16[128,2048]{1,0:T(8,128)(2,1)}, bf16[128,2048]{1,0:T(8,128)(2,1)S(1)}, u32[]{:S(2)}, u32[]{:S(2)}) collective-permute-start(bf16[128,2048]{1,0:T(8,128)(2,1)} %get-tuple-element.48), channel_id=1, source_target_pairs={{0,8},{8,16},{16,24},{24,0},{1,9},{9,17},{17,25},{25,1},{2,10},{10... | collective-permute-start | bytes 1572872 | tf_op jit(solution)/shard_map/ppermute | solution.py:386
  (40 other events, 533.3 us)
where the time goes:
time: 201 us; the launch traced here: 200 us
  starting transfers between devices  80.3 us (40%)
  waiting for transfers between devices  60.3 us (30%)
  Pallas kernels  37.7 us (19%)
  local copies, waits for them, and re-layouts  14.1 us (7%)
  other arithmetic  6.14 us (3%)
    ppermute x3, waiting for transfers between devices, layer(): total = total + lax.ppermute(shares[k], 'y', ring(NY, k)).astype(f32)  25.6 us
    ppermute x12, waiting for transfers between devices, direct(): return [a] + [lax.ppermute(a, axis, ring(n, k)) for k in range(1, n)]  22.4 us
    ppermute x12, starting transfers between devices, direct(): return [a] + [lax.ppermute(a, axis, ring(n, k)) for k in range(1, n)]  21 us
    ppermute x6, starting transfers between devices, z_ring(): down = lax.ppermute(down, 'z', ring(NZ, -1))  15.7 us
    ppermute x3, starting transfers between devices, layer(): lax.ppermute(sent, 'z', line(NZ, k)).astype(f32)  10.1 us
    unnamed x67, local copies, waits for them, and re-layouts  8.08 us
    ppermute x6, starting transfers between devices, swap(): return lax.ppermute(a, 'c', SWAP)  8.05 us
    ppermute x1, starting transfers between devices, layer(): lax.ppermute((state + span_decay * near).astype(bf16), 'z', line(NZ, 4))  7.63 us
  transfers between devices with their start and end apart: 43, of which 14 were waited for; matrix products, arithmetic and copies ran while one was open for 4% of the time, Pallas kernels for 16%

commit v1 on v0

v1 whole, which is shorter than its diff:
```python
import jax
import jax.numpy as jnp
from jax import lax
from jax.experimental import pallas as pl
from jax.experimental.pallas import tpu as pltpu
from jax.sharding import Mesh
from jax.sharding import PartitionSpec as P

NZ, NY, NX = 8, 4, 4
SPAN = 512
HALO = 16
HEAD = 256
HALF = 128
eps = 1e-06
rope_base = 10000.0

bf16 = jnp.bfloat16
f32 = jnp.float32


def ring(n, k):
    return [(i, (i + k) % n) for i in range(n)]


def line(n, k):
    return [(i, i + k) for i in range(n - k)]


def to_heads(k):
    return [(2 * y + c, 2 * (2 * c + (k + y) % 2) + y // 2) for y in range(NY) for c in range(2)]


SWAP = [(0, 1), (1, 0)]


def swap(a):
    return lax.ppermute(a, "c", SWAP)


def direct(a, axis, n):
    return [a] + [lax.ppermute(a, axis, ring(n, k)) for k in range(1, n)]


def x_ring(a):
    n = a.shape[0] // 2
    one = lax.ppermute(a, "x", ring(NX, 1))
    three = lax.ppermute(a, "x", ring(NX, -1))
    top = lax.ppermute(one[:n], "x", ring(NX, 1))
    low = lax.ppermute(three[n:], "x", ring(NX, -1))
    return [a, one, top, low, three]


def z_ring(a, halves):
    chunks = [None] * NZ
    chunks[0] = a
    up = down = a
    for s in range(1, 4):
        up = lax.ppermute(up, "z", ring(NZ, 1))
        down = lax.ppermute(down, "z", ring(NZ, -1))
        chunks[NZ - s], chunks[s] = up, down
    if not halves:
        chunks[4] = lax.ppermute(up, "z", ring(NZ, 1))
        return chunks
    n = a.shape[0] // 2
    return chunks[:4] + chunks[5:] + [lax.ppermute(up[:n], "z", ring(NZ, 1)), lax.ppermute(down[n:], "z", ring(NZ, -1))]


VM = pl.BlockSpec(memory_space=pltpu.VMEM)
SM = pl.BlockSpec(memory_space=pltpu.SMEM)
ANY = pl.BlockSpec(memory_space=pl.ANY)


def local(body, **kw):
    return pl.pallas_call(body, compiler_params=pltpu.CompilerParams(vmem_limit_bytes=16 * 2**20), **kw)


ROWS = 112


def pack_body(at, decay, pool, query, key, value, state, pback, rback, s0, s1):
    y = at[1]
    for k, out in enumerate((s0, s1)):
        p = (y + k) % 2
        at_head = pl.ds(pl.multiple_of(p * HEAD, HEAD), HEAD)
        out[0:32, :256] = key[:, at_head]
        out[0:32, 256:] = value[:, at_head]
        out[32:64, :256] = pool[:, at_head]
        out[32:64, 256:] = query[:, at_head]
        out[64:96, :256] = pback[:, at_head]
        out[64:96, 256:] = rback[:, at_head]
        s = state[p]
        hi = s.astype(bf16)
        lo = (s - hi.astype(f32)).astype(bf16)
        d = jnp.full((8, HALF), decay[p], f32)
        d1 = d.astype(bf16)
        d2 = (d - d1.astype(f32)).astype(bf16)
        d3 = (d - d1.astype(f32) - d2.astype(f32)).astype(bf16)
        out[96:112, :256] = jnp.concatenate([hi, jnp.concatenate([d1, d2], axis=1)], axis=0)
        out[96:112, 256:] = jnp.concatenate([lo, jnp.concatenate([d3, d3], axis=1)], axis=0)


def pack(at, *args):
    return local(
        pack_body, in_specs=[SM, SM] + [VM] * 7, out_specs=[VM] * 2,
        out_shape=[jax.ShapeDtypeStruct((ROWS, 512), bf16)] * 2, name="pack",
    )(at, *args)


def norm_body(at, tok, gain, out, full):
    z, x, c = at[0], at[2], at[3]
    v = tok[...].astype(f32)
    v = v * lax.rsqrt(jnp.mean(v * v, axis=-1, keepdims=True) + eps) * gain[...]
    full[...] = v.astype(bf16)
    lane_in = lax.broadcasted_iota(jnp.int32, (512, 512), 0)
    lane_out = lax.broadcasted_iota(jnp.int32, (512, 512), 1)
    source = (lane_out % 128) // 64 * 256 + (lane_out % 64) // 32 * 128 + (x + NX - lane_out // 128) % NX * 32 + lane_out % 32
    order = (lane_in == source).astype(bf16)
    for pair in range(NZ // 2):
        two = [full[:, pl.ds(pl.multiple_of((z + 2 * pair + i) % NZ * 512 + c * 256, 256), 256)] for i in range(2)]
        r = jnp.dot(jnp.concatenate(two, axis=1), order, preferred_element_type=f32).astype(bf16)
        for kx in range(NX):
            out[kx, :, pair * 128:pair * 128 + 128] = r[:, kx * 128:kx * 128 + 128]


def norm(at, tok, gain):
    return local(
        norm_body, in_specs=[SM, VM, VM], out_specs=VM,
        out_shape=jax.ShapeDtypeStruct((NX, HALF, 512), bf16),
        scratch_shapes=[pltpu.VMEM((HALF, 4096), bf16)], name="norm",
    )(at, tok, gain)


def split_kv_body(*refs):
    for kz in range(NZ):
        refs[NZ][kz * 64:kz * 64 + 64, :] = refs[kz][0:64, :]


def split_kv(chunks):
    return local(
        split_kv_body, in_specs=[VM] * NZ, out_specs=VM,
        out_shape=jax.ShapeDtypeStruct((512, 512), bf16), name="split_kv",
    )(*chunks)


def split_pq_body(at, *refs):
    z, c = at[0], at[3]
    ins, (pq, keep, give) = refs[:NZ], refs[NZ:]
    for kz in range(NZ):
        pq[kz * 64:kz * 64 + 64, :] = ins[kz][64:128, :]
        for out, half in ((keep, c), (give, 1 - c)):
            hi = ins[kz][128:144, pl.ds(pl.multiple_of(half * HALF, HALF), HALF)].astype(f32)
            lo = ins[kz][128:144, pl.ds(pl.multiple_of(HEAD + half * HALF, HALF), HALF)].astype(f32)
            out[pl.ds(pl.multiple_of(((z + kz) % NZ) * 16, 16), 16), :] = hi + lo


def split_pq(at, chunks):
    return local(
        split_pq_body, in_specs=[SM] + [VM] * NZ, out_specs=[VM] * 3,
        out_shape=[jax.ShapeDtypeStruct((512, 512), bf16)] + [jax.ShapeDtypeStruct((HALF, HALF), f32)] * 2,
        name="split_pq",
    )(at, *chunks)


def multiply(toks, ws):
    w0, w1, w2a, w2b, w3 = ws
    acc = None
    for kx in range(NX):
        w = jnp.concatenate([w2a[...], w2b[...]], axis=0) if kx == 2 else (w0, w1, None, w3)[kx][...]
        rows = jnp.concatenate([t[kx] for t in toks], axis=0)
        r = jnp.dot(rows, w, preferred_element_type=f32)
        acc = r if acc is None else acc + r
    return acc


def span_rows(y, k):
    return pl.ds(pl.multiple_of(((y + NY - k) % NY) * HALF, HALF), HALF)


def kv_body(at, *refs):
    y, c = at[1], at[3]
    toks, ws, (kpart, vkeep, send) = refs[:4], refs[4:9], refs[9:]
    acc = multiply(toks, ws)
    for k in range(NY):
        r = acc[k * HALF:(k + 1) * HALF]
        rows = span_rows(y, k)
        kpart[rows, :] = r[:, :256]
        vkeep[rows, :] = jnp.where(c == 0, r[:, 256:384], r[:, 384:])
        send[rows, :256] = r[:, :256].astype(bf16)
        send[rows, 256:] = jnp.where(c == 0, r[:, 384:], r[:, 256:384]).astype(bf16)


def project_kv(at, toks, ws):
    return local(
        kv_body, in_specs=[SM] + [VM] * 9, out_specs=[VM] * 3,
        out_shape=[jax.ShapeDtypeStruct((SPAN, HEAD), f32), jax.ShapeDtypeStruct((SPAN, HALF), f32),
                   jax.ShapeDtypeStruct((SPAN, 384), bf16)],
        name="project_kv",
    )(at, *toks, *ws)


def pq_body(at, *refs):
    toks, ws, (own, send) = refs[:4], refs[4:9], refs[9:]
    acc = multiply(toks, ws)
    for k in range(NY):
        r = acc[k * HALF:(k + 1) * HALF]
        rows = span_rows(at[1], k)
        own[rows, :] = r
        send[rows, :] = r.astype(bf16)


def project_pq(at, toks, ws):
    return local(
        pq_body, in_specs=[SM] + [VM] * 9, out_specs=[VM] * 2,
        out_shape=[jax.ShapeDtypeStruct((SPAN, 512), f32), jax.ShapeDtypeStruct((SPAN, 512), bf16)],
        name="project_pq",
    )(at, *toks, *ws)


def turn(v, cosine, sine):
    a, b = v[:, :HALF], v[:, HALF:]
    return jnp.concatenate([a * cosine - b * sine, a * sine + b * cosine], axis=1)


def state_body(at, rates, kpart, vkeep, got, cosine, sine, keep, other, rk, val, state, sent, start):
    z, c = at[0], at[3]
    for zs in range(NZ):
        start[pl.ds(pl.multiple_of(zs * 32 + c * 16, 16), 16), :] = keep[zs * 16:zs * 16 + 16, :]
        start[pl.ds(pl.multiple_of(zs * 32 + (1 - c) * 16, 16), 16), :] = other[zs * 16:zs * 16 + 16, :]
    key = (kpart[...] + got[:, :256].astype(f32)).astype(bf16).astype(f32)
    value = (vkeep[...] + got[:, 256:].astype(f32)).astype(bf16)
    val[...] = value
    turned = turn(key, cosine[...], sine[...]) * HEAD ** -0.5
    rk[...] = turned.astype(bf16)
    within = lax.broadcasted_iota(jnp.int32, (SPAN, HALF), 0).astype(f32)
    fade = jnp.exp(-(SPAN - 1.0 - within) * rates[0:1, :])
    faded = (turned * jnp.concatenate([fade, fade], axis=1)).astype(bf16)
    s = lax.dot_general(faded, value, (((0,), (0,)), ((), ())), preferred_element_type=f32)
    s = s + jnp.where(z == 0, rates[8:9, :], 0.0) * start[...]
    state[...] = s
    sent[...] = s.astype(bf16)


def span_state(at, rates, *args):
    return local(
        state_body, in_specs=[SM] + [VM] * 8, out_specs=[VM] * 5,
        out_shape=[jax.ShapeDtypeStruct((SPAN, HEAD), bf16), jax.ShapeDtypeStruct((SPAN, HALF), bf16),
                   jax.ShapeDtypeStruct((HEAD, HALF), f32), jax.ShapeDtypeStruct((HEAD, HALF), bf16),
                   jax.ShapeDtypeStruct((HEAD, HALF), f32)],
        name="span_state",
    )(at, rates, *args)


def inside_body(rates, own, got, cosine, sine, rk, val, pool_in, tail, inside, faded):
    p = (own[:, :256] + got[:, :256].astype(f32)).astype(bf16)
    pool_in[...] = p
    tail[...] = p[SPAN - HALO:]
    query = (own[:, 256:] + got[:, 256:].astype(f32)).astype(bf16).astype(f32)
    rq = turn(query, cosine[...], sine[...])
    within = lax.broadcasted_iota(jnp.int32, (SPAN, HALF), 0).astype(f32)
    fade = jnp.exp(-(within + 1.0) * rates[0:1, :])
    faded[...] = (rq * jnp.concatenate([fade, fade], axis=1)).astype(bf16)
    rq = rq.astype(bf16)
    for b in range(4):
        n = (b + 1) * 128
        scores = lax.dot_general(rq[b * 128:n], rk[:n, :], (((1,), (1,)), ((), ())), preferred_element_type=f32)
        far = lax.broadcasted_iota(jnp.int32, (128, n), 0) + b * 128 - lax.broadcasted_iota(jnp.int32, (128, n), 1)
        fade = jnp.exp(-jnp.maximum(far, 0).astype(f32) * jnp.concatenate([rates[0:1, :]] * (b + 1), axis=1))
        weights = jnp.where(far >= 0, scores * fade, 0.0).astype(bf16)
        inside[b * 128:n, :] = jnp.dot(weights, val[:n, :], preferred_element_type=f32)


def inside_span(rates, *args):
    return local(
        inside_body, in_specs=[VM] * 7, out_specs=[VM] * 4,
        out_shape=[jax.ShapeDtypeStruct((SPAN, HEAD), bf16), jax.ShapeDtypeStruct((HALO, HEAD), bf16),
                   jax.ShapeDtypeStruct((SPAN, HALF), f32),
                   jax.ShapeDtypeStruct((SPAN, HEAD), bf16)],
        name="inside",
    )(rates, *args)


def across_body(at, rates, inside, faded, near, far, start, ret):
    d = rates[8:9, :]
    carried = near[...] + d * d * d * far[...].astype(f32) + jnp.where(at[0] == 0, 1.0, 0.0) * start[...]
    ret[...] = inside[...] + jnp.dot(faded[...], carried.astype(bf16), preferred_element_type=f32)


def across_spans(at, rates, *args):
    return local(
        across_body, in_specs=[SM] + [VM] * 6, out_specs=VM,
        out_shape=jax.ShapeDtypeStruct((SPAN, HALF), f32), name="across",
    )(at, rates, *args)


def pool_body(at, pool_in, before, group_map, scale, out):
    z, y = at[0], at[1]
    ext = jnp.concatenate([before[...], pool_in[...]], axis=0).astype(f32)
    sums = ext
    chosen = None
    for g in range(4):
        sums = sums + pltpu.roll(sums, 2 ** g, 0)
        chosen = sums if chosen is None else jnp.where(y == g, sums, chosen)
    rows = lax.broadcasted_iota(jnp.int32, (SPAN, HEAD), 0) + z * SPAN + 1
    counts = jnp.minimum(lax.shift_left(jnp.int32(2), y), rows).astype(f32)
    differ = (chosen[HALO:] / counts - ext[HALO:]).astype(bf16)
    out[...] = (jnp.dot(differ, group_map[y], preferred_element_type=f32) * scale[:, pl.ds(pl.multiple_of(y * HEAD, HEAD), HEAD)]).astype(bf16)


def pooling(at, *args):
    return local(
        pool_body, in_specs=[SM] + [VM] * 4, out_specs=VM,
        out_shape=jax.ShapeDtypeStruct((SPAN, HEAD), bf16), name="pooling",
    )(at, *args)


def back_body(at, pool, ret, other, *refs):
    y, c = at[1], at[3]
    ws, outs, act, res = refs[:9], refs[9:13], refs[13], refs[14]
    r, o = ret[...], other[...]
    square = jnp.sum(r * r, axis=-1, keepdims=True) + jnp.sum(o * o, axis=-1, keepdims=True)
    factor = lax.rsqrt(square * (1.0 / HEAD) + eps)
    act[:, :256] = pool[...]
    act[:, pl.ds(pl.multiple_of(HEAD + c * HALF, HALF), HALF)] = (r * factor).astype(bf16)
    act[:, pl.ds(pl.multiple_of(HEAD + (1 - c) * HALF, HALF), HALF)] = (o * factor).astype(bf16)
    for i, kz in enumerate((0, 1, 2, 3, 5, 6, 7, 4)):
        w = ws[i][...] if kz != 4 else jnp.concatenate([ws[7][...], ws[8][...]], axis=0)
        r = lax.dot_general(act[...], w, (((1,), (1,)), ((), ())), preferred_element_type=f32)
        res[:, kz * 256:kz * 256 + 256] = r.astype(bf16)
    for k, out in enumerate(outs):
        out[...] = res[pl.ds(pl.multiple_of(((y + k) % NY) * HALF, HALF), HALF), :]


def back(at, pool, ret, other, ws):
    return local(
        back_body, in_specs=[SM] + [VM] * 12, out_specs=[VM] * 4,
        out_shape=[jax.ShapeDtypeStruct((HALF, 2048), bf16)] * 4,
        scratch_shapes=[pltpu.VMEM((SPAN, 512), bf16), pltpu.VMEM((SPAN, 2048), bf16)], name="back",
    )(at, pool, ret, other, *ws)


def total_body(at, s0, s1, s2, s3, keep, give):
    c = at[3]
    for out, half in ((keep, c), (give, 1 - c)):
        rows = pl.ds(pl.multiple_of(half * 64, 64), 64)
        out[...] = (s0[rows, :].astype(f32) + s1[rows, :].astype(f32) + (s2[rows, :].astype(f32) + s3[rows, :].astype(f32))).astype(bf16)


def total(at, arrived):
    return local(
        total_body, in_specs=[SM] + [VM] * 4, out_specs=[VM] * 2,
        out_shape=[jax.ShapeDtypeStruct((64, 2048), bf16)] * 2, name="total",
    )(at, *arrived)


def mixed_body(at, keep, got, out):
    z, x, c = at[0], at[2], at[3]
    lane_in = lax.broadcasted_iota(jnp.int32, (256, 256), 0)
    lane_out = lax.broadcasted_iota(jnp.int32, (256, 256), 1)
    source = (x + NX - (lane_out % 128) // 32) % NX * 64 + lane_out // 128 * 32 + lane_out % 32
    order = (lane_in == source).astype(bf16)
    for kz in range(NZ):
        for ref, core in ((keep, c), (got, 1 - c)):
            r = jnp.dot(ref[:, kz * 256:kz * 256 + 256], order, preferred_element_type=f32).astype(bf16)
            out[:, pl.ds(pl.multiple_of((z + kz) % NZ * 512 + core * 256, 256), 256)] = r


def mixed(at, keep, got):
    return local(
        mixed_body, in_specs=[SM] + [VM] * 2, out_specs=VM,
        out_shape=jax.ShapeDtypeStruct((64, 4096), bf16), name="mixed",
    )(at, keep, got)


def layer(tokens, norm_gain, pool_proj, query_proj, key_proj, value_proj, pool_map, pool_scale,
          decay_rate, start_state, pool_back, retention_back):
    z, y, x, c = (lax.axis_index(a) for a in ("z", "y", "x", "c"))
    at = jnp.stack([z, y, x, c]).astype(jnp.int32)

    s0, s1 = pack(at, decay_rate, pool_proj, query_proj, key_proj, value_proj, start_state[0], pool_back.T, retention_back.T)
    r0 = lax.ppermute(s0, ("y", "c"), to_heads(0))
    r1 = lax.ppermute(s1, ("y", "c"), to_heads(1))
    even = y % 2 == 0
    a, b = jnp.where(even, r0, r1), jnp.where(even, r1, r0)
    shard_in = jnp.concatenate([a[:32], b[:32], a[32:64], b[32:64], a[96:104], b[96:104]], axis=0)
    shard_out = jnp.concatenate([a[64:96], b[64:96]], axis=0)

    toks = direct(norm(at, tokens[0], norm_gain[None]), "y", NY)


    in_z = z_ring(shard_in, False)
    kv_list = x_ring(split_kv(in_z))
    plane_pq, keep, give = split_pq(at, in_z)
    pq_list = x_ring(plane_pq)
    start_other = swap(give)

    plane_o = jnp.concatenate(direct(shard_out, "x", NX), axis=0)
    wt = z_ring(plane_o, True)

    three = r0[104:112, :].astype(f32)
    rate = (three[:, :128] + three[:, 128:256]) + three[:, 256:384]
    rates = jnp.concatenate([rate, jnp.exp(-SPAN * rate)], axis=0)
    span_decay = rates[8:9, :]
    positions = (jnp.arange(SPAN, dtype=jnp.int32) + z * SPAN)
    inv_freq = 1.0 / rope_base ** jnp.linspace(0.0, 1.0, HALF, dtype=f32)
    angles = positions.astype(f32)[:, None] * inv_freq[None, :]
    cosine, sine = jnp.cos(angles), jnp.sin(angles)

    kpart, vkeep, send = project_kv(at, toks, kv_list)
    got = swap(send)
    rk, val, state, sent, start = span_state(at, rates, kpart, vkeep, got, cosine, sine, keep, start_other)
    n1, n2, n3 = (lax.ppermute(sent, "z", line(NZ, k)).astype(f32) for k in (1, 2, 3))
    near = n1 + span_decay * (n2 + span_decay * n3)
    far = lax.ppermute((state + span_decay * near).astype(bf16), "z", line(NZ, 4))

    own, send = project_pq(at, toks, pq_list)
    got = swap(send)
    pool_in, tail, inside, faded = inside_span(rates, own, got, cosine, sine, rk, val)
    before = lax.ppermute(tail, "z", line(NZ, 1))
    pool_out = pooling(at, pool_in, before, pool_map, pool_scale[None])
    ret = across_spans(at, rates, inside, faded, near, far, start)
    other = swap(ret)

    shares = back(at, pool_out, ret, other, wt)
    arrived = [shares[0]] + [lax.ppermute(shares[k], "y", ring(NY, k)) for k in range(1, NY)]
    keep, give = total(at, arrived)
    got = swap(give)
    return mixed(at, keep, got)[None]


def solution(mesh):
    torus = Mesh(mesh.devices.reshape(NZ, NY, NX, 2), ("z", "y", "x", "c"))
    sp, sp_fs = ("z", "y"), ("z", "y", "x")
    placed = (
        P("x", sp, None), P(), P(sp_fs, "c"), P(sp_fs, "c"), P(sp_fs, "c"), P(sp_fs, "c"), P(), P(),
        P("c"), P("x", "c", sp, None), P("c", sp_fs), P("c", sp_fs),
    )
    return jax.shard_map(layer, mesh=torus, in_specs=placed, out_specs=P("x", ("z", "y", "c"), None), check_vma=False)
```

time: 201 us -> 179 us (0.89); the launches traced: 200 us -> 176 us
  Pallas kernels: 37.7 us -> 14.8 us
  waiting for transfers between devices: 60.3 us -> 65 us
  other arithmetic: 6.14 us -> 1.93 us
  starting transfers between devices: 80.3 us -> 77.9 us
    pallas_call x12 -> x13, Pallas kernels: 37.7 us -> 14.8 us  [the longest x1 2.16 us: back(): local(back_body, in_specs=[SM] + [VM] * 12, out_specs=[VM] * 4, out_shape...]
    ppermute x12 -> x6, starting transfers between devices: 21 us -> 5.75 us  [direct(): return [a] + [lax.ppermute(a, axis, ring(n, k)) for k in range(1, n)]]
    ppermute x4 -> x12, starting transfers between devices: 4.97 us -> 17.6 us  [the longest x2 6.16 us: x_ring(): low = lax.ppermute(three[n:], 'x', ring(NX, -1))]
    ppermute x12 -> x6, waiting for transfers between devices: 22.4 us -> 11.2 us  [direct(): return [a] + [lax.ppermute(a, axis, ring(n, k)) for k in range(1, n)]]
    ppermute x4 -> x12, waiting for transfers between devices: 25.6 us -> 33.6 us  [the longest x3 22.3 us: layer(): lax.ppermute(shares[k], 'y', ring(NY, k))]
    ppermute x6, waiting for transfers between devices: 0.03 us -> 7.58 us  [z_ring(): up = lax.ppermute(up, 'z', ring(NZ, 1))]
    ppermute x6, starting transfers between devices: 15.7 us -> 9.37 us  [z_ring(): down = lax.ppermute(down, 'z', ring(NZ, -1))]
    unnamed x67 -> x57, local copies, waits for them, and re-layouts: 8.08 us -> 14.1 us
  transfers between devices with their start and end apart: 43 -> 44, of which waited for: 14 -> 19; matrix products, arithmetic and copies ran while one was open for 4% -> 2% of each run, Pallas kernels for 16% -> 5%
where the time goes in v1:
time: 179 us; the launch traced here: 176 us
  starting transfers between devices  77.9 us (44%)
  waiting for transfers between devices  65 us (36%)
  local copies, waits for them, and re-layouts  15.4 us (9%)
  Pallas kernels  14.8 us (8%)
  other arithmetic  1.93 us (1%)
    ppermute x3, waiting for transfers between devices, layer(): lax.ppermute(shares[k], 'y', ring(NY, k))  22.3 us
    unnamed x57, local copies, waits for them, and re-layouts  14.1 us
    ppermute x6, waiting for transfers between devices, direct(): return [a] + [lax.ppermute(a, axis, ring(n, k)) for k in range(1, n)]  11.2 us
    ppermute x3, starting transfers between devices, layer(): lax.ppermute(sent, 'z', line(NZ, k)).astype(f32)  10.7 us
    ppermute x5, starting transfers between devices, swap(): return lax.ppermute(a, 'c', SWAP)  10.3 us
    ppermute x6, starting transfers between devices, z_ring(): down = lax.ppermute(down, 'z', ring(NZ, -1))  9.37 us
    ppermute x1, starting transfers between devices, layer(): lax.ppermute((state + span_decay * near).astype(bf16), 'z', line(NZ, 4))  8.32 us
    ppermute x6, waiting for transfers between devices, z_ring(): up = lax.ppermute(up, 'z', ring(NZ, 1))  7.58 us
  transfers between devices with their start and end apart: 44, of which 19 were waited for; matrix products, arithmetic and copies ran while one was open for 2% of the time, Pallas kernels for 5%

profile of v1, /device:TPU:1, one launch (start us, length us, event | category | flops | bytes accessed | tf_op | source)
XLA Modules:
  0.0 175.5 jit_solution(17601606539754070032)
XLA Ops:
  5.8 6.2 %collective-permute-start = (bf16[112,512]{1,0:T(8,128)(2,1)S(1)}, bf16[112,512]{1,0:T(8,128)(2,1)S(1)}, u32[]{:S(2)}, u32[]{:S(2)}) collective-permute-start(bf16[112,512]{1,0:T(8,128)(2,1)S(1)} %get-tuple-element.30), channel_id=1, source_target_pairs={{0,0},{1,16},{8,8},{9,24},{16,1},{17,17},{24,9},{25,25},{2,2},{3,1... | collective-permute-start | bytes 344072 | tf_op jit(solution)/shard_map/ppermute | solution.py:380
  12.6 2.1 %collective-permute-done = bf16[112,512]{1,0:T(8,128)(2,1)S(1)} collective-permute-done((bf16[112,512]{1,0:T(8,128)(2,1)S(1)}, bf16[112,512]{1,0:T(8,128)(2,1)S(1)}, u32[]{:S(2)}, u32[]{:S(2)}) %collective-permute-start) | collective-permute-done | bytes 114720 | tf_op jit(solution)/shard_map/ppermute | solution.py:380
  14.8 2.8 %collective-permute-done.4 = bf16[112,512]{1,0:T(8,128)(2,1)S(1)} collective-permute-done((bf16[112,512]{1,0:T(8,128)(2,1)S(1)}, bf16[112,512]{1,0:T(8,128)(2,1)S(1)}, u32[]{:S(2)}, u32[]{:S(2)}) %collective-permute-start.4) | collective-permute-done | bytes 114720 | tf_op jit(solution)/shard_map/ppermute | solution.py:381
  20.5 3.9 %collective-permute-start.5 = (bf16[144,512]{1,0:T(8,128)(2,1)S(1)}, bf16[144,512]{1,0:T(8,128)(2,1)S(1)}, u32[]{:S(2)}, u32[]{:S(2)}) collective-permute-start(bf16[144,512]{1,0:T(8,128)(2,1)S(1)} %constant_dynamic-update-slice_fusion.refs_0_), channel_id=1, source_target_pairs={{0,224},{32,0},{64,32},{96,64},{128,96},{160,128},{192,160},{224,1... | collective-permute-start | bytes 442376 | tf_op jit(solution)/shard_map/ppermute | solution.py:59
  24.5 2.5 %collective-permute-done.8.refs_7_ = bf16[144,512]{1,0:T(8,128)(2,1)S(1)} collective-permute-done((bf16[144,512]{1,0:T(8,128)(2,1)S(1)}, bf16[144,512]{1,0:T(8,128)(2,1)S(1)}, u32[]{:S(2)}, u32[]{:S(2)}) %collective-permute-start.8) | collective-permute-done | bytes 147488 | tf_op jit(solution)/shard_map/ppermute | solution.py:58
  27.0 2.7 %collective-permute-start.6 = (bf16[144,512]{1,0:T(8,128)(2,1)S(1)}, bf16[144,512]{1,0:T(8,128)(2,1)S(1)}, u32[]{:S(2)}, u32[]{:S(2)}) collective-permute-start(bf16[144,512]{1,0:T(8,128)(2,1)S(1)} %collective-permute-done.5.refs_1_), channel_id=1, source_target_pairs={{0,224},{32,0},{64,32},{96,64},{128,96},{160,128},{192,160},{224,1... | collective-permute-start | bytes 442376 | tf_op jit(solution)/shard_map/ppermute | solution.py:59
  29.7 2.5 %collective-permute-done.9.refs_6_ = bf16[144,512]{1,0:T(8,128)(2,1)S(1)} collective-permute-done((bf16[144,512]{1,0:T(8,128)(2,1)S(1)}, bf16[144,512]{1,0:T(8,128)(2,1)S(1)}, u32[]{:S(2)}, u32[]{:S(2)}) %collective-permute-start.9) | collective-permute-done | bytes 147488 | tf_op jit(solution)/shard_map/ppermute | solution.py:58
  32.2 2.7 %collective-permute-start.7 = (bf16[144,512]{1,0:T(8,128)(2,1)S(1)}, bf16[144,512]{1,0:T(8,128)(2,1)S(1)}, u32[]{:S(2)}, u32[]{:S(2)}) collective-permute-start(bf16[144,512]{1,0:T(8,128)(2,1)S(1)} %collective-permute-done.6.refs_2_), channel_id=1, source_target_pairs={{0,224},{32,0},{64,32},{96,64},{128,96},{160,128},{192,160},{224,1... | collective-permute-start | bytes 442376 | tf_op jit(solution)/shard_map/ppermute | solution.py:59
  34.9 2.5 %collective-permute-done.10.refs_5_ = bf16[144,512]{1,0:T(8,128)(2,1)S(1)} collective-permute-done((bf16[144,512]{1,0:T(8,128)(2,1)S(1)}, bf16[144,512]{1,0:T(8,128)(2,1)S(1)}, u32[]{:S(2)}, u32[]{:S(2)}) %collective-permute-start.10) | collective-permute-done | bytes 147488 | tf_op jit(solution)/shard_map/ppermute | solution.py:58
  37.4 5.7 %collective-permute-done.11.refs_4_ = bf16[144,512]{1,0:T(8,128)(2,1)S(1)} collective-permute-done((bf16[144,512]{1,0:T(8,128)(2,1)S(1)}, bf16[144,512]{1,0:T(8,128)(2,1)S(1)}, u32[]{:S(2)}, u32[]{:S(2)}) %collective-permute-start.11) | collective-permute-done | bytes 147488 | tf_op jit(solution)/shard_map/ppermute | solution.py:62
  50.1 1.7 collective-permute-start.1
  51.7 10.0 %collective-permute-done.29 = bf16[64,512]{1,0:T(8,128)(2,1)} collective-permute-done((bf16[64,512]{1,0:T(8,128)(2,1)S(1)}, bf16[64,512]{1,0:T(8,128)(2,1)}, u32[]{:S(2)}, u32[]{:S(2)}) %collective-permute-start.29) | collective-permute-done | bytes 65568 | tf_op jit(solution)/shard_map/ppermute | solution.py:41
  70.9 2.4 %collective-permute-start.31 = (bf16[64,512]{1,0:T(8,128)(2,1)S(1)}, bf16[64,512]{1,0:T(8,128)(2,1)S(1)}, u32[]{:S(2)}, u32[]{:S(2)}) collective-permute-start(bf16[64,512]{1,0:T(8,128)(2,1)S(1)} %pad_maximum_fusion), channel_id=1, source_target_pairs={{0,6},{2,0},{4,2},{6,4},{1,7},{3,1},{5,3},{7,5},{8,14},{10,8},{12,... | collective-permute-start | bytes 196616 | tf_op jit(solution)/shard_map/ppermute | solution.py:41
  74.6 3.3 %collective-permute-start.14 = (bf16[512,512]{1,0:T(8,128)(2,1)S(1)}, bf16[512,512]{1,0:T(8,128)(2,1)S(1)}, u32[]{:S(2)}, u32[]{:S(2)}) collective-permute-start(bf16[512,512]{1,0:T(8,128)(2,1)S(1)} %get-tuple-element.32.refs_4_), channel_id=1, source_target_pairs={{0,6},{2,0},{4,2},{6,4},{1,7},{3,1},{5,3},{7,5},{8,14},{10,8},{12,... | collective-permute-start | bytes 1572872 | tf_op jit(solution)/shard_map/ppermute | solution.py:47
  77.9 2.7 %collective-permute-start.20 = (bf16[256,512]{1,0:T(8,128)(2,1)S(1)}, bf16[256,512]{1,0:T(8,128)(2,1)S(1)}, u32[]{:S(2)}, u32[]{:S(2)}) collective-permute-start(bf16[256,512]{1,0:T(8,128)(2,1)S(1)} %slice.89), channel_id=1, source_target_pairs={{0,6},{2,0},{4,2},{6,4},{1,7},{3,1},{5,3},{7,5},{8,14},{10,8},{12,... | collective-permute-start | bytes 786440 | tf_op jit(solution)/shard_map/ppermute | solution.py:49
  80.6 2.9 %collective-permute-done.12.refs_5_ = bf16[512,512]{1,0:T(8,128)(2,1)S(1)} collective-permute-done((bf16[512,512]{1,0:T(8,128)(2,1)S(1)}, bf16[512,512]{1,0:T(8,128)(2,1)S(1)}, u32[]{:S(2)}, u32[]{:S(2)}) %collective-permute-start.12) | collective-permute-done | bytes 524320 | tf_op jit(solution)/shard_map/ppermute | solution.py:46
  86.1 2.1 %collective-permute-done.18.refs_6_ = bf16[256,512]{1,0:T(8,128)(2,1)S(1)} collective-permute-done((bf16[256,512]{1,0:T(8,128)(2,1)S(1)}, bf16[256,512]{1,0:T(8,128)(2,1)S(1)}, u32[]{:S(2)}, u32[]{:S(2)}) %collective-permute-start.18) | collective-permute-done | bytes 262176 | tf_op jit(solution)/shard_map/ppermute | solution.py:48
  88.2 2.3 %collective-permute-done.20.refs_7_ = bf16[256,512]{1,0:T(8,128)(2,1)S(1)} collective-permute-done((bf16[256,512]{1,0:T(8,128)(2,1)S(1)}, bf16[256,512]{1,0:T(8,128)(2,1)S(1)}, u32[]{:S(2)}, u32[]{:S(2)}) %collective-permute-start.20) | collective-permute-done | bytes 262176 | tf_op jit(solution)/shard_map/ppermute | solution.py:49
  90.5 1.8 %project_kv.1 = (f32[512,256]{1,0:T(8,128)S(1)}, f32[512,128]{1,0:T(8,128)S(1)}, bf16[512,384]{1,0:T(8,128)(2,1)S(1)}) custom-call(s32[4]{0:T(128)S(1)} %pad_add_fusion.at, bf16[4,128,512]{2,1,0:T(8,128)(2,1)S(1)} %norm.1.refs_0_, bf16[4,128,512]{2,1,0:T(8,128)(2,1)S(1)} %collective-permute-done.1.refs_1_, ...), custom_call_target="tpu_custom_call" | custom-call | tf_op jit(solution)/shard_map/project_kv/pallas_call | solution.py:193
  92.3 5.3 %collective-permute-start.21 = (bf16[512,384]{1,0:T(8,128)(2,1)S(1)}, bf16[512,384]{1,0:T(8,128)(2,1)S(1)}, u32[]{:S(2)}, u32[]{:S(2)}) collective-permute-start(bf16[512,384]{1,0:T(8,128)(2,1)S(1)} %get-tuple-element.37), channel_id=1, source_target_pairs={{0,1},{1,0},{2,3},{3,2},{4,5},{5,4},{6,7},{7,6},{8,9},{9,8},{10,11... | collective-permute-start | bytes 1179656 | tf_op jit(solution)/shard_map/ppermute | solution.py:37
  98.3 3.5 %collective-permute-start.15 = (bf16[256,512]{1,0:T(8,128)(2,1)S(1)}, bf16[256,512]{1,0:T(8,128)(2,1)S(1)}, u32[]{:S(2)}, u32[]{:S(2)}) collective-permute-start(bf16[256,512]{1,0:T(8,128)(2,1)S(1)} %slice.87), channel_id=1, source_target_pairs={{0,6},{2,0},{4,2},{6,4},{1,7},{3,1},{5,3},{7,5},{8,14},{10,8},{12,... | collective-permute-start | bytes 786440 | tf_op jit(solution)/shard_map/ppermute | solution.py:49
  104.2 3.2 %collective-permute-done.15.refs_7_ = bf16[256,512]{1,0:T(8,128)(2,1)S(1)} collective-permute-done((bf16[256,512]{1,0:T(8,128)(2,1)S(1)}, bf16[256,512]{1,0:T(8,128)(2,1)S(1)}, u32[]{:S(2)}, u32[]{:S(2)}) %collective-permute-start.15) | collective-permute-done | bytes 262176 | tf_op jit(solution)/shard_map/ppermute | solution.py:49
  107.4 1.8 %project_pq.1 = (f32[512,512]{1,0:T(8,128)S(1)}, bf16[512,512]{1,0:T(8,128)(2,1)S(1)}) custom-call(s32[4]{0:T(128)S(1)} %pad_add_fusion.at, bf16[4,128,512]{2,1,0:T(8,128)(2,1)S(1)} %norm.1.refs_0_, bf16[4,128,512]{2,1,0:T(8,128)(2,1)S(1)} %collective-permute-done.1.refs_1_, bf16[4,128,512]{2,1,0:T(8,128)(2,1)S(1)} %collective-permute-done.2.refs_2_, ...), custom_call_target="tpu_custom_call" | custom-call | tf_op jit(solution)/shard_map/project_pq/pallas_call | solution.py:212
  111.4 3.4 %collective-permute-start.26 = (bf16[256,128]{1,0:T(8,128)(2,1)S(1)}, bf16[256,128]{1,0:T(8,128)(2,1)S(1)}, u32[]{:S(2)}, u32[]{:S(2)}) collective-permute-start(bf16[256,128]{1,0:T(8,128)(2,1)S(1)} %get-tuple-element.46), channel_id=1, source_target_pairs={{0,96},{32,128},{64,160},{96,192},{128,224},{1,97},{33,129},{65,16... | collective-permute-start | bytes 196616 | tf_op jit(solution)/shard_map/ppermute | solution.py:411
  114.8 6.0 %collective-permute-start.25 = (bf16[256,128]{1,0:T(8,128)(2,1)S(1)}, bf16[256,128]{1,0:T(8,128)(2,1)S(1)}, u32[]{:S(2)}, u32[]{:S(2)}) collective-permute-start(bf16[256,128]{1,0:T(8,128)(2,1)S(1)} %get-tuple-element.46), channel_id=1, source_target_pairs={{0,64},{32,96},{64,128},{96,160},{128,192},{160,224},{1,65},{33,97... | collective-permute-start | bytes 196616 | tf_op jit(solution)/shard_map/ppermute | solution.py:411
  123.8 8.3 %collective-permute-start.27 = (bf16[256,128]{1,0:T(8,128)(2,1)S(1)}, bf16[256,128]{1,0:T(8,128)(2,1)S(1)}, u32[]{:S(2)}, u32[]{:S(2)}) collective-permute-start(bf16[256,128]{1,0:T(8,128)(2,1)S(1)} %get-tuple-element.55), channel_id=1, source_target_pairs={{0,128},{32,160},{64,192},{96,224},{1,129},{33,161},{65,193},{97,2... | collective-permute-start | bytes 196616 | tf_op jit(solution)/shard_map/ppermute | solution.py:413
  135.8 2.7 %collective-permute-start.39 = (bf16[128,512]{1,0:T(8,128)(2,1)S(1)}, bf16[128,512]{1,0:T(8,128)(2,1)S(1)}, u32[]{:S(2)}, u32[]{:S(2)}) collective-permute-start(bf16[128,512]{1,0:T(8,128)(2,1)S(1)} %slice.93), channel_id=1, source_target_pairs={{0,224},{32,0},{64,32},{96,64},{128,96},{160,128},{192,160},{224,1... | collective-permute-start | bytes 393224 | tf_op jit(solution)/shard_map/ppermute | solution.py:65
  142.0 2.2 %back.1 = (bf16[128,2048]{1,0:T(8,128)(2,1)S(1)}, bf16[128,2048]{1,0:T(8,128)(2,1)S(1)}, bf16[128,2048]{1,0:T(8,128)(2,1)S(1)}, bf16[128,2048]{1,0:T(8,128)(2,1)S(1)}) custom-call(s32[4]{0:T(128)S(1)} %pad_add_fusion.at, bf16[512,256]{1,0:T(8,128)(2,1)S(1)} %pooling.1.pool, f32[512,128]{1,0:T(8,128)S(1)} %across.1.ret, ...), custom_call_target="tpu_custom_call" | custom-call | tf_op jit(solution)/shard_map/back/pallas_call | solution.py:334
  145.8 2.0 %collective-permute-start.42 = (bf16[128,2048]{1,0:T(8,128)(2,1)S(1)}, bf16[128,2048]{1,0:T(8,128)(2,1)S(1)}, u32[]{:S(2)}, u32[]{:S(2)}) collective-permute-start(bf16[128,2048]{1,0:T(8,128)(2,1)S(1)} %get-tuple-element.52), channel_id=1, source_target_pairs={{0,24},{8,0},{16,8},{24,16},{1,25},{9,1},{17,9},{25,17},{2,26},{10... | collective-permute-start | bytes 1572872 | tf_op jit(solution)/shard_map/ppermute | solution.py:424
  147.8 11.1 %collective-permute-done.40.s1 = bf16[128,2048]{1,0:T(8,128)(2,1)S(1)} collective-permute-done((bf16[128,2048]{1,0:T(8,128)(2,1)S(1)}, bf16[128,2048]{1,0:T(8,128)(2,1)S(1)}, u32[]{:S(2)}, u32[]{:S(2)}) %collective-permute-start.40) | collective-permute-done | bytes 524320 | tf_op jit(solution)/shard_map/ppermute | solution.py:424
  158.9 9.5 %collective-permute-done.41.s2 = bf16[128,2048]{1,0:T(8,128)(2,1)S(1)} collective-permute-done((bf16[128,2048]{1,0:T(8,128)(2,1)S(1)}, bf16[128,2048]{1,0:T(8,128)(2,1)S(1)}, u32[]{:S(2)}, u32[]{:S(2)}) %collective-permute-start.41) | collective-permute-done | bytes 524320 | tf_op jit(solution)/shard_map/ppermute | solution.py:424
  173.7 1.8 %mixed.1 = bf16[64,4096]{1,0:T(8,128)(2,1)} custom-call(s32[4]{0:T(128)S(1)} %pad_add_fusion.at, bf16[64,2048]{1,0:T(8,128)(2,1)S(1)} %get-tuple-element.53.keep, bf16[64,2048]{1,0:T(8,128)(2,1)S(1)} %collective-permute-done.43.got), custom_call_target="tpu_custom_call" | custom-call | tf_op jit(solution)/shard_map/mixed/pallas_call | solution.py:368
  (148 shorter events, 51.5 us)
Async XLA Ops:
  5.8 8.9 %collective-permute-start = (bf16[112,512]{1,0:T(8,128)(2,1)S(1)}, bf16[112,512]{1,0:T(8,128)(2,1)S(1)}, u32[]{:S(2)}, u32[]{:S(2)}) collective-permute-start(bf16[112,512]{1,0:T(8,128)(2,1)S(1)} %get-tuple-element.30), channel_id=1, source_target_pairs={{0,0},{1,16},{8,8},{9,24},{16,1},{17,17},{24,9},{25,25},{2,2},{3,1... | collective-permute-start | bytes 344072 | tf_op jit(solution)/shard_map/ppermute | solution.py:380
  18.9 8.1 %collective-permute-start.8 = (bf16[144,512]{1,0:T(8,128)(2,1)S(1)}, bf16[144,512]{1,0:T(8,128)(2,1)S(1)}, u32[]{:S(2)}, u32[]{:S(2)}) collective-permute-start(bf16[144,512]{1,0:T(8,128)(2,1)S(1)} %constant_dynamic-update-slice_fusion.refs_0_), channel_id=1, source_target_pairs={{0,32},{32,64},{64,96},{96,128},{128,160},{160,192},{192,224},{224... | collective-permute-start | bytes 442376 | tf_op jit(solution)/shard_map/ppermute | solution.py:58
  20.5 6.5 %collective-permute-start.5 = (bf16[144,512]{1,0:T(8,128)(2,1)S(1)}, bf16[144,512]{1,0:T(8,128)(2,1)S(1)}, u32[]{:S(2)}, u32[]{:S(2)}) collective-permute-start(bf16[144,512]{1,0:T(8,128)(2,1)S(1)} %constant_dynamic-update-slice_fusion.refs_0_), channel_id=1, source_target_pairs={{0,224},{32,0},{64,32},{96,64},{128,96},{160,128},{192,160},{224,1... | collective-permute-start | bytes 442376 | tf_op jit(solution)/shard_map/ppermute | solution.py:59
  45.1 24.8 %collective-permute-start.17 = (bf16[512,512]{1,0:T(8,128)(2,1)S(1)}, bf16[512,512]{1,0:T(8,128)(2,1)S(1)}, u32[]{:S(2)}, u32[]{:S(2)}) collective-permute-start(bf16[512,512]{1,0:T(8,128)(2,1)S(1)} %split_kv.1.refs_4_), channel_id=1, source_target_pairs={{0,2},{2,4},{4,6},{6,0},{1,3},{3,5},{5,7},{7,1},{8,10},{10,12},{12... | collective-permute-start | bytes 1572872 | tf_op jit(solution)/shard_map/ppermute | solution.py:46
  46.4 24.6 %collective-permute-start.19 = (bf16[512,512]{1,0:T(8,128)(2,1)S(1)}, bf16[512,512]{1,0:T(8,128)(2,1)S(1)}, u32[]{:S(2)}, u32[]{:S(2)}) collective-permute-start(bf16[512,512]{1,0:T(8,128)(2,1)S(1)} %split_kv.1.refs_4_), channel_id=1, source_target_pairs={{0,6},{2,0},{4,2},{6,4},{1,7},{3,1},{5,3},{7,5},{8,14},{10,8},{12,... | collective-permute-start | bytes 1572872 | tf_op jit(solution)/shard_map/ppermute | solution.py:47
  47.8 13.9 %collective-permute-start.29 = (bf16[64,512]{1,0:T(8,128)(2,1)S(1)}, bf16[64,512]{1,0:T(8,128)(2,1)}, u32[]{:S(2)}, u32[]{:S(2)}) collective-permute-start(bf16[64,512]{1,0:T(8,128)(2,1)S(1)} %pad_maximum_fusion), channel_id=1, source_target_pairs={{0,2},{2,4},{4,6},{6,0},{1,3},{3,5},{5,7},{7,1},{8,10},{10,12},{12... | collective-permute-start | bytes 196616 | tf_op jit(solution)/shard_map/ppermute | solution.py:41
  50.1 27.9 %collective-permute-start.1 = (bf16[4,128,512]{2,1,0:T(8,128)(2,1)S(1)}, bf16[4,128,512]{2,1,0:T(8,128)(2,1)S(1)}, u32[]{:S(2)}, u32[]{:S(2)}) collective-permute-start(bf16[4,128,512]{2,1,0:T(8,128)(2,1)S(1)} %norm.1.refs_0_), channel_id=1, source_target_pairs={{0,8},{8,16},{16,24},{24,0},{1,9},{9,17},{17,25},{25,1},{2,10},{10... | collective-permute-start | bytes 1572872 | tf_op jit(solution)/shard_map/ppermute | solution.py:41
  51.7 26.2 %collective-permute-start.2 = (bf16[4,128,512]{2,1,0:T(8,128)(2,1)S(1)}, bf16[4,128,512]{2,1,0:T(8,128)(2,1)S(1)}, u32[]{:S(2)}, u32[]{:S(2)}) collective-permute-start(bf16[4,128,512]{2,1,0:T(8,128)(2,1)S(1)} %norm.1.refs_0_), channel_id=1, source_target_pairs={{0,16},{8,24},{16,0},{24,8},{1,17},{9,25},{17,1},{25,9},{2,18},{10... | collective-permute-start | bytes 1572872 | tf_op jit(solution)/shard_map/ppermute | solution.py:41
  61.7 7.6 %collective-permute-start.30 = (bf16[64,512]{1,0:T(8,128)(2,1)S(1)}, bf16[64,512]{1,0:T(8,128)(2,1)S(1)}, u32[]{:S(2)}, u32[]{:S(2)}) collective-permute-start(bf16[64,512]{1,0:T(8,128)(2,1)S(1)} %pad_maximum_fusion), channel_id=1, source_target_pairs={{0,4},{2,6},{4,0},{6,2},{1,5},{3,7},{5,1},{7,3},{8,12},{10,14},{12... | collective-permute-start | bytes 196616 | tf_op jit(solution)/shard_map/ppermute | solution.py:41
  69.3 14.2 %collective-permute-start.12 = (bf16[512,512]{1,0:T(8,128)(2,1)S(1)}, bf16[512,512]{1,0:T(8,128)(2,1)S(1)}, u32[]{:S(2)}, u32[]{:S(2)}) collective-permute-start(bf16[512,512]{1,0:T(8,128)(2,1)S(1)} %get-tuple-element.32.refs_4_), channel_id=1, source_target_pairs={{0,2},{2,4},{4,6},{6,0},{1,3},{3,5},{5,7},{7,1},{8,10},{10,12},{12... | collective-permute-start | bytes 1572872 | tf_op jit(solution)/shard_map/ppermute | solution.py:46
  70.0 14.5 %collective-permute-start.3 = (bf16[4,128,512]{2,1,0:T(8,128)(2,1)S(1)}, bf16[4,128,512]{2,1,0:T(8,128)(2,1)S(1)}, u32[]{:S(2)}, u32[]{:S(2)}) collective-permute-start(bf16[4,128,512]{2,1,0:T(8,128)(2,1)S(1)} %norm.1.refs_0_), channel_id=1, source_target_pairs={{0,24},{8,0},{16,8},{24,16},{1,25},{9,1},{17,9},{25,17},{2,26},{10... | collective-permute-start | bytes 1572872 | tf_op jit(solution)/shard_map/ppermute | solution.py:41
  74.6 23.6 %collective-permute-start.14 = (bf16[512,512]{1,0:T(8,128)(2,1)S(1)}, bf16[512,512]{1,0:T(8,128)(2,1)S(1)}, u32[]{:S(2)}, u32[]{:S(2)}) collective-permute-start(bf16[512,512]{1,0:T(8,128)(2,1)S(1)} %get-tuple-element.32.refs_4_), channel_id=1, source_target_pairs={{0,6},{2,0},{4,2},{6,4},{1,7},{3,1},{5,3},{7,5},{8,14},{10,8},{12,... | collective-permute-start | bytes 1572872 | tf_op jit(solution)/shard_map/ppermute | solution.py:47
  77.9 10.3 %collective-permute-start.18 = (bf16[256,512]{1,0:T(8,128)(2,1)S(1)}, bf16[256,512]{1,0:T(8,128)(2,1)S(1)}, u32[]{:S(2)}, u32[]{:S(2)}) collective-permute-start(bf16[256,512]{1,0:T(8,128)(2,1)S(1)} %slice.88), channel_id=1, source_target_pairs={{0,2},{2,4},{4,6},{6,0},{1,3},{3,5},{5,7},{7,1},{8,10},{10,12},{12... | collective-permute-start | bytes 786440 | tf_op jit(solution)/shard_map/ppermute | solution.py:48
  77.9 12.6 %collective-permute-start.20 = (bf16[256,512]{1,0:T(8,128)(2,1)S(1)}, bf16[256,512]{1,0:T(8,128)(2,1)S(1)}, u32[]{:S(2)}, u32[]{:S(2)}) collective-permute-start(bf16[256,512]{1,0:T(8,128)(2,1)S(1)} %slice.89), channel_id=1, source_target_pairs={{0,6},{2,0},{4,2},{6,4},{1,7},{3,1},{5,3},{7,5},{8,14},{10,8},{12,... | collective-permute-start | bytes 786440 | tf_op jit(solution)/shard_map/ppermute | solution.py:49
  83.5 14.8 %collective-permute-start.32 = (bf16[256,512]{1,0:T(8,128)(2,1)S(1)}, bf16[256,512]{1,0:T(8,128)(2,1)S(1)}, u32[]{:S(2)}, u32[]{:S(2)}) collective-permute-start(bf16[256,512]{1,0:T(8,128)(2,1)S(1)} %constant_dynamic-update-slice_fusion.2.refs_0_), channel_id=1, source_target_pairs={{0,224},{32,0},{64,32},{96,64},{128,96},{160,128},{192,160},{224,1... | collective-permute-start | bytes 786440 | tf_op jit(solution)/shard_map/ppermute | solution.py:59
  84.5 17.3 %collective-permute-start.35 = (bf16[256,512]{1,0:T(8,128)(2,1)S(1)}, bf16[256,512]{1,0:T(8,128)(2,1)S(1)}, u32[]{:S(2)}, u32[]{:S(2)}) collective-permute-start(bf16[256,512]{1,0:T(8,128)(2,1)S(1)} %constant_dynamic-update-slice_fusion.2.refs_0_), channel_id=1, source_target_pairs={{0,32},{32,64},{64,96},{96,128},{128,160},{160,192},{192,224},{224... | collective-permute-start | bytes 786440 | tf_op jit(solution)/shard_map/ppermute | solution.py:58
  88.2 15.1 %collective-permute-start.13 = (bf16[256,512]{1,0:T(8,128)(2,1)S(1)}, bf16[256,512]{1,0:T(8,128)(2,1)S(1)}, u32[]{:S(2)}, u32[]{:S(2)}) collective-permute-start(bf16[256,512]{1,0:T(8,128)(2,1)S(1)} %slice.86), channel_id=1, source_target_pairs={{0,2},{2,4},{4,6},{6,0},{1,3},{3,5},{5,7},{7,1},{8,10},{10,12},{12... | collective-permute-start | bytes 786440 | tf_op jit(solution)/shard_map/ppermute | solution.py:48
  92.3 18.1 %collective-permute-start.21 = (bf16[512,384]{1,0:T(8,128)(2,1)S(1)}, bf16[512,384]{1,0:T(8,128)(2,1)S(1)}, u32[]{:S(2)}, u32[]{:S(2)}) collective-permute-start(bf16[512,384]{1,0:T(8,128)(2,1)S(1)} %get-tuple-element.37), channel_id=1, source_target_pairs={{0,1},{1,0},{2,3},{3,2},{4,5},{5,4},{6,7},{7,6},{8,9},{9,8},{10,11... | collective-permute-start | bytes 1179656 | tf_op jit(solution)/shard_map/ppermute | solution.py:37
  98.3 22.6 %collective-permute-start.33 = (bf16[256,512]{1,0:T(8,128)(2,1)S(1)}, bf16[256,512]{1,0:T(8,128)(2,1)S(1)}, u32[]{:S(2)}, u32[]{:S(2)}) collective-permute-start(bf16[256,512]{1,0:T(8,128)(2,1)S(1)} %collective-permute-done.32.refs_1_), channel_id=1, source_target_pairs={{0,224},{32,0},{64,32},{96,64},{128,96},{160,128},{192,160},{224,1... | collective-permute-start | bytes 786440 | tf_op jit(solution)/shard_map/ppermute | solution.py:59
  98.3 9.1 %collective-permute-start.15 = (bf16[256,512]{1,0:T(8,128)(2,1)S(1)}, bf16[256,512]{1,0:T(8,128)(2,1)S(1)}, u32[]{:S(2)}, u32[]{:S(2)}) collective-permute-start(bf16[256,512]{1,0:T(8,128)(2,1)S(1)} %slice.87), channel_id=1, source_target_pairs={{0,6},{2,0},{4,2},{6,4},{1,7},{3,1},{5,3},{7,5},{8,14},{10,8},{12,... | collective-permute-start | bytes 786440 | tf_op jit(solution)/shard_map/ppermute | solution.py:49
  101.8 20.4 %collective-permute-start.36 = (bf16[256,512]{1,0:T(8,128)(2,1)S(1)}, bf16[256,512]{1,0:T(8,128)(2,1)S(1)}, u32[]{:S(2)}, u32[]{:S(2)}) collective-permute-start(bf16[256,512]{1,0:T(8,128)(2,1)S(1)} %collective-permute-done.35.refs_6_), channel_id=1, source_target_pairs={{0,32},{32,64},{64,96},{96,128},{128,160},{160,192},{192,224},{224... | collective-permute-start | bytes 786440 | tf_op jit(solution)/shard_map/ppermute | solution.py:58
  103.3 7.1 %collective-permute-start.22 = (f32[128,128]{1,0:T(8,128)S(1)}, f32[128,128]{1,0:T(8,128)S(1)}, u32[]{:S(2)}, u32[]{:S(2)}) collective-permute-start(f32[128,128]{1,0:T(8,128)S(1)} %get-tuple-element.39), channel_id=1, source_target_pairs={{0,1},{1,0},{2,3},{3,2},{4,5},{5,4},{6,7},{7,6},{8,9},{9,8},{10,11... | collective-permute-start | bytes 196616 | tf_op jit(solution)/shard_map/ppermute | solution.py:37
  109.2 22.9 %collective-permute-start.16 = (bf16[512,512]{1,0:T(8,128)(2,1)S(1)}, bf16[512,512]{1,0:T(8,128)(2,1)S(1)}, u32[]{:S(2)}, u32[]{:S(2)}) collective-permute-start(bf16[512,512]{1,0:T(8,128)(2,1)S(1)} %get-tuple-element.34), channel_id=1, source_target_pairs={{0,1},{1,0},{2,3},{3,2},{4,5},{5,4},{6,7},{7,6},{8,9},{9,8},{10,11... | collective-permute-start | bytes 1572872 | tf_op jit(solution)/shard_map/ppermute | solution.py:37
  111.4 10.9 %collective-permute-start.26 = (bf16[256,128]{1,0:T(8,128)(2,1)S(1)}, bf16[256,128]{1,0:T(8,128)(2,1)S(1)}, u32[]{:S(2)}, u32[]{:S(2)}) collective-permute-start(bf16[256,128]{1,0:T(8,128)(2,1)S(1)} %get-tuple-element.46), channel_id=1, source_target_pairs={{0,96},{32,128},{64,160},{96,192},{128,224},{1,97},{33,129},{65,16... | collective-permute-start | bytes 196616 | tf_op jit(solution)/shard_map/ppermute | solution.py:411
  114.8 8.9 %collective-permute-start.25 = (bf16[256,128]{1,0:T(8,128)(2,1)S(1)}, bf16[256,128]{1,0:T(8,128)(2,1)S(1)}, u32[]{:S(2)}, u32[]{:S(2)}) collective-permute-start(bf16[256,128]{1,0:T(8,128)(2,1)S(1)} %get-tuple-element.46), channel_id=1, source_target_pairs={{0,64},{32,96},{64,128},{96,160},{128,192},{160,224},{1,65},{33,97... | collective-permute-start | bytes 196616 | tf_op jit(solution)/shard_map/ppermute | solution.py:411
  122.2 13.6 %collective-permute-start.34 = (bf16[256,512]{1,0:T(8,128)(2,1)S(1)}, bf16[256,512]{1,0:T(8,128)(2,1)S(1)}, u32[]{:S(2)}, u32[]{:S(2)}) collective-permute-start(bf16[256,512]{1,0:T(8,128)(2,1)S(1)} %collective-permute-done.33.refs_2_), channel_id=1, source_target_pairs={{0,224},{32,0},{64,32},{96,64},{128,96},{160,128},{192,160},{224,1... | collective-permute-start | bytes 786440 | tf_op jit(solution)/shard_map/ppermute | solution.py:59
  122.3 13.4 %collective-permute-start.37 = (bf16[256,512]{1,0:T(8,128)(2,1)S(1)}, bf16[256,512]{1,0:T(8,128)(2,1)S(1)}, u32[]{:S(2)}, u32[]{:S(2)}) collective-permute-start(bf16[256,512]{1,0:T(8,128)(2,1)S(1)} %collective-permute-done.36.refs_5_), channel_id=1, source_target_pairs={{0,32},{32,64},{64,96},{96,128},{128,160},{160,192},{192,224},{224... | collective-permute-start | bytes 786440 | tf_op jit(solution)/shard_map/ppermute | solution.py:58
  123.8 9.6 %collective-permute-start.27 = (bf16[256,128]{1,0:T(8,128)(2,1)S(1)}, bf16[256,128]{1,0:T(8,128)(2,1)S(1)}, u32[]{:S(2)}, u32[]{:S(2)}) collective-permute-start(bf16[256,128]{1,0:T(8,128)(2,1)S(1)} %get-tuple-element.55), channel_id=1, source_target_pairs={{0,128},{32,160},{64,192},{96,224},{1,129},{33,161},{65,193},{97,2... | collective-permute-start | bytes 196616 | tf_op jit(solution)/shard_map/ppermute | solution.py:413
  134.2 7.8 %collective-permute-start.28 = (f32[512,128]{1,0:T(8,128)S(1)}, f32[512,128]{1,0:T(8,128)S(1)}, u32[]{:S(2)}, u32[]{:S(2)}) collective-permute-start(f32[512,128]{1,0:T(8,128)S(1)} %across.1.ret), channel_id=1, source_target_pairs={{0,1},{1,0},{2,3},{3,2},{4,5},{5,4},{6,7},{7,6},{8,9},{9,8},{10,11... | collective-permute-start | bytes 786440 | tf_op jit(solution)/shard_map/ppermute | solution.py:37
  144.2 14.8 %collective-permute-start.40 = (bf16[128,2048]{1,0:T(8,128)(2,1)S(1)}, bf16[128,2048]{1,0:T(8,128)(2,1)S(1)}, u32[]{:S(2)}, u32[]{:S(2)}) collective-permute-start(bf16[128,2048]{1,0:T(8,128)(2,1)S(1)} %get-tuple-element.50), channel_id=1, source_target_pairs={{0,8},{8,16},{16,24},{24,0},{1,9},{9,17},{17,25},{25,1},{2,10},{10... | collective-permute-start | bytes 1572872 | tf_op jit(solution)/shard_map/ppermute | solution.py:424
  145.2 23.2 %collective-permute-start.41 = (bf16[128,2048]{1,0:T(8,128)(2,1)S(1)}, bf16[128,2048]{1,0:T(8,128)(2,1)S(1)}, u32[]{:S(2)}, u32[]{:S(2)}) collective-permute-start(bf16[128,2048]{1,0:T(8,128)(2,1)S(1)} %get-tuple-element.51), channel_id=1, source_target_pairs={{0,16},{8,24},{16,0},{24,8},{1,17},{9,25},{17,1},{25,9},{2,18},{10... | collective-permute-start | bytes 1572872 | tf_op jit(solution)/shard_map/ppermute | solution.py:424
  145.8 24.2 %collective-permute-start.42 = (bf16[128,2048]{1,0:T(8,128)(2,1)S(1)}, bf16[128,2048]{1,0:T(8,128)(2,1)S(1)}, u32[]{:S(2)}, u32[]{:S(2)}) collective-permute-start(bf16[128,2048]{1,0:T(8,128)(2,1)S(1)} %get-tuple-element.52), channel_id=1, source_target_pairs={{0,24},{8,0},{16,8},{24,16},{1,25},{9,1},{17,9},{25,17},{2,26},{10... | collective-permute-start | bytes 1572872 | tf_op jit(solution)/shard_map/ppermute | solution.py:424
  (38 other events, 148.2 us)

commit v2 on v1

--- a/solution.py
+++ b/solution.py
@@ -39,15 +39,6 @@
 
 def direct(a, axis, n):
     return [a] + [lax.ppermute(a, axis, ring(n, k)) for k in range(1, n)]
-
-
-def x_ring(a):
-    n = a.shape[0] // 2
-    one = lax.ppermute(a, "x", ring(NX, 1))
-    three = lax.ppermute(a, "x", ring(NX, -1))
-    top = lax.ppermute(one[:n], "x", ring(NX, 1))
-    low = lax.ppermute(three[n:], "x", ring(NX, -1))
-    return [a, one, top, low, three]
 
 
 def z_ring(a, halves):
@@ -77,8 +68,15 @@
 ROWS = 112
 
 
-def pack_body(at, decay, pool, query, key, value, state, pback, rback, s0, s1):
+def pack_body(at, decay, *refs):
     y = at[1]
+    sources, (s0, s1), held, sem = refs[:7], refs[7:9], refs[9:16], refs[16]
+    copies = [pltpu.make_async_copy(a, b, sem.at[i]) for i, (a, b) in enumerate(zip(sources, held))]
+    for cp in copies:
+        cp.start()
+    for cp in copies:
+        cp.wait()
+    pool, query, key, value, state, pback, rback = held
     for k, out in enumerate((s0, s1)):
         p = (y + k) % 2
         at_head = pl.ds(pl.multiple_of(p * HEAD, HEAD), HEAD)
@@ -99,11 +97,52 @@
         out[96:112, 256:] = jnp.concatenate([lo, jnp.concatenate([d3, d3], axis=1)], axis=0)
 
 
-def pack(at, *args):
-    return local(
-        pack_body, in_specs=[SM, SM] + [VM] * 7, out_specs=[VM] * 2,
-        out_shape=[jax.ShapeDtypeStruct((ROWS, 512), bf16)] * 2, name="pack",
-    )(at, *args)
+def pack(at, decay, *args):
+    return pl.pallas_call(
+        pack_body, in_specs=[SM, SM] + [pl.BlockSpec(memory_space=pltpu.HBM)] * 7, out_specs=[VM] * 2,
+        out_shape=[jax.ShapeDtypeStruct((ROWS, 512), bf16)] * 2,
+        scratch_shapes=[pltpu.VMEM(a.shape, a.dtype) for a in args] + [pltpu.SemaphoreType.DMA((7,))], name="pack",
+    )(at, decay, *args)
+
+
+def merge_body(at, r0, r1, weights, pq_rows, rates):
+    def place(a, b):
+        for i, r in enumerate((a, b)):
+            weights[i * 32:i * 32 + 32, :] = r[0:32, :]
+            weights[64 + i * 32:96 + i * 32, :] = r[64:96, :]
+            pq_rows[i * 32:i * 32 + 32, :] = r[32:64, :]
+        weights[128:144, :] = jnp.concatenate([a[96:112, :].astype(f32)[:8], b[96:112, :].astype(f32)[:8]], axis=0).astype(bf16)
+
+    @pl.when(at[1] % 2 == 0)
+    def _():
+        place(r0, r1)
+
+    @pl.when(at[1] % 2 == 1)
+    def _():
+        place(r1, r0)
+
+    three = r0[96:112, :].astype(f32)[8:]
+    rate = (three[:, :128] + three[:, 128:256]) + three[:, 256:384]
+    rates[0:8, :] = rate
+    rates[8:16, :] = jnp.exp(-SPAN * rate)
+
+
+def merge(at, r0, r1):
+    return local(
+        merge_body, in_specs=[SM] + [VM] * 2, out_specs=[VM] * 3,
+        out_shape=[jax.ShapeDtypeStruct((144, 512), bf16), jax.ShapeDtypeStruct((64, 512), bf16),
+                   jax.ShapeDtypeStruct((16, HALF), f32)],
+        name="merge",
+    )(at, r0, r1)
+
+
+def join_body(a, b, c, d, out):
+    for i, r in enumerate((a, b, c, d)):
+        out[i * 64:i * 64 + 64, :] = r[...]
+
+
+def join(parts):
+    return local(join_body, in_specs=[VM] * 4, out_specs=VM, out_shape=jax.ShapeDtypeStruct((256, 512), bf16), name="join")(*parts)
 
 
 def norm_body(at, tok, gain, out, full):
@@ -130,44 +169,31 @@
     )(at, tok, gain)
 
 
-def split_kv_body(*refs):
+def split_body(at, *refs):
+    z, c = at[0], at[3]
+    ins, (kv, out_w, keep, give) = refs[:NZ], refs[NZ:]
     for kz in range(NZ):
-        refs[NZ][kz * 64:kz * 64 + 64, :] = refs[kz][0:64, :]
-
-
-def split_kv(chunks):
-    return local(
-        split_kv_body, in_specs=[VM] * NZ, out_specs=VM,
-        out_shape=jax.ShapeDtypeStruct((512, 512), bf16), name="split_kv",
-    )(*chunks)
-
-
-def split_pq_body(at, *refs):
-    z, c = at[0], at[3]
-    ins, (pq, keep, give) = refs[:NZ], refs[NZ:]
-    for kz in range(NZ):
-        pq[kz * 64:kz * 64 + 64, :] = ins[kz][64:128, :]
+        kv[kz * 64:kz * 64 + 64, :] = ins[kz][0:64, :]
+        out_w[kz * 64:kz * 64 + 64, :] = ins[kz][64:128, :]
         for out, half in ((keep, c), (give, 1 - c)):
             hi = ins[kz][128:144, pl.ds(pl.multiple_of(half * HALF, HALF), HALF)].astype(f32)
             lo = ins[kz][128:144, pl.ds(pl.multiple_of(HEAD + half * HALF, HALF), HALF)].astype(f32)
             out[pl.ds(pl.multiple_of(((z + kz) % NZ) * 16, 16), 16), :] = hi + lo
 
 
-def split_pq(at, chunks):
-    return local(
-        split_pq_body, in_specs=[SM] + [VM] * NZ, out_specs=[VM] * 3,
-        out_shape=[jax.ShapeDtypeStruct((512, 512), bf16)] + [jax.ShapeDtypeStruct((HALF, HALF), f32)] * 2,
-        name="split_pq",
+def split(at, chunks):
+    return local(
+        split_body, in_specs=[SM] + [VM] * NZ, out_specs=[VM] * 4,
+        out_shape=[jax.ShapeDtypeStruct((512, 512), bf16)] * 2 + [jax.ShapeDtypeStruct((HALF, HALF), f32)] * 2,
+        name="split",
     )(at, *chunks)
 
 
-def multiply(toks, ws):
-    w0, w1, w2a, w2b, w3 = ws
+def multiply(toks, pick):
     acc = None
     for kx in range(NX):
-        w = jnp.concatenate([w2a[...], w2b[...]], axis=0) if kx == 2 else (w0, w1, None, w3)[kx][...]
         rows = jnp.concatenate([t[kx] for t in toks], axis=0)
-        r = jnp.dot(rows, w, preferred_element_type=f32)
+        r = jnp.dot(rows, pick(kx), preferred_element_type=f32)
         acc = r if acc is None else acc + r
     return acc
 
@@ -178,8 +204,8 @@
 
 def kv_body(at, *refs):
     y, c = at[1], at[3]
-    toks, ws, (kpart, vkeep, send) = refs[:4], refs[4:9], refs[9:]
-    acc = multiply(toks, ws)
+    toks, ws, (kpart, vkeep, send) = refs[:4], refs[4:8], refs[8:]
+    acc = multiply(toks, lambda kx: ws[kx][...])
     for k in range(NY):
         r = acc[k * HALF:(k + 1) * HALF]
         rows = span_rows(y, k)
@@ -191,7 +217,7 @@
 
 def project_kv(at, toks, ws):
     return local(
-        kv_body, in_specs=[SM] + [VM] * 9, out_specs=[VM] * 3,
+        kv_body, in_specs=[SM] + [VM] * 8, out_specs=[VM] * 3,
         out_shape=[jax.ShapeDtypeStruct((SPAN, HEAD), f32), jax.ShapeDtypeStruct((SPAN, HALF), f32),
                    jax.ShapeDtypeStruct((SPAN, 384), bf16)],
         name="project_kv",
@@ -199,8 +225,13 @@
 
 
 def pq_body(at, *refs):
-    toks, ws, (own, send) = refs[:4], refs[4:9], refs[9:]
-    acc = multiply(toks, ws)
+    toks, ws, (own, send, rhs) = refs[:4], refs[4:13], refs[13:]
+    for i, kz in enumerate((0, 1, 2, 3, 5, 6, 7)):
+        for kx in range(NX):
+            rhs[kx, kz * 64:kz * 64 + 64, :] = ws[i][kx * 64:kx * 64 + 64, :]
+    for kx in range(NX):
+        rhs[kx, 256:320, :] = ws[7 + kx // 2][kx % 2 * 64:kx % 2 * 64 + 64, :]
+    acc = multiply(toks, lambda kx: rhs[kx])
     for k in range(NY):
         r = acc[k * HALF:(k + 1) * HALF]
         rows = span_rows(at[1], k)
@@ -210,9 +241,9 @@
 
 def project_pq(at, toks, ws):
     return local(
-        pq_body, in_specs=[SM] + [VM] * 9, out_specs=[VM] * 2,
+        pq_body, in_specs=[SM] + [VM] * 13, out_specs=[VM] * 2,
         out_shape=[jax.ShapeDtypeStruct((SPAN, 512), f32), jax.ShapeDtypeStruct((SPAN, 512), bf16)],
-        name="project_pq",
+        scratch_shapes=[pltpu.VMEM((NX, 512, 512), bf16)], name="project_pq",
     )(at, *toks, *ws)
 
 
@@ -221,7 +252,7 @@
     return jnp.concatenate([a * cosine - b * sine, a * sine + b * cosine], axis=1)
 
 
-def state_body(at, rates, kpart, vkeep, got, cosine, sine, keep, other, rk, val, state, sent, start):
+def state_body(at, rates, kpart, vkeep, got, cosine, sine, keep, other, rk, val, sent, start):
     z, c = at[0], at[3]
     for zs in range(NZ):
         start[pl.ds(pl.multiple_of(zs * 32 + c * 16, 16), 16), :] = keep[zs * 16:zs * 16 + 16, :]
@@ -236,24 +267,32 @@
     faded = (turned * jnp.concatenate([fade, fade], axis=1)).astype(bf16)
     s = lax.dot_general(faded, value, (((0,), (0,)), ((), ())), preferred_element_type=f32)
     s = s + jnp.where(z == 0, rates[8:9, :], 0.0) * start[...]
-    state[...] = s
     sent[...] = s.astype(bf16)
 
 
 def span_state(at, rates, *args):
     return local(
-        state_body, in_specs=[SM] + [VM] * 8, out_specs=[VM] * 5,
+        state_body, in_specs=[SM] + [VM] * 8, out_specs=[VM] * 4,
         out_shape=[jax.ShapeDtypeStruct((SPAN, HEAD), bf16), jax.ShapeDtypeStruct((SPAN, HALF), bf16),
-                   jax.ShapeDtypeStruct((HEAD, HALF), f32), jax.ShapeDtypeStruct((HEAD, HALF), bf16),
-                   jax.ShapeDtypeStruct((HEAD, HALF), f32)],
+                   jax.ShapeDtypeStruct((HEAD, HALF), bf16), jax.ShapeDtypeStruct((HEAD, HALF), f32)],
         name="span_state",
     )(at, rates, *args)
 
 
-def inside_body(rates, own, got, cosine, sine, rk, val, pool_in, tail, inside, faded):
+def pool_sum_body(own, got, pool_in, tail):
     p = (own[:, :256] + got[:, :256].astype(f32)).astype(bf16)
     pool_in[...] = p
     tail[...] = p[SPAN - HALO:]
+
+
+def pool_sum(own, got):
+    return local(
+        pool_sum_body, in_specs=[VM] * 2, out_specs=[VM] * 2,
+        out_shape=[jax.ShapeDtypeStruct((SPAN, HEAD), bf16), jax.ShapeDtypeStruct((HALO, HEAD), bf16)], name="pool_sum",
+    )(own, got)
+
+
+def inside_body(rates, own, got, cosine, sine, rk, val, inside, faded):
     query = (own[:, 256:] + got[:, 256:].astype(f32)).astype(bf16).astype(f32)
     rq = turn(query, cosine[...], sine[...])
     within = lax.broadcasted_iota(jnp.int32, (SPAN, HALF), 0).astype(f32)
@@ -271,25 +310,28 @@
 
 def inside_span(rates, *args):
     return local(
-        inside_body, in_specs=[VM] * 7, out_specs=[VM] * 4,
-        out_shape=[jax.ShapeDtypeStruct((SPAN, HEAD), bf16), jax.ShapeDtypeStruct((HALO, HEAD), bf16),
-                   jax.ShapeDtypeStruct((SPAN, HALF), f32),
+        inside_body, in_specs=[VM] * 7, out_specs=[VM] * 2,
+        out_shape=[jax.ShapeDtypeStruct((SPAN, HALF), f32),
                    jax.ShapeDtypeStruct((SPAN, HEAD), bf16)],
         name="inside",
     )(rates, *args)
 
 
-def across_body(at, rates, inside, faded, near, far, start, ret):
+def across_body(at, rates, inside, faded, start, *refs):
+    earlier, ret = refs[:NZ - 1], refs[NZ - 1]
     d = rates[8:9, :]
-    carried = near[...] + d * d * d * far[...].astype(f32) + jnp.where(at[0] == 0, 1.0, 0.0) * start[...]
+    carried = earlier[NZ - 2][...].astype(f32)
+    for r in reversed(earlier[:NZ - 2]):
+        carried = r[...].astype(f32) + d * carried
+    carried = carried + jnp.where(at[0] == 0, 1.0, 0.0) * start[...]
     ret[...] = inside[...] + jnp.dot(faded[...], carried.astype(bf16), preferred_element_type=f32)
 
 
-def across_spans(at, rates, *args):
-    return local(
-        across_body, in_specs=[SM] + [VM] * 6, out_specs=VM,
+def across_spans(at, rates, inside, faded, start, earlier):
+    return local(
+        across_body, in_specs=[SM] + [VM] * (NZ + 3), out_specs=VM,
         out_shape=jax.ShapeDtypeStruct((SPAN, HALF), f32), name="across",
-    )(at, rates, *args)
+    )(at, rates, inside, faded, start, *earlier)
 
 
 def pool_body(at, pool_in, before, group_map, scale, out):
@@ -315,24 +357,23 @@
 
 def back_body(at, pool, ret, other, *refs):
     y, c = at[1], at[3]
-    ws, outs, act, res = refs[:9], refs[9:13], refs[13], refs[14]
+    ws, outs, act, res = refs[:4], refs[4:8], refs[8], refs[9]
     r, o = ret[...], other[...]
     square = jnp.sum(r * r, axis=-1, keepdims=True) + jnp.sum(o * o, axis=-1, keepdims=True)
     factor = lax.rsqrt(square * (1.0 / HEAD) + eps)
     act[:, :256] = pool[...]
     act[:, pl.ds(pl.multiple_of(HEAD + c * HALF, HALF), HALF)] = (r * factor).astype(bf16)
     act[:, pl.ds(pl.multiple_of(HEAD + (1 - c) * HALF, HALF), HALF)] = (o * factor).astype(bf16)
-    for i, kz in enumerate((0, 1, 2, 3, 5, 6, 7, 4)):
-        w = ws[i][...] if kz != 4 else jnp.concatenate([ws[7][...], ws[8][...]], axis=0)
-        r = lax.dot_general(act[...], w, (((1,), (1,)), ((), ())), preferred_element_type=f32)
-        res[:, kz * 256:kz * 256 + 256] = r.astype(bf16)
+    for kx in range(NX):
+        r = lax.dot_general(act[...], ws[kx][...], (((1,), (1,)), ((), ())), preferred_element_type=f32)
+        res[:, kx * 512:kx * 512 + 512] = r.astype(bf16)
     for k, out in enumerate(outs):
         out[...] = res[pl.ds(pl.multiple_of(((y + k) % NY) * HALF, HALF), HALF), :]
 
 
 def back(at, pool, ret, other, ws):
     return local(
-        back_body, in_specs=[SM] + [VM] * 12, out_specs=[VM] * 4,
+        back_body, in_specs=[SM] + [VM] * 7, out_specs=[VM] * 4,
         out_shape=[jax.ShapeDtypeStruct((HALF, 2048), bf16)] * 4,
         scratch_shapes=[pltpu.VMEM((SPAN, 512), bf16), pltpu.VMEM((SPAN, 2048), bf16)], name="back",
     )(at, pool, ret, other, *ws)
@@ -354,14 +395,16 @@
 
 def mixed_body(at, keep, got, out):
     z, x, c = at[0], at[2], at[3]
-    lane_in = lax.broadcasted_iota(jnp.int32, (256, 256), 0)
-    lane_out = lax.broadcasted_iota(jnp.int32, (256, 256), 1)
-    source = (x + NX - (lane_out % 128) // 32) % NX * 64 + lane_out // 128 * 32 + lane_out % 32
+    lane_in = lax.broadcasted_iota(jnp.int32, (512, 512), 0)
+    lane_out = lax.broadcasted_iota(jnp.int32, (512, 512), 1)
+    source = (x + NX - (lane_out % 128) // 32) % NX * 128 + lane_out // 256 * 64 + (lane_out % 256) // 128 * 32 + lane_out % 32
     order = (lane_in == source).astype(bf16)
-    for kz in range(NZ):
+    for pair in range(NZ // 2):
         for ref, core in ((keep, c), (got, 1 - c)):
-            r = jnp.dot(ref[:, kz * 256:kz * 256 + 256], order, preferred_element_type=f32).astype(bf16)
-            out[:, pl.ds(pl.multiple_of((z + kz) % NZ * 512 + core * 256, 256), 256)] = r
+            rows = jnp.concatenate([ref[:, kx * 512 + pair * 128:kx * 512 + pair * 128 + 128] for kx in range(NX)], axis=1)
+            r = jnp.dot(rows, order, preferred_element_type=f32).astype(bf16)
+            for i in range(2):
+                out[:, pl.ds(pl.multiple_of((z + 2 * pair + i) % NZ * 512 + core * 256, 256), 256)] = r[:, i * 256:i * 256 + 256]
 
 
 def mixed(at, keep, got):
@@ -379,27 +422,22 @@
     s0, s1 = pack(at, decay_rate, pool_proj, query_proj, key_proj, value_proj, start_state[0], pool_back.T, retention_back.T)
     r0 = lax.ppermute(s0, ("y", "c"), to_heads(0))
     r1 = lax.ppermute(s1, ("y", "c"), to_heads(1))
-    even = y % 2 == 0
-    a, b = jnp.where(even, r0, r1), jnp.where(even, r1, r0)
-    shard_in = jnp.concatenate([a[:32], b[:32], a[32:64], b[32:64], a[96:104], b[96:104]], axis=0)
-    shard_out = jnp.concatenate([a[64:96], b[64:96]], axis=0)
-
-    toks = direct(norm(at, tokens[0], norm_gain[None]), "y", NY)
+    shard_in, shard_pq, rates = merge(at, r0, r1)
+
+    toks = [norm(at, tokens[0], norm_gain[None])]
+    for k in (1, 2, 3):
+        toks.append(lax.ppermute(toks[0], "y", ring(NY, k)))
 
 
     in_z = z_ring(shard_in, False)
-    kv_list = x_ring(split_kv(in_z))
-    plane_pq, keep, give = split_pq(at, in_z)
-    pq_list = x_ring(plane_pq)
+    plane_kv, plane_out, keep, give = split(at, in_z)
+    kv_list = direct(plane_kv, "x", NX)
+    out_list = direct(plane_out, "x", NX)
     start_other = swap(give)
 
-    plane_o = jnp.concatenate(direct(shard_out, "x", NX), axis=0)
-    wt = z_ring(plane_o, True)
-
-    three = r0[104:112, :].astype(f32)
-    rate = (three[:, :128] + three[:, 128:256]) + three[:, 256:384]
-    rates = jnp.concatenate([rate, jnp.exp(-SPAN * rate)], axis=0)
-    span_decay = rates[8:9, :]
+    plane_pq = join(direct(shard_pq, "x", NX))
+    pq_list = z_ring(plane_pq, True)
+
     positions = (jnp.arange(SPAN, dtype=jnp.int32) + z * SPAN)
     inv_freq = 1.0 / rope_base ** jnp.linspace(0.0, 1.0, HALF, dtype=f32)
     angles = positions.astype(f32)[:, None] * inv_freq[None, :]
@@ -407,20 +445,19 @@
 
     kpart, vkeep, send = project_kv(at, toks, kv_list)
     got = swap(send)
-    rk, val, state, sent, start = span_state(at, rates, kpart, vkeep, got, cosine, sine, keep, start_other)
-    n1, n2, n3 = (lax.ppermute(sent, "z", line(NZ, k)).astype(f32) for k in (1, 2, 3))
-    near = n1 + span_decay * (n2 + span_decay * n3)
-    far = lax.ppermute((state + span_decay * near).astype(bf16), "z", line(NZ, 4))
+    rk, val, sent, start = span_state(at, rates, kpart, vkeep, got, cosine, sine, keep, start_other)
+    earlier = [lax.ppermute(sent, "z", line(NZ, k)) for k in range(1, NZ)]
 
     own, send = project_pq(at, toks, pq_list)
     got = swap(send)
-    pool_in, tail, inside, faded = inside_span(rates, own, got, cosine, sine, rk, val)
+    pool_in, tail = pool_sum(own, got)
+    inside, faded = inside_span(rates, own, got, cosine, sine, rk, val)
     before = lax.ppermute(tail, "z", line(NZ, 1))
     pool_out = pooling(at, pool_in, before, pool_map, pool_scale[None])
-    ret = across_spans(at, rates, inside, faded, near, far, start)
+    ret = across_spans(at, rates, inside, faded, start, earlier)
     other = swap(ret)
 
-    shares = back(at, pool_out, ret, other, wt)
+    shares = back(at, pool_out, ret, other, out_list)
     arrived = [shares[0]] + [lax.ppermute(shares[k], "y", ring(NY, k)) for k in range(1, NY)]
     keep, give = total(at, arrived)
     got = swap(give)

time: 179 us -> 172 us (0.961); the launches traced: 176 us -> 172 us
  local copies, waits for them, and re-layouts: 15.4 us -> 1.26 us
  starting transfers between devices: 77.9 us -> 86.1 us
  Pallas kernels: 14.8 us -> 19.1 us
    unnamed x57 -> x10, local copies, waits for them, and re-layouts: 14.1 us -> 1.24 us
    ppermute x6 -> x9, waiting for transfers between devices: 11.2 us -> 1.98 us  [direct(): return [a] + [lax.ppermute(a, axis, ring(n, k)) for k in range(1, n)]]
    ppermute x6 -> x9, starting transfers between devices: 5.75 us -> 13.9 us  [direct(): return [a] + [lax.ppermute(a, axis, ring(n, k)) for k in range(1, n)]]
    ppermute x6, starting transfers between devices: 9.37 us -> 16.7 us  [z_ring(): down = lax.ppermute(down, 'z', ring(NZ, -1))]
    ppermute x6, waiting for transfers between devices: 0.02 us -> 6.34 us  [z_ring(): down = lax.ppermute(down, 'z', ring(NZ, -1))]
    ppermute x6, starting transfers between devices: 6.16 us -> 2.13 us  [z_ring(): up = lax.ppermute(up, 'z', ring(NZ, 1))]
    pallas_call x9 -> x11, Pallas kernels: 9.66 us -> 13.6 us  [the longest x1 2.58 us: project_pq(): local(pq_body, in_specs=[SM] + [VM] * 13, out_specs=[VM] * 2, out_shape=[...]
    ppermute x12 -> x10, waiting for transfers between devices: 10.9 us -> 14.7 us  [the longest x3 14.1 us: layer(): toks.append(lax.ppermute(toks[0], 'y', ring(NY, k)))]
  transfers between devices with their start and end apart: 44 -> 45, of which waited for: 19 -> 18; matrix products, arithmetic and copies ran while one was open for 2% -> 1% of each run, Pallas kernels for 5% -> 6%
where the time goes in v2:
time: 172 us
  starting transfers between devices  86.1 us (50%)
  waiting for transfers between devices  63.4 us (37%)
  Pallas kernels  19.1 us (11%)
    ppermute x7, starting transfers between devices, layer(): earlier = [lax.ppermute(sent, 'z', line(NZ, k)) for k in range(1, NZ)]  27.3 us
    ppermute x3, waiting for transfers between devices, layer(): lax.ppermute(shares[k], 'y', ring(NY, k))  22.7 us
    ppermute x6, starting transfers between devices, z_ring(): down = lax.ppermute(down, 'z', ring(NZ, -1))  16.7 us
    ppermute x3, waiting for transfers between devices, layer(): toks.append(lax.ppermute(toks[0], 'y', ring(NY, k)))  14.1 us
    ppermute x9, starting transfers between devices, direct(): return [a] + [lax.ppermute(a, axis, ring(n, k)) for k in range(1, n)]  13.9 us
    ppermute x5, starting transfers between devices, swap(): return lax.ppermute(a, 'c', SWAP)  9.29 us
    ppermute x6, waiting for transfers between devices, z_ring(): down = lax.ppermute(down, 'z', ring(NZ, -1))  6.34 us
    ppermute x1, starting transfers between devices, layer(): r0 = lax.ppermute(s0, ('y', 'c'), to_heads(0))  6.2 us
  transfers between devices with their start and end apart: 45, of which 18 were waited for; matrix products, arithmetic and copies ran while one was open for 1% of the time, Pallas kernels for 6%

profile of v2, /device:TPU:1, one launch (start us, length us, event | category | flops | bytes accessed | tf_op | source)
XLA Modules:
  0.0 171.8 jit_solution(17347375624544748315)
XLA Ops:
  0.6 2.3 %pack.1 = (bf16[112,512]{1,0:T(8,128)(2,1)}, bf16[112,512]{1,0:T(8,128)(2,1)}) custom-call(s32[4]{0:T(128)} %pad_add_fusion.at, f32[2]{0:T(128)} %decay.1, bf16[32,512]{1,0:T(8,128)(2,1)} %refs_0_.1, bf16[32,512]{1,0:T(8,128)(2,1)} %refs_1_.1, bf16[32,512]{1,0:T(8,128)(2,1)} %refs_2_.1, bf16[32,512]{1,0:T(8,128)(2,1)} %refs_3_.1, f32[2,8,256]{2,1,0:T(8,128)} %bitcast.16, ...), custom_call_target="tpu_custom_call" | custom-call | tf_op jit(solution)/shard_map/pack/pallas_call | solution.py:101
  2.9 6.2 %collective-permute-start.3 = (bf16[112,512]{1,0:T(8,128)(2,1)}, bf16[112,512]{1,0:T(8,128)(2,1)S(1)}, u32[]{:S(2)}, u32[]{:S(2)}) collective-permute-start(bf16[112,512]{1,0:T(8,128)(2,1)} %get-tuple-element.33), channel_id=1, source_target_pairs={{0,0},{1,16},{8,8},{9,24},{16,1},{17,17},{24,9},{25,25},{2,2},{3,1... | collective-permute-start | bytes 344072 | tf_op jit(solution)/shard_map/ppermute | solution.py:423
  9.6 3.1 %collective-permute-done.3.r0 = bf16[112,512]{1,0:T(8,128)(2,1)S(1)} collective-permute-done((bf16[112,512]{1,0:T(8,128)(2,1)}, bf16[112,512]{1,0:T(8,128)(2,1)S(1)}, u32[]{:S(2)}, u32[]{:S(2)}) %collective-permute-start.3) | collective-permute-done | bytes 114720 | tf_op jit(solution)/shard_map/ppermute | solution.py:423
  12.8 2.0 %collective-permute-done.4.r1 = bf16[112,512]{1,0:T(8,128)(2,1)S(1)} collective-permute-done((bf16[112,512]{1,0:T(8,128)(2,1)}, bf16[112,512]{1,0:T(8,128)(2,1)S(1)}, u32[]{:S(2)}, u32[]{:S(2)}) %collective-permute-start.4) | collective-permute-done | bytes 114720 | tf_op jit(solution)/shard_map/ppermute | solution.py:424
  16.7 2.5 %collective-permute-start.6 = (bf16[64,512]{1,0:T(8,128)(2,1)S(1)}, bf16[64,512]{1,0:T(8,128)(2,1)S(1)}, u32[]{:S(2)}, u32[]{:S(2)}) collective-permute-start(bf16[64,512]{1,0:T(8,128)(2,1)S(1)} %get-tuple-element.35.a), channel_id=1, source_target_pairs={{0,4},{2,6},{4,0},{6,2},{1,5},{3,7},{5,1},{7,3},{8,12},{10,14},{12... | collective-permute-start | bytes 196616 | tf_op jit(solution)/shard_map/ppermute | solution.py:41
  24.0 4.0 %collective-permute-start.8 = (bf16[256,512]{1,0:T(8,128)(2,1)S(1)}, bf16[256,512]{1,0:T(8,128)(2,1)S(1)}, u32[]{:S(2)}, u32[]{:S(2)}) collective-permute-start(bf16[256,512]{1,0:T(8,128)(2,1)S(1)} %join.1.refs_4_), channel_id=1, source_target_pairs={{0,224},{32,0},{64,32},{96,64},{128,96},{160,128},{192,160},{224,1... | collective-permute-start | bytes 786440 | tf_op jit(solution)/shard_map/ppermute | solution.py:50
  28.0 2.7 %collective-permute-start.18 = (bf16[144,512]{1,0:T(8,128)(2,1)S(1)}, bf16[144,512]{1,0:T(8,128)(2,1)S(1)}, u32[]{:S(2)}, u32[]{:S(2)}) collective-permute-start(bf16[144,512]{1,0:T(8,128)(2,1)S(1)} %get-tuple-element.41.refs_0_), channel_id=1, source_target_pairs={{0,224},{32,0},{64,32},{96,64},{128,96},{160,128},{192,160},{224,1... | collective-permute-start | bytes 442376 | tf_op jit(solution)/shard_map/ppermute | solution.py:50
  30.7 5.0 %collective-permute-done.21.refs_7_ = bf16[144,512]{1,0:T(8,128)(2,1)S(1)} collective-permute-done((bf16[144,512]{1,0:T(8,128)(2,1)S(1)}, bf16[144,512]{1,0:T(8,128)(2,1)S(1)}, u32[]{:S(2)}, u32[]{:S(2)}) %collective-permute-start.21) | collective-permute-done | bytes 147488 | tf_op jit(solution)/shard_map/ppermute | solution.py:49
  40.0 2.8 %collective-permute-start.9 = (bf16[256,512]{1,0:T(8,128)(2,1)S(1)}, bf16[256,512]{1,0:T(8,128)(2,1)S(1)}, u32[]{:S(2)}, u32[]{:S(2)}) collective-permute-start(bf16[256,512]{1,0:T(8,128)(2,1)S(1)} %collective-permute-done.8.refs_5_), channel_id=1, source_target_pairs={{0,224},{32,0},{64,32},{96,64},{128,96},{160,128},{192,160},{224,1... | collective-permute-start | bytes 786440 | tf_op jit(solution)/shard_map/ppermute | solution.py:50
  44.2 6.3 %collective-permute-done.19.refs_2_ = bf16[144,512]{1,0:T(8,128)(2,1)S(1)} collective-permute-done((bf16[144,512]{1,0:T(8,128)(2,1)S(1)}, bf16[144,512]{1,0:T(8,128)(2,1)S(1)}, u32[]{:S(2)}, u32[]{:S(2)}) %collective-permute-start.19) | collective-permute-done | bytes 147488 | tf_op jit(solution)/shard_map/ppermute | solution.py:50
  50.5 3.4 %collective-permute-start.20 = (bf16[144,512]{1,0:T(8,128)(2,1)S(1)}, bf16[144,512]{1,0:T(8,128)(2,1)S(1)}, u32[]{:S(2)}, u32[]{:S(2)}) collective-permute-start(bf16[144,512]{1,0:T(8,128)(2,1)S(1)} %collective-permute-done.19.refs_2_), channel_id=1, source_target_pairs={{0,224},{32,0},{64,32},{96,64},{128,96},{160,128},{192,160},{224,1... | collective-permute-start | bytes 442376 | tf_op jit(solution)/shard_map/ppermute | solution.py:50
  54.3 2.4 %collective-permute-start.10 = (bf16[256,512]{1,0:T(8,128)(2,1)S(1)}, bf16[256,512]{1,0:T(8,128)(2,1)S(1)}, u32[]{:S(2)}, u32[]{:S(2)}) collective-permute-start(bf16[256,512]{1,0:T(8,128)(2,1)S(1)} %collective-permute-done.9.refs_6_), channel_id=1, source_target_pairs={{0,224},{32,0},{64,32},{96,64},{128,96},{160,128},{192,160},{224,1... | collective-permute-start | bytes 786440 | tf_op jit(solution)/shard_map/ppermute | solution.py:50
  56.7 2.4 %collective-permute-done.24.refs_4_ = bf16[144,512]{1,0:T(8,128)(2,1)S(1)} collective-permute-done((bf16[144,512]{1,0:T(8,128)(2,1)S(1)}, bf16[144,512]{1,0:T(8,128)(2,1)S(1)}, u32[]{:S(2)}, u32[]{:S(2)}) %collective-permute-start.24) | collective-permute-done | bytes 147488 | tf_op jit(solution)/shard_map/ppermute | solution.py:53
  61.2 2.0 %collective-permute-start.25 = (bf16[512,512]{1,0:T(8,128)(2,1)S(1)}, bf16[512,512]{1,0:T(8,128)(2,1)S(1)}, u32[]{:S(2)}, u32[]{:S(2)}) collective-permute-start(bf16[512,512]{1,0:T(8,128)(2,1)S(1)} %get-tuple-element.42.refs_4_), channel_id=1, source_target_pairs={{0,2},{2,4},{4,6},{6,0},{1,3},{3,5},{5,7},{7,1},{8,10},{10,12},{12... | collective-permute-start | bytes 1572872 | tf_op jit(solution)/shard_map/ppermute | solution.py:41
  68.5 12.8 %collective-permute-done.2.refs_3_ = bf16[4,128,512]{2,1,0:T(8,128)(2,1)S(1)} collective-permute-done((bf16[4,128,512]{2,1,0:T(8,128)(2,1)S(1)}, bf16[4,128,512]{2,1,0:T(8,128)(2,1)S(1)}, u32[]{:S(2)}, u32[]{:S(2)}) %collective-permute-start.2) | collective-permute-done | bytes 524320 | tf_op jit(solution)/shard_map/ppermute | solution.py:429
  81.3 2.4 %collective-permute-start.15 = (bf16[128,512]{1,0:T(8,128)(2,1)S(1)}, bf16[128,512]{1,0:T(8,128)(2,1)S(1)}, u32[]{:S(2)}, u32[]{:S(2)}) collective-permute-start(bf16[128,512]{1,0:T(8,128)(2,1)S(1)} %slice.9), channel_id=1, source_target_pairs={{0,224},{32,0},{64,32},{96,64},{128,96},{160,128},{192,160},{224,1... | collective-permute-start | bytes 393224 | tf_op jit(solution)/shard_map/ppermute | solution.py:56
  83.7 1.9 %collective-permute-done.15.refs_12_ = bf16[128,512]{1,0:T(8,128)(2,1)S(1)} collective-permute-done((bf16[128,512]{1,0:T(8,128)(2,1)S(1)}, bf16[128,512]{1,0:T(8,128)(2,1)S(1)}, u32[]{:S(2)}, u32[]{:S(2)}) %collective-permute-start.15) | collective-permute-done | bytes 131104 | tf_op jit(solution)/shard_map/ppermute | solution.py:56
  85.7 2.6 %project_pq.1 = (f32[512,512]{1,0:T(8,128)S(1)}, bf16[512,512]{1,0:T(8,128)(2,1)}) custom-call(s32[4]{0:T(128)S(1)} %copy-done.2, bf16[4,128,512]{2,1,0:T(8,128)(2,1)S(1)} %norm.1.refs_0_, bf16[4,128,512]{2,1,0:T(8,128)(2,1)S(1)} %collective-permute-done.refs_1_, bf16[4,128,512]{2,1,0:T(8,128)(2,1)S(1)} %collective-permute-done.1.refs_2_, ...), custom_call_target="tpu_custom_call" | custom-call | tf_op jit(solution)/shard_map/project_pq/pallas_call | solution.py:243
  88.2 2.4 %collective-permute-start.16 = (bf16[512,512]{1,0:T(8,128)(2,1)}, bf16[512,512]{1,0:T(8,128)(2,1)S(1)}, u32[]{:S(2)}, u32[]{:S(2)}) collective-permute-start(bf16[512,512]{1,0:T(8,128)(2,1)} %get-tuple-element.37), channel_id=1, source_target_pairs={{0,1},{1,0},{2,3},{3,2},{4,5},{5,4},{6,7},{7,6},{8,9},{9,8},{10,11... | collective-permute-start | bytes 1572872 | tf_op jit(solution)/shard_map/ppermute | solution.py:37
  90.7 2.5 %project_kv.1 = (f32[512,256]{1,0:T(8,128)S(1)}, f32[512,128]{1,0:T(8,128)S(1)}, bf16[512,384]{1,0:T(8,128)(2,1)}) custom-call(s32[4]{0:T(128)S(1)} %copy-done.2, bf16[4,128,512]{2,1,0:T(8,128)(2,1)S(1)} %norm.1.refs_0_, bf16[4,128,512]{2,1,0:T(8,128)(2,1)S(1)} %collective-permute-done.refs_1_, bf16[4,128,512]{2,1,0:T(8,128)(2,1)S(1)} %collective-permute-done.1.refs_2_, ...), custom_call_target="tpu_custom_call" | custom-call | tf_op jit(solution)/shard_map/project_kv/pallas_call | solution.py:219
  96.3 2.6 %collective-permute-start.30 = (bf16[256,128]{1,0:T(8,128)(2,1)S(1)}, bf16[256,128]{1,0:T(8,128)(2,1)S(1)}, u32[]{:S(2)}, u32[]{:S(2)}) collective-permute-start(bf16[256,128]{1,0:T(8,128)(2,1)S(1)} %get-tuple-element.53), channel_id=1, source_target_pairs={{0,32},{32,64},{64,96},{96,128},{128,160},{160,192},{192,224},{1,3... | collective-permute-start | bytes 196616 | tf_op jit(solution)/shard_map/ppermute | solution.py:449
  100.2 2.5 %collective-permute-start.39 = (bf16[512,512]{1,0:T(8,128)(2,1)S(1)}, bf16[512,512]{1,0:T(8,128)(2,1)S(1)}, u32[]{:S(2)}, u32[]{:S(2)}) collective-permute-start(bf16[512,512]{1,0:T(8,128)(2,1)S(1)} %get-tuple-element.54.refs_0_), channel_id=1, source_target_pairs={{0,4},{2,6},{4,0},{6,2},{1,5},{3,7},{5,1},{7,3},{8,12},{10,14},{12... | collective-permute-start | bytes 1572872 | tf_op jit(solution)/shard_map/ppermute | solution.py:41
  102.7 6.8 %collective-permute-start.31 = (bf16[256,128]{1,0:T(8,128)(2,1)S(1)}, bf16[256,128]{1,0:T(8,128)(2,1)S(1)}, u32[]{:S(2)}, u32[]{:S(2)}) collective-permute-start(bf16[256,128]{1,0:T(8,128)(2,1)S(1)} %get-tuple-element.53), channel_id=1, source_target_pairs={{0,64},{32,96},{64,128},{96,160},{128,192},{160,224},{1,65},{33,97... | collective-permute-start | bytes 196616 | tf_op jit(solution)/shard_map/ppermute | solution.py:449
  111.2 5.2 %collective-permute-start.33 = (bf16[256,128]{1,0:T(8,128)(2,1)S(1)}, bf16[256,128]{1,0:T(8,128)(2,1)S(1)}, u32[]{:S(2)}, u32[]{:S(2)}) collective-permute-start(bf16[256,128]{1,0:T(8,128)(2,1)S(1)} %get-tuple-element.53), channel_id=1, source_target_pairs={{0,128},{32,160},{64,192},{96,224},{1,129},{33,161},{65,193},{97,2... | collective-permute-start | bytes 196616 | tf_op jit(solution)/shard_map/ppermute | solution.py:449
  116.4 4.2 %collective-permute-start.34 = (bf16[256,128]{1,0:T(8,128)(2,1)S(1)}, bf16[256,128]{1,0:T(8,128)(2,1)S(1)}, u32[]{:S(2)}, u32[]{:S(2)}) collective-permute-start(bf16[256,128]{1,0:T(8,128)(2,1)S(1)} %get-tuple-element.53), channel_id=1, source_target_pairs={{0,160},{32,192},{64,224},{1,161},{33,193},{65,225},{2,162},{34,19... | collective-permute-start | bytes 196616 | tf_op jit(solution)/shard_map/ppermute | solution.py:449
  120.6 5.2 %collective-permute-start.35 = (bf16[256,128]{1,0:T(8,128)(2,1)S(1)}, bf16[256,128]{1,0:T(8,128)(2,1)S(1)}, u32[]{:S(2)}, u32[]{:S(2)}) collective-permute-start(bf16[256,128]{1,0:T(8,128)(2,1)S(1)} %get-tuple-element.53), channel_id=1, source_target_pairs={{0,192},{32,224},{1,193},{33,225},{2,194},{34,226},{3,195},{35,227... | collective-permute-start | bytes 196616 | tf_op jit(solution)/shard_map/ppermute | solution.py:449
  129.9 4.8 %collective-permute-start.37 = (f32[512,128]{1,0:T(8,128)S(1)}, f32[512,128]{1,0:T(8,128)S(1)}, u32[]{:S(2)}, u32[]{:S(2)}) collective-permute-start(f32[512,128]{1,0:T(8,128)S(1)} %across.1.ret), channel_id=1, source_target_pairs={{0,1},{1,0},{2,3},{3,2},{4,5},{5,4},{6,7},{7,6},{8,9},{9,8},{10,11... | collective-permute-start | bytes 786440 | tf_op jit(solution)/shard_map/ppermute | solution.py:37
  137.9 2.2 %back.1 = (bf16[128,2048]{1,0:T(8,128)(2,1)S(1)}, bf16[128,2048]{1,0:T(8,128)(2,1)S(1)}, bf16[128,2048]{1,0:T(8,128)(2,1)S(1)}, bf16[128,2048]{1,0:T(8,128)(2,1)S(1)}) custom-call(s32[4]{0:T(128)S(1)} %copy-done.2, bf16[512,256]{1,0:T(8,128)(2,1)S(1)} %pooling.1.pool, f32[512,128]{1,0:T(8,128)S(1)} %across.1.ret, ...), custom_call_target="tpu_custom_call" | custom-call | tf_op jit(solution)/shard_map/back/pallas_call | solution.py:375
  140.7 2.7 %collective-permute-start.42 = (bf16[128,2048]{1,0:T(8,128)(2,1)S(1)}, bf16[128,2048]{1,0:T(8,128)(2,1)S(1)}, u32[]{:S(2)}, u32[]{:S(2)}) collective-permute-start(bf16[128,2048]{1,0:T(8,128)(2,1)S(1)} %get-tuple-element.57), channel_id=1, source_target_pairs={{0,16},{8,24},{16,0},{24,8},{1,17},{9,25},{17,1},{25,9},{2,18},{10... | collective-permute-start | bytes 1572872 | tf_op jit(solution)/shard_map/ppermute | solution.py:461
  143.5 10.8 %collective-permute-done.41.s1 = bf16[128,2048]{1,0:T(8,128)(2,1)S(1)} collective-permute-done((bf16[128,2048]{1,0:T(8,128)(2,1)S(1)}, bf16[128,2048]{1,0:T(8,128)(2,1)S(1)}, u32[]{:S(2)}, u32[]{:S(2)}) %collective-permute-start.41) | collective-permute-done | bytes 524320 | tf_op jit(solution)/shard_map/ppermute | solution.py:461
  154.2 11.9 %collective-permute-done.42.s2 = bf16[128,2048]{1,0:T(8,128)(2,1)S(1)} collective-permute-done((bf16[128,2048]{1,0:T(8,128)(2,1)S(1)}, bf16[128,2048]{1,0:T(8,128)(2,1)S(1)}, u32[]{:S(2)}, u32[]{:S(2)}) %collective-permute-start.42) | collective-permute-done | bytes 524320 | tf_op jit(solution)/shard_map/ppermute | solution.py:461
  169.6 2.2 %mixed.1 = bf16[64,4096]{1,0:T(8,128)(2,1)} custom-call(s32[4]{0:T(128)S(1)} %copy-done.2, bf16[64,2048]{1,0:T(8,128)(2,1)S(1)} %get-tuple-element.59.keep, bf16[64,2048]{1,0:T(8,128)(2,1)S(1)} %collective-permute-done.44.got), custom_call_target="tpu_custom_call" | custom-call | tf_op jit(solution)/shard_map/mixed/pallas_call | solution.py:411
  (90 shorter events, 38.8 us)
Async XLA Ops:
  2.9 9.9 %collective-permute-start.3 = (bf16[112,512]{1,0:T(8,128)(2,1)}, bf16[112,512]{1,0:T(8,128)(2,1)S(1)}, u32[]{:S(2)}, u32[]{:S(2)}) collective-permute-start(bf16[112,512]{1,0:T(8,128)(2,1)} %get-tuple-element.33), channel_id=1, source_target_pairs={{0,0},{1,16},{8,8},{9,24},{16,1},{17,17},{24,9},{25,25},{2,2},{3,1... | collective-permute-start | bytes 344072 | tf_op jit(solution)/shard_map/ppermute | solution.py:423
  22.3 17.7 %collective-permute-start.11 = (bf16[256,512]{1,0:T(8,128)(2,1)S(1)}, bf16[256,512]{1,0:T(8,128)(2,1)S(1)}, u32[]{:S(2)}, u32[]{:S(2)}) collective-permute-start(bf16[256,512]{1,0:T(8,128)(2,1)S(1)} %join.1.refs_4_), channel_id=1, source_target_pairs={{0,32},{32,64},{64,96},{96,128},{128,160},{160,192},{192,224},{224... | collective-permute-start | bytes 786440 | tf_op jit(solution)/shard_map/ppermute | solution.py:49
  24.0 16.0 %collective-permute-start.8 = (bf16[256,512]{1,0:T(8,128)(2,1)S(1)}, bf16[256,512]{1,0:T(8,128)(2,1)S(1)}, u32[]{:S(2)}, u32[]{:S(2)}) collective-permute-start(bf16[256,512]{1,0:T(8,128)(2,1)S(1)} %join.1.refs_4_), channel_id=1, source_target_pairs={{0,224},{32,0},{64,32},{96,64},{128,96},{160,128},{192,160},{224,1... | collective-permute-start | bytes 786440 | tf_op jit(solution)/shard_map/ppermute | solution.py:50
  28.0 7.7 %collective-permute-start.21 = (bf16[144,512]{1,0:T(8,128)(2,1)S(1)}, bf16[144,512]{1,0:T(8,128)(2,1)S(1)}, u32[]{:S(2)}, u32[]{:S(2)}) collective-permute-start(bf16[144,512]{1,0:T(8,128)(2,1)S(1)} %get-tuple-element.41.refs_0_), channel_id=1, source_target_pairs={{0,32},{32,64},{64,96},{96,128},{128,160},{160,192},{192,224},{224... | collective-permute-start | bytes 442376 | tf_op jit(solution)/shard_map/ppermute | solution.py:49
  28.0 14.7 %collective-permute-start.18 = (bf16[144,512]{1,0:T(8,128)(2,1)S(1)}, bf16[144,512]{1,0:T(8,128)(2,1)S(1)}, u32[]{:S(2)}, u32[]{:S(2)}) collective-permute-start(bf16[144,512]{1,0:T(8,128)(2,1)S(1)} %get-tuple-element.41.refs_0_), channel_id=1, source_target_pairs={{0,224},{32,0},{64,32},{96,64},{128,96},{160,128},{192,160},{224,1... | collective-permute-start | bytes 442376 | tf_op jit(solution)/shard_map/ppermute | solution.py:50
  35.7 8.4 %collective-permute-start.22 = (bf16[144,512]{1,0:T(8,128)(2,1)S(1)}, bf16[144,512]{1,0:T(8,128)(2,1)S(1)}, u32[]{:S(2)}, u32[]{:S(2)}) collective-permute-start(bf16[144,512]{1,0:T(8,128)(2,1)S(1)} %collective-permute-done.21.refs_7_), channel_id=1, source_target_pairs={{0,32},{32,64},{64,96},{96,128},{128,160},{160,192},{192,224},{224... | collective-permute-start | bytes 442376 | tf_op jit(solution)/shard_map/ppermute | solution.py:49
  38.4 22.8 %collective-permute-start = (bf16[4,128,512]{2,1,0:T(8,128)(2,1)S(1)}, bf16[4,128,512]{2,1,0:T(8,128)(2,1)S(1)}, u32[]{:S(2)}, u32[]{:S(2)}) collective-permute-start(bf16[4,128,512]{2,1,0:T(8,128)(2,1)S(1)} %norm.1.refs_0_), channel_id=1, source_target_pairs={{0,8},{8,16},{16,24},{24,0},{1,9},{9,17},{17,25},{25,1},{2,10},{10... | collective-permute-start | bytes 1572872 | tf_op jit(solution)/shard_map/ppermute | solution.py:429
  39.9 14.0 %collective-permute-start.12 = (bf16[256,512]{1,0:T(8,128)(2,1)S(1)}, bf16[256,512]{1,0:T(8,128)(2,1)S(1)}, u32[]{:S(2)}, u32[]{:S(2)}) collective-permute-start(bf16[256,512]{1,0:T(8,128)(2,1)S(1)} %collective-permute-done.11.refs_10_), channel_id=1, source_target_pairs={{0,32},{32,64},{64,96},{96,128},{128,160},{160,192},{192,224},{224... | collective-permute-start | bytes 786440 | tf_op jit(solution)/shard_map/ppermute | solution.py:49
  40.0 14.3 %collective-permute-start.9 = (bf16[256,512]{1,0:T(8,128)(2,1)S(1)}, bf16[256,512]{1,0:T(8,128)(2,1)S(1)}, u32[]{:S(2)}, u32[]{:S(2)}) collective-permute-start(bf16[256,512]{1,0:T(8,128)(2,1)S(1)} %collective-permute-done.8.refs_5_), channel_id=1, source_target_pairs={{0,224},{32,0},{64,32},{96,64},{128,96},{160,128},{192,160},{224,1... | collective-permute-start | bytes 786440 | tf_op jit(solution)/shard_map/ppermute | solution.py:50
  42.7 7.8 %collective-permute-start.19 = (bf16[144,512]{1,0:T(8,128)(2,1)S(1)}, bf16[144,512]{1,0:T(8,128)(2,1)S(1)}, u32[]{:S(2)}, u32[]{:S(2)}) collective-permute-start(bf16[144,512]{1,0:T(8,128)(2,1)S(1)} %collective-permute-done.18.refs_1_), channel_id=1, source_target_pairs={{0,224},{32,0},{64,32},{96,64},{128,96},{160,128},{192,160},{224,1... | collective-permute-start | bytes 442376 | tf_op jit(solution)/shard_map/ppermute | solution.py:50
  44.1 9.8 %collective-permute-start.23 = (bf16[144,512]{1,0:T(8,128)(2,1)S(1)}, bf16[144,512]{1,0:T(8,128)(2,1)S(1)}, u32[]{:S(2)}, u32[]{:S(2)}) collective-permute-start(bf16[144,512]{1,0:T(8,128)(2,1)S(1)} %collective-permute-done.22.refs_6_), channel_id=1, source_target_pairs={{0,32},{32,64},{64,96},{96,128},{128,160},{160,192},{192,224},{224... | collective-permute-start | bytes 442376 | tf_op jit(solution)/shard_map/ppermute | solution.py:49
  53.9 10.1 %collective-permute-start.13 = (bf16[256,512]{1,0:T(8,128)(2,1)S(1)}, bf16[256,512]{1,0:T(8,128)(2,1)S(1)}, u32[]{:S(2)}, u32[]{:S(2)}) collective-permute-start(bf16[256,512]{1,0:T(8,128)(2,1)S(1)} %collective-permute-done.12.refs_9_), channel_id=1, source_target_pairs={{0,32},{32,64},{64,96},{96,128},{128,160},{160,192},{192,224},{224... | collective-permute-start | bytes 786440 | tf_op jit(solution)/shard_map/ppermute | solution.py:49
  54.3 11.4 %collective-permute-start.10 = (bf16[256,512]{1,0:T(8,128)(2,1)S(1)}, bf16[256,512]{1,0:T(8,128)(2,1)S(1)}, u32[]{:S(2)}, u32[]{:S(2)}) collective-permute-start(bf16[256,512]{1,0:T(8,128)(2,1)S(1)} %collective-permute-done.9.refs_6_), channel_id=1, source_target_pairs={{0,224},{32,0},{64,32},{96,64},{128,96},{160,128},{192,160},{224,1... | collective-permute-start | bytes 786440 | tf_op jit(solution)/shard_map/ppermute | solution.py:50
  56.7 11.8 %collective-permute-start.1 = (bf16[4,128,512]{2,1,0:T(8,128)(2,1)S(1)}, bf16[4,128,512]{2,1,0:T(8,128)(2,1)S(1)}, u32[]{:S(2)}, u32[]{:S(2)}) collective-permute-start(bf16[4,128,512]{2,1,0:T(8,128)(2,1)S(1)} %norm.1.refs_0_), channel_id=1, source_target_pairs={{0,16},{8,24},{16,0},{24,8},{1,17},{9,25},{17,1},{25,9},{2,18},{10... | collective-permute-start | bytes 1572872 | tf_op jit(solution)/shard_map/ppermute | solution.py:429
  59.1 22.2 %collective-permute-start.2 = (bf16[4,128,512]{2,1,0:T(8,128)(2,1)S(1)}, bf16[4,128,512]{2,1,0:T(8,128)(2,1)S(1)}, u32[]{:S(2)}, u32[]{:S(2)}) collective-permute-start(bf16[4,128,512]{2,1,0:T(8,128)(2,1)S(1)} %norm.1.refs_0_), channel_id=1, source_target_pairs={{0,24},{8,0},{16,8},{24,16},{1,25},{9,1},{17,9},{25,17},{2,26},{10... | collective-permute-start | bytes 1572872 | tf_op jit(solution)/shard_map/ppermute | solution.py:429
  61.2 29.5 %collective-permute-start.25 = (bf16[512,512]{1,0:T(8,128)(2,1)S(1)}, bf16[512,512]{1,0:T(8,128)(2,1)S(1)}, u32[]{:S(2)}, u32[]{:S(2)}) collective-permute-start(bf16[512,512]{1,0:T(8,128)(2,1)S(1)} %get-tuple-element.42.refs_4_), channel_id=1, source_target_pairs={{0,2},{2,4},{4,6},{6,0},{1,3},{3,5},{5,7},{7,1},{8,10},{10,12},{12... | collective-permute-start | bytes 1572872 | tf_op jit(solution)/shard_map/ppermute | solution.py:41
  64.0 26.7 %collective-permute-start.26 = (bf16[512,512]{1,0:T(8,128)(2,1)S(1)}, bf16[512,512]{1,0:T(8,128)(2,1)S(1)}, u32[]{:S(2)}, u32[]{:S(2)}) collective-permute-start(bf16[512,512]{1,0:T(8,128)(2,1)S(1)} %get-tuple-element.42.refs_4_), channel_id=1, source_target_pairs={{0,4},{2,6},{4,0},{6,2},{1,5},{3,7},{5,1},{7,3},{8,12},{10,14},{12... | collective-permute-start | bytes 1572872 | tf_op jit(solution)/shard_map/ppermute | solution.py:41
  65.7 25.0 %collective-permute-start.27 = (bf16[512,512]{1,0:T(8,128)(2,1)S(1)}, bf16[512,512]{1,0:T(8,128)(2,1)S(1)}, u32[]{:S(2)}, u32[]{:S(2)}) collective-permute-start(bf16[512,512]{1,0:T(8,128)(2,1)S(1)} %get-tuple-element.42.refs_4_), channel_id=1, source_target_pairs={{0,6},{2,0},{4,2},{6,4},{1,7},{3,1},{5,3},{7,5},{8,14},{10,8},{12,... | collective-permute-start | bytes 1572872 | tf_op jit(solution)/shard_map/ppermute | solution.py:41
  68.5 15.2 %collective-permute-start.14 = (bf16[128,512]{1,0:T(8,128)(2,1)S(1)}, bf16[128,512]{1,0:T(8,128)(2,1)S(1)}, u32[]{:S(2)}, u32[]{:S(2)}) collective-permute-start(bf16[128,512]{1,0:T(8,128)(2,1)S(1)} %slice.8), channel_id=1, source_target_pairs={{0,32},{32,64},{64,96},{96,128},{128,160},{160,192},{192,224},{224... | collective-permute-start | bytes 393224 | tf_op jit(solution)/shard_map/ppermute | solution.py:56
  88.2 14.5 %collective-permute-start.16 = (bf16[512,512]{1,0:T(8,128)(2,1)}, bf16[512,512]{1,0:T(8,128)(2,1)S(1)}, u32[]{:S(2)}, u32[]{:S(2)}) collective-permute-start(bf16[512,512]{1,0:T(8,128)(2,1)} %get-tuple-element.37), channel_id=1, source_target_pairs={{0,1},{1,0},{2,3},{3,2},{4,5},{5,4},{6,7},{7,6},{8,9},{9,8},{10,11... | collective-permute-start | bytes 1572872 | tf_op jit(solution)/shard_map/ppermute | solution.py:37
  96.3 13.2 %collective-permute-start.30 = (bf16[256,128]{1,0:T(8,128)(2,1)S(1)}, bf16[256,128]{1,0:T(8,128)(2,1)S(1)}, u32[]{:S(2)}, u32[]{:S(2)}) collective-permute-start(bf16[256,128]{1,0:T(8,128)(2,1)S(1)} %get-tuple-element.53), channel_id=1, source_target_pairs={{0,32},{32,64},{64,96},{96,128},{128,160},{160,192},{192,224},{1,3... | collective-permute-start | bytes 196616 | tf_op jit(solution)/shard_map/ppermute | solution.py:449
  98.9 39.0 %collective-permute-start.38 = (bf16[512,512]{1,0:T(8,128)(2,1)S(1)}, bf16[512,512]{1,0:T(8,128)(2,1)S(1)}, u32[]{:S(2)}, u32[]{:S(2)}) collective-permute-start(bf16[512,512]{1,0:T(8,128)(2,1)S(1)} %get-tuple-element.54.refs_0_), channel_id=1, source_target_pairs={{0,2},{2,4},{4,6},{6,0},{1,3},{3,5},{5,7},{7,1},{8,10},{10,12},{12... | collective-permute-start | bytes 1572872 | tf_op jit(solution)/shard_map/ppermute | solution.py:41
  100.2 37.7 %collective-permute-start.39 = (bf16[512,512]{1,0:T(8,128)(2,1)S(1)}, bf16[512,512]{1,0:T(8,128)(2,1)S(1)}, u32[]{:S(2)}, u32[]{:S(2)}) collective-permute-start(bf16[512,512]{1,0:T(8,128)(2,1)S(1)} %get-tuple-element.54.refs_0_), channel_id=1, source_target_pairs={{0,4},{2,6},{4,0},{6,2},{1,5},{3,7},{5,1},{7,3},{8,12},{10,14},{12... | collective-permute-start | bytes 1572872 | tf_op jit(solution)/shard_map/ppermute | solution.py:41
  102.7 35.1 %collective-permute-start.40 = (bf16[512,512]{1,0:T(8,128)(2,1)S(1)}, bf16[512,512]{1,0:T(8,128)(2,1)S(1)}, u32[]{:S(2)}, u32[]{:S(2)}) collective-permute-start(bf16[512,512]{1,0:T(8,128)(2,1)S(1)} %get-tuple-element.54.refs_0_), channel_id=1, source_target_pairs={{0,6},{2,0},{4,2},{6,4},{1,7},{3,1},{5,3},{7,5},{8,14},{10,8},{12,... | collective-permute-start | bytes 1572872 | tf_op jit(solution)/shard_map/ppermute | solution.py:41
  102.7 8.5 %collective-permute-start.31 = (bf16[256,128]{1,0:T(8,128)(2,1)S(1)}, bf16[256,128]{1,0:T(8,128)(2,1)S(1)}, u32[]{:S(2)}, u32[]{:S(2)}) collective-permute-start(bf16[256,128]{1,0:T(8,128)(2,1)S(1)} %get-tuple-element.53), channel_id=1, source_target_pairs={{0,64},{32,96},{64,128},{96,160},{128,192},{160,224},{1,65},{33,97... | collective-permute-start | bytes 196616 | tf_op jit(solution)/shard_map/ppermute | solution.py:449
  111.2 9.4 %collective-permute-start.33 = (bf16[256,128]{1,0:T(8,128)(2,1)S(1)}, bf16[256,128]{1,0:T(8,128)(2,1)S(1)}, u32[]{:S(2)}, u32[]{:S(2)}) collective-permute-start(bf16[256,128]{1,0:T(8,128)(2,1)S(1)} %get-tuple-element.53), channel_id=1, source_target_pairs={{0,128},{32,160},{64,192},{96,224},{1,129},{33,161},{65,193},{97,2... | collective-permute-start | bytes 196616 | tf_op jit(solution)/shard_map/ppermute | solution.py:449
  116.4 9.4 %collective-permute-start.34 = (bf16[256,128]{1,0:T(8,128)(2,1)S(1)}, bf16[256,128]{1,0:T(8,128)(2,1)S(1)}, u32[]{:S(2)}, u32[]{:S(2)}) collective-permute-start(bf16[256,128]{1,0:T(8,128)(2,1)S(1)} %get-tuple-element.53), channel_id=1, source_target_pairs={{0,160},{32,192},{64,224},{1,161},{33,193},{65,225},{2,162},{34,19... | collective-permute-start | bytes 196616 | tf_op jit(solution)/shard_map/ppermute | solution.py:449
  120.6 7.8 %collective-permute-start.35 = (bf16[256,128]{1,0:T(8,128)(2,1)S(1)}, bf16[256,128]{1,0:T(8,128)(2,1)S(1)}, u32[]{:S(2)}, u32[]{:S(2)}) collective-permute-start(bf16[256,128]{1,0:T(8,128)(2,1)S(1)} %get-tuple-element.53), channel_id=1, source_target_pairs={{0,192},{32,224},{1,193},{33,225},{2,194},{34,226},{3,195},{35,227... | collective-permute-start | bytes 196616 | tf_op jit(solution)/shard_map/ppermute | solution.py:449
  129.9 8.0 %collective-permute-start.37 = (f32[512,128]{1,0:T(8,128)S(1)}, f32[512,128]{1,0:T(8,128)S(1)}, u32[]{:S(2)}, u32[]{:S(2)}) collective-permute-start(f32[512,128]{1,0:T(8,128)S(1)} %across.1.ret), channel_id=1, source_target_pairs={{0,1},{1,0},{2,3},{3,2},{4,5},{5,4},{6,7},{7,6},{8,9},{9,8},{10,11... | collective-permute-start | bytes 786440 | tf_op jit(solution)/shard_map/ppermute | solution.py:37
  140.1 14.2 %collective-permute-start.41 = (bf16[128,2048]{1,0:T(8,128)(2,1)S(1)}, bf16[128,2048]{1,0:T(8,128)(2,1)S(1)}, u32[]{:S(2)}, u32[]{:S(2)}) collective-permute-start(bf16[128,2048]{1,0:T(8,128)(2,1)S(1)} %get-tuple-element.56), channel_id=1, source_target_pairs={{0,8},{8,16},{16,24},{24,0},{1,9},{9,17},{17,25},{25,1},{2,10},{10... | collective-permute-start | bytes 1572872 | tf_op jit(solution)/shard_map/ppermute | solution.py:461
  140.7 25.4 %collective-permute-start.42 = (bf16[128,2048]{1,0:T(8,128)(2,1)S(1)}, bf16[128,2048]{1,0:T(8,128)(2,1)S(1)}, u32[]{:S(2)}, u32[]{:S(2)}) collective-permute-start(bf16[128,2048]{1,0:T(8,128)(2,1)S(1)} %get-tuple-element.57), channel_id=1, source_target_pairs={{0,16},{8,24},{16,0},{24,8},{1,17},{9,25},{17,1},{25,9},{2,18},{10... | collective-permute-start | bytes 1572872 | tf_op jit(solution)/shard_map/ppermute | solution.py:461
  143.5 22.7 %collective-permute-start.43 = (bf16[128,2048]{1,0:T(8,128)(2,1)S(1)}, bf16[128,2048]{1,0:T(8,128)(2,1)S(1)}, u32[]{:S(2)}, u32[]{:S(2)}) collective-permute-start(bf16[128,2048]{1,0:T(8,128)(2,1)S(1)} %get-tuple-element.58), channel_id=1, source_target_pairs={{0,24},{8,0},{16,8},{24,16},{1,25},{9,1},{17,9},{25,17},{2,26},{10... | collective-permute-start | bytes 1572872 | tf_op jit(solution)/shard_map/ppermute | solution.py:461
  (18 other events, 88.8 us)

commit v3 on v2

--- a/solution.py
+++ b/solution.py
@@ -8,6 +8,8 @@
 
 NZ, NY, NX = 8, 4, 4
 SPAN = 512
+ORDER = (0, 1, 7, 2, 6, 3, 5, 4)
+EARLY = 6
 HALO = 16
 HEAD = 256
 HALF = 128
@@ -147,15 +149,20 @@
 
 def norm_body(at, tok, gain, out, full):
     z, x, c = at[0], at[2], at[3]
-    v = tok[...].astype(f32)
-    v = v * lax.rsqrt(jnp.mean(v * v, axis=-1, keepdims=True) + eps) * gain[...]
-    full[...] = v.astype(bf16)
+
+    @pl.loop(0, HALF // 16)
+    def _(i):
+        rows = pl.ds(pl.multiple_of(i * 16, 16), 16)
+        v = tok[rows, :].astype(f32)
+        v = v * lax.rsqrt(jnp.mean(v * v, axis=-1, keepdims=True) + eps) * gain[...]
+        full[rows, :] = v.astype(bf16)
+
     lane_in = lax.broadcasted_iota(jnp.int32, (512, 512), 0)
     lane_out = lax.broadcasted_iota(jnp.int32, (512, 512), 1)
     source = (lane_out % 128) // 64 * 256 + (lane_out % 64) // 32 * 128 + (x + NX - lane_out // 128) % NX * 32 + lane_out % 32
     order = (lane_in == source).astype(bf16)
     for pair in range(NZ // 2):
-        two = [full[:, pl.ds(pl.multiple_of((z + 2 * pair + i) % NZ * 512 + c * 256, 256), 256)] for i in range(2)]
+        two = [full[:, pl.ds(pl.multiple_of((z + ORDER[2 * pair + i]) % NZ * 512 + c * 256, 256), 256)] for i in range(2)]
         r = jnp.dot(jnp.concatenate(two, axis=1), order, preferred_element_type=f32).astype(bf16)
         for kx in range(NX):
             out[kx, :, pair * 128:pair * 128 + 128] = r[:, kx * 128:kx * 128 + 128]
@@ -169,11 +176,24 @@
     )(at, tok, gain)
 
 
-def split_body(at, *refs):
+def early_body(*refs):
+    for i in range(EARLY):
+        refs[EARLY][i * 64:i * 64 + 64, :] = refs[i][0:64, :]
+
+
+def split_early(chunks):
+    return local(
+        early_body, in_specs=[VM] * EARLY, out_specs=VM,
+        out_shape=jax.ShapeDtypeStruct((EARLY * 64, 512), bf16), name="split_early",
+    )(*[chunks[kz] for kz in ORDER[:EARLY]])
+
+
+def late_body(at, *refs):
     z, c = at[0], at[3]
     ins, (kv, out_w, keep, give) = refs[:NZ], refs[NZ:]
+    for i, kz in enumerate(ORDER[EARLY:]):
+        kv[i * 64:i * 64 + 64, :] = ins[kz][0:64, :]
     for kz in range(NZ):
-        kv[kz * 64:kz * 64 + 64, :] = ins[kz][0:64, :]
         out_w[kz * 64:kz * 64 + 64, :] = ins[kz][64:128, :]
         for out, half in ((keep, c), (give, 1 - c)):
             hi = ins[kz][128:144, pl.ds(pl.multiple_of(half * HALF, HALF), HALF)].astype(f32)
@@ -181,11 +201,12 @@
             out[pl.ds(pl.multiple_of(((z + kz) % NZ) * 16, 16), 16), :] = hi + lo
 
 
-def split(at, chunks):
-    return local(
-        split_body, in_specs=[SM] + [VM] * NZ, out_specs=[VM] * 4,
-        out_shape=[jax.ShapeDtypeStruct((512, 512), bf16)] * 2 + [jax.ShapeDtypeStruct((HALF, HALF), f32)] * 2,
-        name="split",
+def split_late(at, chunks):
+    return local(
+        late_body, in_specs=[SM] + [VM] * NZ, out_specs=[VM] * 4,
+        out_shape=[jax.ShapeDtypeStruct(((NZ - EARLY) * 64, 512), bf16), jax.ShapeDtypeStruct((512, 512), bf16)]
+        + [jax.ShapeDtypeStruct((HALF, HALF), f32)] * 2,
+        name="split_late",
     )(at, *chunks)
 
 
@@ -204,8 +225,8 @@
 
 def kv_body(at, *refs):
     y, c = at[1], at[3]
-    toks, ws, (kpart, vkeep, send) = refs[:4], refs[4:8], refs[8:]
-    acc = multiply(toks, lambda kx: ws[kx][...])
+    toks, early, late, (kpart, vkeep, send) = refs[:4], refs[4:8], refs[8:12], refs[12:]
+    acc = multiply(toks, lambda kx: jnp.concatenate([early[kx][...], late[kx][...]], axis=0))
     for k in range(NY):
         r = acc[k * HALF:(k + 1) * HALF]
         rows = span_rows(y, k)
@@ -217,7 +238,7 @@
 
 def project_kv(at, toks, ws):
     return local(
-        kv_body, in_specs=[SM] + [VM] * 8, out_specs=[VM] * 3,
+        kv_body, in_specs=[SM] + [VM] * 12, out_specs=[VM] * 3,
         out_shape=[jax.ShapeDtypeStruct((SPAN, HEAD), f32), jax.ShapeDtypeStruct((SPAN, HALF), f32),
                    jax.ShapeDtypeStruct((SPAN, 384), bf16)],
         name="project_kv",
@@ -225,12 +246,10 @@
 
 
 def pq_body(at, *refs):
-    toks, ws, (own, send, rhs) = refs[:4], refs[4:13], refs[13:]
-    for i, kz in enumerate((0, 1, 2, 3, 5, 6, 7)):
+    toks, ws, (own, send, rhs) = refs[:4], refs[4:12], refs[12:]
+    for kz in range(NZ):
         for kx in range(NX):
-            rhs[kx, kz * 64:kz * 64 + 64, :] = ws[i][kx * 64:kx * 64 + 64, :]
-    for kx in range(NX):
-        rhs[kx, 256:320, :] = ws[7 + kx // 2][kx % 2 * 64:kx % 2 * 64 + 64, :]
+            rhs[kx, ORDER.index(kz) * 64:ORDER.index(kz) * 64 + 64, :] = ws[kz][kx * 64:kx * 64 + 64, :]
     acc = multiply(toks, lambda kx: rhs[kx])
     for k in range(NY):
         r = acc[k * HALF:(k + 1) * HALF]
@@ -241,7 +260,7 @@
 
 def project_pq(at, toks, ws):
     return local(
-        pq_body, in_specs=[SM] + [VM] * 13, out_specs=[VM] * 2,
+        pq_body, in_specs=[SM] + [VM] * 12, out_specs=[VM] * 2,
         out_shape=[jax.ShapeDtypeStruct((SPAN, 512), f32), jax.ShapeDtypeStruct((SPAN, 512), bf16)],
         scratch_shapes=[pltpu.VMEM((NX, 512, 512), bf16)], name="project_pq",
     )(at, *toks, *ws)
@@ -357,7 +376,7 @@
 
 def back_body(at, pool, ret, other, *refs):
     y, c = at[1], at[3]
-    ws, outs, act, res = refs[:4], refs[4:8], refs[8], refs[9]
+    ws, outs, act, res = refs[:4], refs[4:12], refs[12], refs[13]
     r, o = ret[...], other[...]
     square = jnp.sum(r * r, axis=-1, keepdims=True) + jnp.sum(o * o, axis=-1, keepdims=True)
     factor = lax.rsqrt(square * (1.0 / HEAD) + eps)
@@ -367,51 +386,52 @@
     for kx in range(NX):
         r = lax.dot_general(act[...], ws[kx][...], (((1,), (1,)), ((), ())), preferred_element_type=f32)
         res[:, kx * 512:kx * 512 + 512] = r.astype(bf16)
-    for k, out in enumerate(outs):
-        out[...] = res[pl.ds(pl.multiple_of(((y + k) % NY) * HALF, HALF), HALF), :]
+    for k in range(NY):
+        for cross, half in enumerate((c, 1 - c)):
+            first = ((y + k) % NY) * HALF + half * 64
+            outs[2 * k + cross][...] = res[pl.ds(pl.multiple_of(first, 64), 64), :]
 
 
 def back(at, pool, ret, other, ws):
     return local(
-        back_body, in_specs=[SM] + [VM] * 7, out_specs=[VM] * 4,
-        out_shape=[jax.ShapeDtypeStruct((HALF, 2048), bf16)] * 4,
+        back_body, in_specs=[SM] + [VM] * 7, out_specs=[VM] * 8,
+        out_shape=[jax.ShapeDtypeStruct((64, 2048), bf16)] * 8,
         scratch_shapes=[pltpu.VMEM((SPAN, 512), bf16), pltpu.VMEM((SPAN, 2048), bf16)], name="back",
     )(at, pool, ret, other, *ws)
 
 
-def total_body(at, s0, s1, s2, s3, keep, give):
-    c = at[3]
-    for out, half in ((keep, c), (give, 1 - c)):
-        rows = pl.ds(pl.multiple_of(half * 64, 64), 64)
-        out[...] = (s0[rows, :].astype(f32) + s1[rows, :].astype(f32) + (s2[rows, :].astype(f32) + s3[rows, :].astype(f32))).astype(bf16)
-
-
-def total(at, arrived):
-    return local(
-        total_body, in_specs=[SM] + [VM] * 4, out_specs=[VM] * 2,
-        out_shape=[jax.ShapeDtypeStruct((64, 2048), bf16)] * 2, name="total",
-    )(at, *arrived)
-
-
-def mixed_body(at, keep, got, out):
+def owner(k, cross):
+    return [(2 * y + c, 2 * ((y + k) % NY) + (c ^ cross)) for y in range(NY) for c in range(2)]
+
+
+def mixed_body(at, *refs):
     z, x, c = at[0], at[2], at[3]
+    shares, out, total = refs[:8], refs[8], refs[9]
     lane_in = lax.broadcasted_iota(jnp.int32, (512, 512), 0)
     lane_out = lax.broadcasted_iota(jnp.int32, (512, 512), 1)
     source = (x + NX - (lane_out % 128) // 32) % NX * 128 + lane_out // 256 * 64 + (lane_out % 256) // 128 * 32 + lane_out % 32
     order = (lane_in == source).astype(bf16)
-    for pair in range(NZ // 2):
-        for ref, core in ((keep, c), (got, 1 - c)):
-            rows = jnp.concatenate([ref[:, kx * 512 + pair * 128:kx * 512 + pair * 128 + 128] for kx in range(NX)], axis=1)
-            r = jnp.dot(rows, order, preferred_element_type=f32).astype(bf16)
+    for cross in range(2):
+        a, b, d, e = (shares[2 * k + cross][...].astype(f32) for k in range(NY))
+        total[cross * 64:cross * 64 + 64, :] = ((a + b) + (d + e)).astype(bf16)
+
+    @pl.loop(0, NZ // 2)
+    def _(pair):
+        at_pair = [pl.ds(pl.multiple_of(kx * 512 + pair * 128, 128), 128) for kx in range(NX)]
+        rows = jnp.concatenate([total[:, lanes] for lanes in at_pair], axis=1)
+        r = jnp.dot(rows, order, preferred_element_type=f32).astype(bf16)
+        for cross, core in enumerate((c, 1 - c)):
             for i in range(2):
-                out[:, pl.ds(pl.multiple_of((z + 2 * pair + i) % NZ * 512 + core * 256, 256), 256)] = r[:, i * 256:i * 256 + 256]
-
-
-def mixed(at, keep, got):
-    return local(
-        mixed_body, in_specs=[SM] + [VM] * 2, out_specs=VM,
-        out_shape=jax.ShapeDtypeStruct((64, 4096), bf16), name="mixed",
-    )(at, keep, got)
+                lanes = pl.ds(pl.multiple_of((z + 2 * pair + i) % NZ * 512 + core * 256, 256), 256)
+                out[:, lanes] = r[cross * 64:cross * 64 + 64, i * 256:i * 256 + 256]
+
+
+def mixed(at, shares):
+    return local(
+        mixed_body, in_specs=[SM] + [VM] * 8, out_specs=VM,
+        out_shape=jax.ShapeDtypeStruct((64, 4096), bf16),
+        scratch_shapes=[pltpu.VMEM((2 * 64, 2048), bf16)], name="mixed",
+    )(at, *shares)
 
 
 def layer(tokens, norm_gain, pool_proj, query_proj, key_proj, value_proj, pool_map, pool_scale,
@@ -430,13 +450,14 @@
 
 
     in_z = z_ring(shard_in, False)
-    plane_kv, plane_out, keep, give = split(at, in_z)
-    kv_list = direct(plane_kv, "x", NX)
+    kv_list = direct(split_early(in_z), "x", NX)
+    plane_kv, plane_out, keep, give = split_late(at, in_z)
+    kv_list = kv_list + direct(plane_kv, "x", NX)
     out_list = direct(plane_out, "x", NX)
     start_other = swap(give)
 
     plane_pq = join(direct(shard_pq, "x", NX))
-    pq_list = z_ring(plane_pq, True)
+    pq_list = z_ring(plane_pq, False)
 
     positions = (jnp.arange(SPAN, dtype=jnp.int32) + z * SPAN)
     inv_freq = 1.0 / rope_base ** jnp.linspace(0.0, 1.0, HALF, dtype=f32)
@@ -458,10 +479,12 @@
     other = swap(ret)
 
     shares = back(at, pool_out, ret, other, out_list)
-    arrived = [shares[0]] + [lax.ppermute(shares[k], "y", ring(NY, k)) for k in range(1, NY)]
-    keep, give = total(at, arrived)
-    got = swap(give)
-    return mixed(at, keep, got)[None]
+    arrived = [shares[0]]
+    for k in range(NY):
+        for cross in range(2):
+            if k + cross > 0:
+                arrived.append(lax.ppermute(shares[2 * k + cross], ("y", "c"), owner(k, cross)))
+    return mixed(at, arrived)[None]
 
 
 def solution(mesh):

time: 172 us -> 187 us (1.087); the launches traced: 172 us -> 185 us
  local copies, waits for them, and re-layouts: 1.26 us -> 8.11 us
  waiting for transfers between devices: 63.4 us -> 66.5 us
  starting transfers between devices: 86.1 us -> 88.8 us
    ppermute x9 -> x12, waiting for transfers between devices: 1.98 us -> 16.9 us  [direct(): return [a] + [lax.ppermute(a, axis, ring(n, k)) for k in range(1, n)]]
    unnamed x10 -> x42, local copies, waits for them, and re-layouts: 1.24 us -> 8.11 us
    ppermute x5 -> x7, waiting for transfers between devices: 24.6 us -> 18.4 us  [layer(): lax.ppermute(shares[2 * k + cross], ('y', 'c'), owner(k, cross))]
    ppermute x6, waiting for transfers between devices: 6.34 us -> 0.39 us  [z_ring(): down = lax.ppermute(down, 'z', ring(NZ, -1))]
    ppermute x6, starting transfers between devices: 16.7 us -> 10.8 us  [z_ring(): down = lax.ppermute(down, 'z', ring(NZ, -1))]
    ppermute x3, waiting for transfers between devices: 14.1 us -> 9.59 us  [layer(): toks.append(lax.ppermute(toks[0], 'y', ring(NY, k)))]
    ppermute x5 -> x7, starting transfers between devices: 5.85 us -> 10.2 us  [layer(): lax.ppermute(shares[2 * k + cross], ('y', 'c'), owner(k, cross))]
    ppermute x7, waiting for transfers between devices: 0.58 us -> 3.68 us  [layer(): earlier = [lax.ppermute(sent, 'z', line(NZ, k)) for k in range(1, NZ)]]
  transfers between devices with their start and end apart: 45 -> 50, of which waited for: 18 -> 19; matrix products, arithmetic and copies ran while one was open for 1% -> 1% of each run, Pallas kernels for 6% -> 6%
where the time goes in v3:
time: 187 us; the launch traced here: 185 us
  starting transfers between devices  88.8 us (47%)
  waiting for transfers between devices  66.5 us (36%)
  Pallas kernels  19.4 us (10%)
  local copies, waits for them, and re-layouts  8.11 us (4%)
    ppermute x7, starting transfers between devices, layer(): earlier = [lax.ppermute(sent, 'z', line(NZ, k)) for k in range(1, NZ)]  28.2 us
    ppermute x7, waiting for transfers between devices, layer(): lax.ppermute(shares[2 * k + cross], ('y', 'c'), owner(k, cross))  18.4 us
    ppermute x12, waiting for transfers between devices, direct(): return [a] + [lax.ppermute(a, axis, ring(n, k)) for k in range(1, n)]  16.9 us
    ppermute x12, starting transfers between devices, direct(): return [a] + [lax.ppermute(a, axis, ring(n, k)) for k in range(1, n)]  16.8 us
    ppermute x6, starting transfers between devices, z_ring(): down = lax.ppermute(down, 'z', ring(NZ, -1))  10.8 us
    ppermute x7, starting transfers between devices, layer(): lax.ppermute(shares[2 * k + cross], ('y', 'c'), owner(k, cross))  10.2 us
    ppermute x3, waiting for transfers between devices, layer(): toks.append(lax.ppermute(toks[0], 'y', ring(NY, k)))  9.59 us
    ppermute x4, starting transfers between devices, swap(): return lax.ppermute(a, 'c', SWAP)  8.52 us
  transfers between devices with their start and end apart: 50, of which 19 were waited for; matrix products, arithmetic and copies ran while one was open for 1% of the time, Pallas kernels for 6%

profile of v3, /device:TPU:1, one launch (start us, length us, event | category | flops | bytes accessed | tf_op | source)
XLA Modules:
  0.0 184.9 jit_solution(10637122520786648149)
XLA Ops:
  0.6 2.3 %pack.1 = (bf16[112,512]{1,0:T(8,128)(2,1)}, bf16[112,512]{1,0:T(8,128)(2,1)}) custom-call(s32[4]{0:T(128)} %pad_add_fusion.at, f32[2]{0:T(128)} %decay.1, bf16[32,512]{1,0:T(8,128)(2,1)} %refs_0_.1, bf16[32,512]{1,0:T(8,128)(2,1)} %refs_1_.1, bf16[32,512]{1,0:T(8,128)(2,1)} %refs_2_.1, bf16[32,512]{1,0:T(8,128)(2,1)} %refs_3_.1, f32[2,8,256]{2,1,0:T(8,128)} %bitcast.16, ...), custom_call_target="tpu_custom_call" | custom-call | tf_op jit(solution)/shard_map/pack/pallas_call | solution.py:103
  2.9 6.2 %collective-permute-start.3 = (bf16[112,512]{1,0:T(8,128)(2,1)}, bf16[112,512]{1,0:T(8,128)(2,1)S(1)}, u32[]{:S(2)}, u32[]{:S(2)}) collective-permute-start(bf16[112,512]{1,0:T(8,128)(2,1)} %get-tuple-element.35), channel_id=1, source_target_pairs={{0,0},{1,16},{8,8},{9,24},{16,1},{17,17},{24,9},{25,25},{2,2},{3,1... | collective-permute-start | bytes 344072 | tf_op jit(solution)/shard_map/ppermute | solution.py:443
  9.7 3.1 %collective-permute-done.3.r0 = bf16[112,512]{1,0:T(8,128)(2,1)S(1)} collective-permute-done((bf16[112,512]{1,0:T(8,128)(2,1)}, bf16[112,512]{1,0:T(8,128)(2,1)S(1)}, u32[]{:S(2)}, u32[]{:S(2)}) %collective-permute-start.3) | collective-permute-done | bytes 114720 | tf_op jit(solution)/shard_map/ppermute | solution.py:443
  16.7 2.5 %collective-permute-start.6 = (bf16[64,512]{1,0:T(8,128)(2,1)S(1)}, bf16[64,512]{1,0:T(8,128)(2,1)S(1)}, u32[]{:S(2)}, u32[]{:S(2)}) collective-permute-start(bf16[64,512]{1,0:T(8,128)(2,1)S(1)} %get-tuple-element.37.a), channel_id=1, source_target_pairs={{0,4},{2,6},{4,0},{6,2},{1,5},{3,7},{5,1},{7,3},{8,12},{10,14},{12... | collective-permute-start | bytes 196616 | tf_op jit(solution)/shard_map/ppermute | solution.py:43
  22.0 3.9 %collective-permute-start.17 = (bf16[144,512]{1,0:T(8,128)(2,1)S(1)}, bf16[144,512]{1,0:T(8,128)(2,1)S(1)}, u32[]{:S(2)}, u32[]{:S(2)}) collective-permute-start(bf16[144,512]{1,0:T(8,128)(2,1)S(1)} %get-tuple-element.43.refs_0_), channel_id=1, source_target_pairs={{0,224},{32,0},{64,32},{96,64},{128,96},{160,128},{192,160},{224,1... | collective-permute-start | bytes 442376 | tf_op jit(solution)/shard_map/ppermute | solution.py:52
  26.0 3.8 %collective-permute-done.18.refs_2_.refs_7_ = bf16[144,512]{1,0:T(8,128)(2,1)S(1)} collective-permute-done((bf16[144,512]{1,0:T(8,128)(2,1)S(1)}, bf16[144,512]{1,0:T(8,128)(2,1)S(1)}, u32[]{:S(2)}, u32[]{:S(2)}) %collective-permute-start.18) | collective-permute-done | bytes 147488 | tf_op jit(solution)/shard_map/ppermute | solution.py:51
  29.8 2.7 %collective-permute-start.19 = (bf16[144,512]{1,0:T(8,128)(2,1)S(1)}, bf16[144,512]{1,0:T(8,128)(2,1)S(1)}, u32[]{:S(2)}, u32[]{:S(2)}) collective-permute-start(bf16[144,512]{1,0:T(8,128)(2,1)S(1)} %collective-permute-done.17.refs_1_), channel_id=1, source_target_pairs={{0,224},{32,0},{64,32},{96,64},{128,96},{160,128},{192,160},{224,1... | collective-permute-start | bytes 442376 | tf_op jit(solution)/shard_map/ppermute | solution.py:52
  34.1 2.2 %norm.1.refs_0_ = bf16[4,128,512]{2,1,0:T(8,128)(2,1)S(1)} custom-call(s32[4]{0:T(128)S(1)} %copy-done.14, bf16[128,4096]{1,0:T(8,128)(2,1)S(1)} %bitcast.11, f32[1,4096]{1,0:T(1,128)S(1)} %bitcast.12), custom_call_target="tpu_custom_call" | custom-call | tf_op jit(solution)/shard_map/norm/pallas_call | solution.py:172
  37.6 2.7 %collective-permute-start.2 = (bf16[4,128,512]{2,1,0:T(8,128)(2,1)S(1)}, bf16[4,128,512]{2,1,0:T(8,128)(2,1)S(1)}, u32[]{:S(2)}, u32[]{:S(2)}) collective-permute-start(bf16[4,128,512]{2,1,0:T(8,128)(2,1)S(1)} %norm.1.refs_0_), channel_id=1, source_target_pairs={{0,24},{8,0},{16,8},{24,16},{1,25},{9,1},{17,9},{25,17},{2,26},{10... | collective-permute-start | bytes 1572872 | tf_op jit(solution)/shard_map/ppermute | solution.py:449
  40.2 2.3 %collective-permute-start.21 = (bf16[144,512]{1,0:T(8,128)(2,1)S(1)}, bf16[144,512]{1,0:T(8,128)(2,1)S(1)}, u32[]{:S(2)}, u32[]{:S(2)}) collective-permute-start(bf16[144,512]{1,0:T(8,128)(2,1)S(1)} %collective-permute-done.19.refs_3_.refs_2_), channel_id=1, source_target_pairs={{0,224},{32,0},{64,32},{96,64},{128,96},{160,128},{192,160},{224,1... | collective-permute-start | bytes 442376 | tf_op jit(solution)/shard_map/ppermute | solution.py:52
  44.7 5.1 %collective-permute-done.26.refs_4_ = bf16[144,512]{1,0:T(8,128)(2,1)S(1)} collective-permute-done((bf16[144,512]{1,0:T(8,128)(2,1)S(1)}, bf16[144,512]{1,0:T(8,128)(2,1)S(1)}, u32[]{:S(2)}, u32[]{:S(2)}) %collective-permute-start.26) | collective-permute-done | bytes 147488 | tf_op jit(solution)/shard_map/ppermute | solution.py:55
  51.6 9.6 %collective-permute-done.refs_1_ = bf16[4,128,512]{2,1,0:T(8,128)(2,1)S(1)} collective-permute-done((bf16[4,128,512]{2,1,0:T(8,128)(2,1)S(1)}, bf16[4,128,512]{2,1,0:T(8,128)(2,1)S(1)}, u32[]{:S(2)}, u32[]{:S(2)}) %collective-permute-start) | collective-permute-done | bytes 524320 | tf_op jit(solution)/shard_map/ppermute | solution.py:449
  63.0 3.2 %collective-permute-start.22 = (bf16[384,512]{1,0:T(8,128)(2,1)S(1)}, bf16[384,512]{1,0:T(8,128)(2,1)}, u32[]{:S(2)}, u32[]{:S(2)}) collective-permute-start(bf16[384,512]{1,0:T(8,128)(2,1)S(1)} %split_early.1.refs_4_), channel_id=1, source_target_pairs={{0,2},{2,4},{4,6},{6,0},{1,3},{3,5},{5,7},{7,1},{8,10},{10,12},{12... | collective-permute-start | bytes 1179656 | tf_op jit(solution)/shard_map/ppermute | solution.py:43
  70.8 16.8 %collective-permute-done.29.refs_11_ = bf16[128,512]{1,0:T(8,128)(2,1)S(1)} collective-permute-done((bf16[128,512]{1,0:T(8,128)(2,1)S(1)}, bf16[128,512]{1,0:T(8,128)(2,1)S(1)}, u32[]{:S(2)}, u32[]{:S(2)}) %collective-permute-start.29) | collective-permute-done | bytes 131104 | tf_op jit(solution)/shard_map/ppermute | solution.py:43
  93.5 2.5 %project_kv.1 = (f32[512,256]{1,0:T(8,128)S(1)}, f32[512,128]{1,0:T(8,128)S(1)}, bf16[512,384]{1,0:T(8,128)(2,1)S(1)}) custom-call(s32[4]{0:T(128)S(1)} %copy-done.14, bf16[4,128,512]{2,1,0:T(8,128)(2,1)S(1)} %norm.1.refs_0_, bf16[4,128,512]{2,1,0:T(8,128)(2,1)S(1)} %collective-permute-done.refs_1_, bf16[4,128,512]{2,1,0:T(8,128)(2,1)S(1)} %collective-permute-done.1.refs_2_, ...), custom_call_target="tpu_custom_call" | custom-call | tf_op jit(solution)/shard_map/project_kv/pallas_call | solution.py:240
  96.0 2.1 %collective-permute-start.30 = (bf16[512,384]{1,0:T(8,128)(2,1)S(1)}, bf16[512,384]{1,0:T(8,128)(2,1)S(1)}, u32[]{:S(2)}, u32[]{:S(2)}) collective-permute-start(bf16[512,384]{1,0:T(8,128)(2,1)S(1)} %get-tuple-element.47), channel_id=1, source_target_pairs={{0,1},{1,0},{2,3},{3,2},{4,5},{5,4},{6,7},{7,6},{8,9},{9,8},{10,11... | collective-permute-start | bytes 1179656 | tf_op jit(solution)/shard_map/ppermute | solution.py:39
  98.2 2.4 %project_pq.1 = (f32[512,512]{1,0:T(8,128)S(1)}, bf16[512,512]{1,0:T(8,128)(2,1)S(1)}) custom-call(s32[4]{0:T(128)S(1)} %copy-done.14, bf16[4,128,512]{2,1,0:T(8,128)(2,1)S(1)} %norm.1.refs_0_, bf16[4,128,512]{2,1,0:T(8,128)(2,1)S(1)} %collective-permute-done.refs_1_, bf16[4,128,512]{2,1,0:T(8,128)(2,1)S(1)} %collective-permute-done.1.refs_2_, ...), custom_call_target="tpu_custom_call" | custom-call | tf_op jit(solution)/shard_map/project_pq/pallas_call | solution.py:262
  106.8 4.1 %collective-permute-start.33 = (bf16[256,128]{1,0:T(8,128)(2,1)S(1)}, bf16[256,128]{1,0:T(8,128)(2,1)S(1)}, u32[]{:S(2)}, u32[]{:S(2)}) collective-permute-start(bf16[256,128]{1,0:T(8,128)(2,1)S(1)} %get-tuple-element.55), channel_id=1, source_target_pairs={{0,64},{32,96},{64,128},{96,160},{128,192},{160,224},{1,65},{33,97... | collective-permute-start | bytes 196616 | tf_op jit(solution)/shard_map/ppermute | solution.py:470
  110.8 3.4 %collective-permute-start.34 = (bf16[256,128]{1,0:T(8,128)(2,1)S(1)}, bf16[256,128]{1,0:T(8,128)(2,1)S(1)}, u32[]{:S(2)}, u32[]{:S(2)}) collective-permute-start(bf16[256,128]{1,0:T(8,128)(2,1)S(1)} %get-tuple-element.55), channel_id=1, source_target_pairs={{0,96},{32,128},{64,160},{96,192},{128,224},{1,97},{33,129},{65,16... | collective-permute-start | bytes 196616 | tf_op jit(solution)/shard_map/ppermute | solution.py:470
  114.2 2.2 %collective-permute-start.40 = (bf16[512,512]{1,0:T(8,128)(2,1)S(1)}, bf16[512,512]{1,0:T(8,128)(2,1)S(1)}, u32[]{:S(2)}, u32[]{:S(2)}) collective-permute-start(bf16[512,512]{1,0:T(8,128)(2,1)S(1)} %get-tuple-element.56.refs_0_), channel_id=1, source_target_pairs={{0,2},{2,4},{4,6},{6,0},{1,3},{3,5},{5,7},{7,1},{8,10},{10,12},{12... | collective-permute-start | bytes 1572872 | tf_op jit(solution)/shard_map/ppermute | solution.py:43
  116.5 2.5 %collective-permute-start.41 = (bf16[512,512]{1,0:T(8,128)(2,1)S(1)}, bf16[512,512]{1,0:T(8,128)(2,1)S(1)}, u32[]{:S(2)}, u32[]{:S(2)}) collective-permute-start(bf16[512,512]{1,0:T(8,128)(2,1)S(1)} %get-tuple-element.56.refs_0_), channel_id=1, source_target_pairs={{0,4},{2,6},{4,0},{6,2},{1,5},{3,7},{5,1},{7,3},{8,12},{10,14},{12... | collective-permute-start | bytes 1572872 | tf_op jit(solution)/shard_map/ppermute | solution.py:43
  119.0 5.0 %collective-permute-start.35 = (bf16[256,128]{1,0:T(8,128)(2,1)S(1)}, bf16[256,128]{1,0:T(8,128)(2,1)S(1)}, u32[]{:S(2)}, u32[]{:S(2)}) collective-permute-start(bf16[256,128]{1,0:T(8,128)(2,1)S(1)} %get-tuple-element.55), channel_id=1, source_target_pairs={{0,128},{32,160},{64,192},{96,224},{1,129},{33,161},{65,193},{97,2... | collective-permute-start | bytes 196616 | tf_op jit(solution)/shard_map/ppermute | solution.py:470
  125.3 11.1 %collective-permute-start.36 = (bf16[256,128]{1,0:T(8,128)(2,1)S(1)}, bf16[256,128]{1,0:T(8,128)(2,1)S(1)}, u32[]{:S(2)}, u32[]{:S(2)}) collective-permute-start(bf16[256,128]{1,0:T(8,128)(2,1)S(1)} %get-tuple-element.55), channel_id=1, source_target_pairs={{0,160},{32,192},{64,224},{1,161},{33,193},{65,225},{2,162},{34,19... | collective-permute-start | bytes 196616 | tf_op jit(solution)/shard_map/ppermute | solution.py:470
  143.7 4.2 %collective-permute-start.39 = (f32[512,128]{1,0:T(8,128)S(1)}, f32[512,128]{1,0:T(8,128)S(1)}, u32[]{:S(2)}, u32[]{:S(2)}) collective-permute-start(f32[512,128]{1,0:T(8,128)S(1)} %across.1.ret), channel_id=1, source_target_pairs={{0,1},{1,0},{2,3},{3,2},{4,5},{5,4},{6,7},{7,6},{8,9},{9,8},{10,11... | collective-permute-start | bytes 786440 | tf_op jit(solution)/shard_map/ppermute | solution.py:39
  151.3 2.2 %back.1 = (bf16[64,2048]{1,0:T(8,128)(2,1)S(1)}, bf16[64,2048]{1,0:T(8,128)(2,1)S(1)}, bf16[64,2048]{1,0:T(8,128)(2,1)S(1)}, bf16[64,2048]{1,0:T(8,128)(2,1)S(1)...) custom-call(s32[4]{0:T(128)S(1)} %copy-done.14, ...), custom_call_target="tpu_custom_call" | custom-call | tf_op jit(solution)/shard_map/back/pallas_call | solution.py:396
  155.2 3.4 %collective-permute-start.46 = (bf16[64,2048]{1,0:T(8,128)(2,1)S(1)}, bf16[64,2048]{1,0:T(8,128)(2,1)S(1)}, u32[]{:S(2)}, u32[]{:S(2)}) collective-permute-start(bf16[64,2048]{1,0:T(8,128)(2,1)S(1)} %get-tuple-element.61), channel_id=1, source_target_pairs={{0,16},{1,17},{8,24},{9,25},{16,0},{17,1},{24,8},{25,9},{2,18},{3,... | collective-permute-start | bytes 786440 | tf_op jit(solution)/shard_map/ppermute | solution.py:486
  158.7 2.7 %collective-permute-start.48 = (bf16[64,2048]{1,0:T(8,128)(2,1)S(1)}, bf16[64,2048]{1,0:T(8,128)(2,1)S(1)}, u32[]{:S(2)}, u32[]{:S(2)}) collective-permute-start(bf16[64,2048]{1,0:T(8,128)(2,1)S(1)} %get-tuple-element.63), channel_id=1, source_target_pairs={{0,24},{1,25},{8,0},{9,1},{16,8},{17,9},{24,16},{25,17},{2,26},{3,... | collective-permute-start | bytes 786440 | tf_op jit(solution)/shard_map/ppermute | solution.py:486
  163.5 2.3 %collective-permute-start.49 = (bf16[64,2048]{1,0:T(8,128)(2,1)S(1)}, bf16[64,2048]{1,0:T(8,128)(2,1)S(1)}, u32[]{:S(2)}, u32[]{:S(2)}) collective-permute-start(bf16[64,2048]{1,0:T(8,128)(2,1)S(1)} %get-tuple-element.64), channel_id=1, source_target_pairs={{0,25},{1,24},{8,1},{9,0},{16,9},{17,8},{24,17},{25,16},{2,27},{3,... | collective-permute-start | bytes 786440 | tf_op jit(solution)/shard_map/ppermute | solution.py:486
  165.8 3.5 %collective-permute-done.45.refs_3_ = bf16[64,2048]{1,0:T(8,128)(2,1)S(1)} collective-permute-done((bf16[64,2048]{1,0:T(8,128)(2,1)S(1)}, bf16[64,2048]{1,0:T(8,128)(2,1)S(1)}, u32[]{:S(2)}, u32[]{:S(2)}) %collective-permute-start.45) | collective-permute-done | bytes 262176 | tf_op jit(solution)/shard_map/ppermute | solution.py:486
  169.3 6.0 %collective-permute-done.46.refs_4_ = bf16[64,2048]{1,0:T(8,128)(2,1)S(1)} collective-permute-done((bf16[64,2048]{1,0:T(8,128)(2,1)S(1)}, bf16[64,2048]{1,0:T(8,128)(2,1)S(1)}, u32[]{:S(2)}, u32[]{:S(2)}) %collective-permute-start.46) | collective-permute-done | bytes 262176 | tf_op jit(solution)/shard_map/ppermute | solution.py:486
  175.4 5.9 %collective-permute-done.47.refs_5_ = bf16[64,2048]{1,0:T(8,128)(2,1)S(1)} collective-permute-done((bf16[64,2048]{1,0:T(8,128)(2,1)S(1)}, bf16[64,2048]{1,0:T(8,128)(2,1)S(1)}, u32[]{:S(2)}, u32[]{:S(2)}) %collective-permute-start.47) | collective-permute-done | bytes 262176 | tf_op jit(solution)/shard_map/ppermute | solution.py:486
  182.1 2.7 %mixed.1 = bf16[64,4096]{1,0:T(8,128)(2,1)} custom-call(s32[4]{0:T(128)S(1)} %copy-done.14, bf16[64,2048]{1,0:T(8,128)(2,1)S(1)} %get-tuple-element.57.refs_0_, bf16[64,2048]{1,0:T(8,128)(2,1)S(1)} %collective-permute-done.43.refs_1_, bf16[64,2048]{1,0:T(8,128)(2,1)S(1)} %collective-permute-done.44.refs_2_, ...), custom_call_target="tpu_custom_call" | custom-call | tf_op jit(solution)/shard_map/mixed/pallas_call | solution.py:430
  (130 shorter events, 50.0 us)
Async XLA Ops:
  2.9 9.9 %collective-permute-start.3 = (bf16[112,512]{1,0:T(8,128)(2,1)}, bf16[112,512]{1,0:T(8,128)(2,1)S(1)}, u32[]{:S(2)}, u32[]{:S(2)}) collective-permute-start(bf16[112,512]{1,0:T(8,128)(2,1)} %get-tuple-element.35), channel_id=1, source_target_pairs={{0,0},{1,16},{8,8},{9,24},{16,1},{17,17},{24,9},{25,25},{2,2},{3,1... | collective-permute-start | bytes 344072 | tf_op jit(solution)/shard_map/ppermute | solution.py:443
  15.4 10.5 %collective-permute-start.5 = (bf16[64,512]{1,0:T(8,128)(2,1)S(1)}, bf16[64,512]{1,0:T(8,128)(2,1)S(1)}, u32[]{:S(2)}, u32[]{:S(2)}) collective-permute-start(bf16[64,512]{1,0:T(8,128)(2,1)S(1)} %get-tuple-element.37.a), channel_id=1, source_target_pairs={{0,2},{2,4},{4,6},{6,0},{1,3},{3,5},{5,7},{7,1},{8,10},{10,12},{12... | collective-permute-start | bytes 196616 | tf_op jit(solution)/shard_map/ppermute | solution.py:43
  16.7 9.2 %collective-permute-start.6 = (bf16[64,512]{1,0:T(8,128)(2,1)S(1)}, bf16[64,512]{1,0:T(8,128)(2,1)S(1)}, u32[]{:S(2)}, u32[]{:S(2)}) collective-permute-start(bf16[64,512]{1,0:T(8,128)(2,1)S(1)} %get-tuple-element.37.a), channel_id=1, source_target_pairs={{0,4},{2,6},{4,0},{6,2},{1,5},{3,7},{5,1},{7,3},{8,12},{10,14},{12... | collective-permute-start | bytes 196616 | tf_op jit(solution)/shard_map/ppermute | solution.py:43
  20.3 9.5 %collective-permute-start.18 = (bf16[144,512]{1,0:T(8,128)(2,1)S(1)}, bf16[144,512]{1,0:T(8,128)(2,1)S(1)}, u32[]{:S(2)}, u32[]{:S(2)}) collective-permute-start(bf16[144,512]{1,0:T(8,128)(2,1)S(1)} %get-tuple-element.43.refs_0_), channel_id=1, source_target_pairs={{0,32},{32,64},{64,96},{96,128},{128,160},{160,192},{192,224},{224... | collective-permute-start | bytes 442376 | tf_op jit(solution)/shard_map/ppermute | solution.py:51
  25.9 11.6 %collective-permute-start.11 = (bf16[256,512]{1,0:T(8,128)(2,1)S(1)}, bf16[256,512]{1,0:T(8,128)(2,1)S(1)}, u32[]{:S(2)}, u32[]{:S(2)}) collective-permute-start(bf16[256,512]{1,0:T(8,128)(2,1)S(1)} %join.1.refs_4_), channel_id=1, source_target_pairs={{0,32},{32,64},{64,96},{96,128},{128,160},{160,192},{192,224},{224... | collective-permute-start | bytes 786440 | tf_op jit(solution)/shard_map/ppermute | solution.py:51
  36.3 24.9 %collective-permute-start = (bf16[4,128,512]{2,1,0:T(8,128)(2,1)S(1)}, bf16[4,128,512]{2,1,0:T(8,128)(2,1)S(1)}, u32[]{:S(2)}, u32[]{:S(2)}) collective-permute-start(bf16[4,128,512]{2,1,0:T(8,128)(2,1)S(1)} %norm.1.refs_0_), channel_id=1, source_target_pairs={{0,8},{8,16},{16,24},{24,0},{1,9},{9,17},{17,25},{25,1},{2,10},{10... | collective-permute-start | bytes 1572872 | tf_op jit(solution)/shard_map/ppermute | solution.py:449
  37.6 24.3 %collective-permute-start.1 = (bf16[4,128,512]{2,1,0:T(8,128)(2,1)S(1)}, bf16[4,128,512]{2,1,0:T(8,128)(2,1)S(1)}, u32[]{:S(2)}, u32[]{:S(2)}) collective-permute-start(bf16[4,128,512]{2,1,0:T(8,128)(2,1)S(1)} %norm.1.refs_0_), channel_id=1, source_target_pairs={{0,16},{8,24},{16,0},{24,8},{1,17},{9,25},{17,1},{25,9},{2,18},{10... | collective-permute-start | bytes 1572872 | tf_op jit(solution)/shard_map/ppermute | solution.py:449
  37.6 25.4 %collective-permute-start.2 = (bf16[4,128,512]{2,1,0:T(8,128)(2,1)S(1)}, bf16[4,128,512]{2,1,0:T(8,128)(2,1)S(1)}, u32[]{:S(2)}, u32[]{:S(2)}) collective-permute-start(bf16[4,128,512]{2,1,0:T(8,128)(2,1)S(1)} %norm.1.refs_0_), channel_id=1, source_target_pairs={{0,24},{8,0},{16,8},{24,16},{1,25},{9,1},{17,9},{25,17},{2,26},{10... | collective-permute-start | bytes 1572872 | tf_op jit(solution)/shard_map/ppermute | solution.py:449
  44.7 17.3 %collective-permute-start.12 = (bf16[256,512]{1,0:T(8,128)(2,1)S(1)}, bf16[256,512]{1,0:T(8,128)(2,1)S(1)}, u32[]{:S(2)}, u32[]{:S(2)}) collective-permute-start(bf16[256,512]{1,0:T(8,128)(2,1)S(1)} %collective-permute-done.11.refs_11_), channel_id=1, source_target_pairs={{0,32},{32,64},{64,96},{96,128},{128,160},{160,192},{192,224},{224... | collective-permute-start | bytes 786440 | tf_op jit(solution)/shard_map/ppermute | solution.py:51
  49.8 16.4 %collective-permute-start.9 = (bf16[256,512]{1,0:T(8,128)(2,1)S(1)}, bf16[256,512]{1,0:T(8,128)(2,1)}, u32[]{:S(2)}, u32[]{:S(2)}) collective-permute-start(bf16[256,512]{1,0:T(8,128)(2,1)S(1)} %collective-permute-done.8.refs_5_), channel_id=1, source_target_pairs={{0,224},{32,0},{64,32},{96,64},{128,96},{160,128},{192,160},{224,1... | collective-permute-start | bytes 786440 | tf_op jit(solution)/shard_map/ppermute | solution.py:52
  61.9 27.8 %collective-permute-start.13 = (bf16[256,512]{1,0:T(8,128)(2,1)S(1)}, bf16[256,512]{1,0:T(8,128)(2,1)}, u32[]{:S(2)}, u32[]{:S(2)}) collective-permute-start(bf16[256,512]{1,0:T(8,128)(2,1)S(1)} %collective-permute-done.12.refs_10_), channel_id=1, source_target_pairs={{0,32},{32,64},{64,96},{96,128},{128,160},{160,192},{192,224},{224... | collective-permute-start | bytes 786440 | tf_op jit(solution)/shard_map/ppermute | solution.py:51
  63.0 26.8 %collective-permute-start.22 = (bf16[384,512]{1,0:T(8,128)(2,1)S(1)}, bf16[384,512]{1,0:T(8,128)(2,1)}, u32[]{:S(2)}, u32[]{:S(2)}) collective-permute-start(bf16[384,512]{1,0:T(8,128)(2,1)S(1)} %split_early.1.refs_4_), channel_id=1, source_target_pairs={{0,2},{2,4},{4,6},{6,0},{1,3},{3,5},{5,7},{7,1},{8,10},{10,12},{12... | collective-permute-start | bytes 1179656 | tf_op jit(solution)/shard_map/ppermute | solution.py:43
  66.2 23.6 %collective-permute-start.23 = (bf16[384,512]{1,0:T(8,128)(2,1)S(1)}, bf16[384,512]{1,0:T(8,128)(2,1)}, u32[]{:S(2)}, u32[]{:S(2)}) collective-permute-start(bf16[384,512]{1,0:T(8,128)(2,1)S(1)} %split_early.1.refs_4_), channel_id=1, source_target_pairs={{0,4},{2,6},{4,0},{6,2},{1,5},{3,7},{5,1},{7,3},{8,12},{10,14},{12... | collective-permute-start | bytes 1179656 | tf_op jit(solution)/shard_map/ppermute | solution.py:43
  67.6 22.3 %collective-permute-start.24 = (bf16[384,512]{1,0:T(8,128)(2,1)S(1)}, bf16[384,512]{1,0:T(8,128)(2,1)}, u32[]{:S(2)}, u32[]{:S(2)}) collective-permute-start(bf16[384,512]{1,0:T(8,128)(2,1)S(1)} %split_early.1.refs_4_), channel_id=1, source_target_pairs={{0,6},{2,0},{4,2},{6,4},{1,7},{3,1},{5,3},{7,5},{8,14},{10,8},{12,... | collective-permute-start | bytes 1179656 | tf_op jit(solution)/shard_map/ppermute | solution.py:43
  70.0 17.6 %collective-permute-start.29 = (bf16[128,512]{1,0:T(8,128)(2,1)S(1)}, bf16[128,512]{1,0:T(8,128)(2,1)S(1)}, u32[]{:S(2)}, u32[]{:S(2)}) collective-permute-start(bf16[128,512]{1,0:T(8,128)(2,1)S(1)} %get-tuple-element.44.refs_8_), channel_id=1, source_target_pairs={{0,6},{2,0},{4,2},{6,4},{1,7},{3,1},{5,3},{7,5},{8,14},{10,8},{12,... | collective-permute-start | bytes 393224 | tf_op jit(solution)/shard_map/ppermute | solution.py:43
  88.3 9.9 %collective-permute-start.10 = (bf16[256,512]{1,0:T(8,128)(2,1)}, bf16[256,512]{1,0:T(8,128)(2,1)}, u32[]{:S(2)}, u32[]{:S(2)}) collective-permute-start(bf16[256,512]{1,0:T(8,128)(2,1)} %collective-permute-done.9.refs_6_), channel_id=1, source_target_pairs={{0,224},{32,0},{64,32},{96,64},{128,96},{160,128},{192,160},{224,1... | collective-permute-start | bytes 786440 | tf_op jit(solution)/shard_map/ppermute | solution.py:52
  89.8 8.4 %collective-permute-start.14 = (bf16[256,512]{1,0:T(8,128)(2,1)}, bf16[256,512]{1,0:T(8,128)(2,1)}, u32[]{:S(2)}, u32[]{:S(2)}) collective-permute-start(bf16[256,512]{1,0:T(8,128)(2,1)} %collective-permute-done.13.refs_9_), channel_id=1, source_target_pairs={{0,32},{32,64},{64,96},{96,128},{128,160},{160,192},{192,224},{224... | collective-permute-start | bytes 786440 | tf_op jit(solution)/shard_map/ppermute | solution.py:55
  96.0 8.2 %collective-permute-start.30 = (bf16[512,384]{1,0:T(8,128)(2,1)S(1)}, bf16[512,384]{1,0:T(8,128)(2,1)S(1)}, u32[]{:S(2)}, u32[]{:S(2)}) collective-permute-start(bf16[512,384]{1,0:T(8,128)(2,1)S(1)} %get-tuple-element.47), channel_id=1, source_target_pairs={{0,1},{1,0},{2,3},{3,2},{4,5},{5,4},{6,7},{7,6},{8,9},{9,8},{10,11... | collective-permute-start | bytes 1179656 | tf_op jit(solution)/shard_map/ppermute | solution.py:39
  100.6 38.8 %collective-permute-start.15 = (bf16[512,512]{1,0:T(8,128)(2,1)S(1)}, bf16[512,512]{1,0:T(8,128)(2,1)S(1)}, u32[]{:S(2)}, u32[]{:S(2)}) collective-permute-start(bf16[512,512]{1,0:T(8,128)(2,1)S(1)} %get-tuple-element.39), channel_id=1, source_target_pairs={{0,1},{1,0},{2,3},{3,2},{4,5},{5,4},{6,7},{7,6},{8,9},{9,8},{10,11... | collective-permute-start | bytes 1572872 | tf_op jit(solution)/shard_map/ppermute | solution.py:39
  105.2 11.2 %collective-permute-start.32 = (bf16[256,128]{1,0:T(8,128)(2,1)S(1)}, bf16[256,128]{1,0:T(8,128)(2,1)S(1)}, u32[]{:S(2)}, u32[]{:S(2)}) collective-permute-start(bf16[256,128]{1,0:T(8,128)(2,1)S(1)} %get-tuple-element.55), channel_id=1, source_target_pairs={{0,32},{32,64},{64,96},{96,128},{128,160},{160,192},{192,224},{1,3... | collective-permute-start | bytes 196616 | tf_op jit(solution)/shard_map/ppermute | solution.py:470
  106.8 12.2 %collective-permute-start.33 = (bf16[256,128]{1,0:T(8,128)(2,1)S(1)}, bf16[256,128]{1,0:T(8,128)(2,1)S(1)}, u32[]{:S(2)}, u32[]{:S(2)}) collective-permute-start(bf16[256,128]{1,0:T(8,128)(2,1)S(1)} %get-tuple-element.55), channel_id=1, source_target_pairs={{0,64},{32,96},{64,128},{96,160},{128,192},{160,224},{1,65},{33,97... | collective-permute-start | bytes 196616 | tf_op jit(solution)/shard_map/ppermute | solution.py:470
  110.8 8.1 %collective-permute-start.34 = (bf16[256,128]{1,0:T(8,128)(2,1)S(1)}, bf16[256,128]{1,0:T(8,128)(2,1)S(1)}, u32[]{:S(2)}, u32[]{:S(2)}) collective-permute-start(bf16[256,128]{1,0:T(8,128)(2,1)S(1)} %get-tuple-element.55), channel_id=1, source_target_pairs={{0,96},{32,128},{64,160},{96,192},{128,224},{1,97},{33,129},{65,16... | collective-permute-start | bytes 196616 | tf_op jit(solution)/shard_map/ppermute | solution.py:470
  114.2 37.1 %collective-permute-start.40 = (bf16[512,512]{1,0:T(8,128)(2,1)S(1)}, bf16[512,512]{1,0:T(8,128)(2,1)S(1)}, u32[]{:S(2)}, u32[]{:S(2)}) collective-permute-start(bf16[512,512]{1,0:T(8,128)(2,1)S(1)} %get-tuple-element.56.refs_0_), channel_id=1, source_target_pairs={{0,2},{2,4},{4,6},{6,0},{1,3},{3,5},{5,7},{7,1},{8,10},{10,12},{12... | collective-permute-start | bytes 1572872 | tf_op jit(solution)/shard_map/ppermute | solution.py:43
  116.5 34.9 %collective-permute-start.41 = (bf16[512,512]{1,0:T(8,128)(2,1)S(1)}, bf16[512,512]{1,0:T(8,128)(2,1)S(1)}, u32[]{:S(2)}, u32[]{:S(2)}) collective-permute-start(bf16[512,512]{1,0:T(8,128)(2,1)S(1)} %get-tuple-element.56.refs_0_), channel_id=1, source_target_pairs={{0,4},{2,6},{4,0},{6,2},{1,5},{3,7},{5,1},{7,3},{8,12},{10,14},{12... | collective-permute-start | bytes 1572872 | tf_op jit(solution)/shard_map/ppermute | solution.py:43
  118.9 32.4 %collective-permute-start.42 = (bf16[512,512]{1,0:T(8,128)(2,1)S(1)}, bf16[512,512]{1,0:T(8,128)(2,1)S(1)}, u32[]{:S(2)}, u32[]{:S(2)}) collective-permute-start(bf16[512,512]{1,0:T(8,128)(2,1)S(1)} %get-tuple-element.56.refs_0_), channel_id=1, source_target_pairs={{0,6},{2,0},{4,2},{6,4},{1,7},{3,1},{5,3},{7,5},{8,14},{10,8},{12,... | collective-permute-start | bytes 1572872 | tf_op jit(solution)/shard_map/ppermute | solution.py:43
  125.3 12.9 %collective-permute-start.36 = (bf16[256,128]{1,0:T(8,128)(2,1)S(1)}, bf16[256,128]{1,0:T(8,128)(2,1)S(1)}, u32[]{:S(2)}, u32[]{:S(2)}) collective-permute-start(bf16[256,128]{1,0:T(8,128)(2,1)S(1)} %get-tuple-element.55), channel_id=1, source_target_pairs={{0,160},{32,192},{64,224},{1,161},{33,193},{65,225},{2,162},{34,19... | collective-permute-start | bytes 196616 | tf_op jit(solution)/shard_map/ppermute | solution.py:470
  154.5 9.0 %collective-permute-start.44 = (bf16[64,2048]{1,0:T(8,128)(2,1)S(1)}, bf16[64,2048]{1,0:T(8,128)(2,1)S(1)}, u32[]{:S(2)}, u32[]{:S(2)}) collective-permute-start(bf16[64,2048]{1,0:T(8,128)(2,1)S(1)} %get-tuple-element.59), channel_id=1, source_target_pairs={{0,8},{1,9},{8,16},{9,17},{16,24},{17,25},{24,0},{25,1},{2,10},{3,... | collective-permute-start | bytes 786440 | tf_op jit(solution)/shard_map/ppermute | solution.py:486
  155.2 14.2 %collective-permute-start.45 = (bf16[64,2048]{1,0:T(8,128)(2,1)S(1)}, bf16[64,2048]{1,0:T(8,128)(2,1)S(1)}, u32[]{:S(2)}, u32[]{:S(2)}) collective-permute-start(bf16[64,2048]{1,0:T(8,128)(2,1)S(1)} %get-tuple-element.60), channel_id=1, source_target_pairs={{0,9},{1,8},{8,17},{9,16},{16,25},{17,24},{24,1},{25,0},{2,11},{3,... | collective-permute-start | bytes 786440 | tf_op jit(solution)/shard_map/ppermute | solution.py:486
  155.2 20.1 %collective-permute-start.46 = (bf16[64,2048]{1,0:T(8,128)(2,1)S(1)}, bf16[64,2048]{1,0:T(8,128)(2,1)S(1)}, u32[]{:S(2)}, u32[]{:S(2)}) collective-permute-start(bf16[64,2048]{1,0:T(8,128)(2,1)S(1)} %get-tuple-element.61), channel_id=1, source_target_pairs={{0,16},{1,17},{8,24},{9,25},{16,0},{17,1},{24,8},{25,9},{2,18},{3,... | collective-permute-start | bytes 786440 | tf_op jit(solution)/shard_map/ppermute | solution.py:486
  158.6 22.7 %collective-permute-start.47 = (bf16[64,2048]{1,0:T(8,128)(2,1)S(1)}, bf16[64,2048]{1,0:T(8,128)(2,1)S(1)}, u32[]{:S(2)}, u32[]{:S(2)}) collective-permute-start(bf16[64,2048]{1,0:T(8,128)(2,1)S(1)} %get-tuple-element.62), channel_id=1, source_target_pairs={{0,17},{1,16},{8,25},{9,24},{16,1},{17,0},{24,9},{25,8},{2,19},{3,... | collective-permute-start | bytes 786440 | tf_op jit(solution)/shard_map/ppermute | solution.py:486
  158.7 22.5 %collective-permute-start.48 = (bf16[64,2048]{1,0:T(8,128)(2,1)S(1)}, bf16[64,2048]{1,0:T(8,128)(2,1)S(1)}, u32[]{:S(2)}, u32[]{:S(2)}) collective-permute-start(bf16[64,2048]{1,0:T(8,128)(2,1)S(1)} %get-tuple-element.63), channel_id=1, source_target_pairs={{0,24},{1,25},{8,0},{9,1},{16,8},{17,9},{24,16},{25,17},{2,26},{3,... | collective-permute-start | bytes 786440 | tf_op jit(solution)/shard_map/ppermute | solution.py:486
  163.5 18.7 %collective-permute-start.49 = (bf16[64,2048]{1,0:T(8,128)(2,1)S(1)}, bf16[64,2048]{1,0:T(8,128)(2,1)S(1)}, u32[]{:S(2)}, u32[]{:S(2)}) collective-permute-start(bf16[64,2048]{1,0:T(8,128)(2,1)S(1)} %get-tuple-element.64), channel_id=1, source_target_pairs={{0,25},{1,24},{8,1},{9,0},{16,9},{17,8},{24,17},{25,16},{2,27},{3,... | collective-permute-start | bytes 786440 | tf_op jit(solution)/shard_map/ppermute | solution.py:486
  (39 other events, 197.3 us)
